TPU v7x, 256 devices: a whole 4x4x8 slice. The times are simulated.
256 devices in a mesh: sp: 64 (over z, x, core), tp: 4 (over y).
Axes of the slice: x: 4, y: 4, z: 8, core: 2. Of those that a mesh axis runs over, the one named last changes fastest.
Arguments:
- tokens: bfloat16 [16384, 2048], P(('sp', 'tp')), may hold values from -6 to 6
- query_weight: bfloat16 [2048, 2048], P('sp', 'tp'), may hold values from -0.125 to 0.125
- key_weight: bfloat16 [2048, 512], P('sp', 'tp'), may hold values from -0.125 to 0.125
- value_weight: bfloat16 [2048, 512], P('sp', 'tp'), may hold values from -0.125 to 0.125
- out_weight: bfloat16 [2048, 2048], P('tp', 'sp'), may hold values from -0.125 to 0.125
- query_gain: float32 [128], replicated, may hold values from 0.1 to 1.9
- key_gain: float32 [128], replicated, may hold values from 0.1 to 1.9
Outputs:
- mixed: bfloat16 [16384, 2048], P(('sp', 'tp'))
All inputs are finite; a program needn't handle non-finite values.
Results may differ from a plain program's by a relative error of at most 0.02.
Values may be sent and summed in bfloat16 or wider, within the bound.
No kernel may reach another device: no remote copies, remote signals or barrier semaphores. Data moves between devices by JAX's collectives and lax.ppermute only.
A program may use at most 64 MiB of HBM per device.

v0:
```python
import functools
import math

import jax
import jax.numpy as jnp
from jax import lax
from jax.experimental import pallas as pl
from jax.experimental.pallas import tpu as pltpu
from jax.sharding import Mesh
from jax.sharding import PartitionSpec as P


HEAD_DIM = 128
GROUP = 4
GRID_W = 64
Z, X, C, Y = "sp_0", "sp_1", "sp_2", "tp"
SP = (Z, X, C)
SP_TP = (Z, X, C, Y)
NZ, NX, NC, NY = 8, 4, 2, 4

eps = 1e-06
rope_base = 10000.0

F32 = jnp.float32
BF16 = jnp.bfloat16
WHOLE = pl.BlockSpec(memory_space=pltpu.VMEM)
SCALARS = pl.BlockSpec(memory_space=pltpu.SMEM)


def other_core(piece):
    return lax.ppermute(piece, C, [(0, 1), (1, 0)])


def turn(piece, axis, count):
    pairs = []
    for i in range(count):
        pairs += [(i * 2, (i + 1) % count * 2), (i * 2 + 1, (i - 1) % count * 2 + 1)]
    return lax.ppermute(piece, (axis, C), pairs)


def shift(piece, axis, count, by):
    return lax.ppermute(piece, axis, [(i, (i + by) % count) for i in range(count)])


def leap(piece, by):
    pairs = []
    for i in range(NZ):
        pairs += [(i * 2, (i + by) % NZ * 2), (i * 2 + 1, (i - by) % NZ * 2 + 1)]
    return lax.ppermute(piece, (Z, C), pairs)


def everyone(piece, axes):
    n = lax.axis_size(axes)
    return lax.all_to_all(jnp.broadcast_to(piece[None], (n,) + piece.shape), axes, 0, 0)


def after(value, *events):
    return lax.optimization_barrier((value, *events))[0]


def call(kernel, outs, *args, scratch=(), flops=0):
    return pl.pallas_call(
        kernel,
        in_specs=[SCALARS] + [WHOLE] * (len(args) - 1),
        out_specs=[WHOLE] * len(outs),
        out_shape=[jax.ShapeDtypeStruct(s, d) for s, d in outs],
        scratch_shapes=list(scratch),
        compiler_params=pltpu.CompilerParams(vmem_limit_bytes=40 * 2**20),
        cost_estimate=pl.CostEstimate(flops=flops, bytes_accessed=4 * 2**20, transcendentals=0),
    )(*args)


def at(index, size):
    return pl.ds(pl.multiple_of(index * size, size), size)


def column_kernel(i_ref, own_ref, other_ref, mine_ref, got_ref, q_ref, q_half_ref, o_ref, o_half_ref):
    z, c = i_ref[0], i_ref[2]
    away = 1 - 2 * c
    width = q_ref.shape[1]

    def put(ref, start, plane, half):
        place = at(half * NZ + (plane + 2 * NZ) % NZ, 32)
        q_ref[place, :] = ref[start : start + 32, :width]
        o_ref[place, :] = ref[start : start + 32, width:]

    put(own_ref, 0, z, c)
    put(other_ref, 0, z, 1 - c)
    for s in range(1, 4):
        for j in range(2):
            half = jnp.where(c == 0, j, 1 - j)
            start = s * 64 - 64 + j * 32
            put(mine_ref, start, z - away * s, half)
            put(got_ref, start, z + away * s, 1 - half)
    put(mine_ref, 192, z + 4, c)
    put(got_ref, 192, z + 4, 1 - c)
    q_half_ref[...] = q_ref[at(c, 256), :]
    o_half_ref[...] = o_ref[at(c, 256), :]


def fill_rows(i_ref, w_ref, column, rest, got):
    x, c = i_ref[1], i_ref[2]
    minus = (x + jnp.where(c == 0, 3, 1)) % NX
    plus = (x + jnp.where(c == 0, 1, 3)) % NX
    opposite = (x + 2) % NX

    def plane(z, nothing):
        row = pl.multiple_of(z * 32, 32)
        for k in range(2):
            place = pl.ds(row + k * 256, 32)
            for ref, where in ((column, x), (rest, minus), (got, plus)):
                w_ref[at((z * NX + where) * 2 + k, 32), :] = ref[place, :]
        w_ref[at((z * NX + opposite) * 2 + c, 32), :] = rest[pl.ds(row + 512, 32), :]
        w_ref[at((z * NX + opposite) * 2 + 1 - c, 32), :] = got[pl.ds(row + 512, 32), :]
        return nothing

    lax.fori_loop(0, NZ, plane, 0)


def rotated(raw, gain, cosine, sine, scale):
    wide = raw.astype(F32)
    n = wide * lax.rsqrt(jnp.mean(wide * wide, axis=-1, keepdims=True) + eps) * gain
    lane = lax.broadcasted_iota(jnp.int32, n.shape, 1)
    swapped = jnp.where(lane // 32 % 2 == 0, pltpu.roll(n, 96, 1), pltpu.roll(n, 32, 1))
    return ((n * cosine + swapped * sine) * scale).astype(BF16)


def kv_kernel(i_ref, t0, t1, t2, t3, own, got, gain, cosine, sine, kv_ref, t_ref, w_ref):
    c, y = i_ref[2], i_ref[3]
    for by, ref in enumerate((t0, t1, t2, t3)):
        t_ref[at((y + by) % NY, 64), :] = ref[...]

    def chip(i, nothing):
        for k in range(4):
            w_ref[at((i * 4 + k) * 2 + c, 32), :] = own[i * 4 + k]
            w_ref[at((i * 4 + k) * 2 + 1 - c, 32), :] = got[i * 4 + k]
        return nothing

    lax.fori_loop(0, NZ * NX // 4, chip, 0)
    raw = jnp.dot(t_ref[...], w_ref[...], preferred_element_type=F32).astype(BF16)
    kv_ref[:, :HEAD_DIM] = rotated(raw[:, :HEAD_DIM], gain[...], cosine[...], sine[...], 1.0)
    kv_ref[:, HEAD_DIM:] = raw[:, HEAD_DIM:]


def q_kernel(i_ref, t_ref, column, rest, got, gain, cosine, sine, q_ref, w_ref):
    fill_rows(i_ref, w_ref, column, rest, got)
    raw = jnp.dot(t_ref[...], w_ref[...], preferred_element_type=F32).astype(BF16)
    rows = raw.shape[0]
    scale = HEAD_DIM ** (-0.5) * math.log2(math.e)
    for h in range(GROUP):
        head = raw[:, h * HEAD_DIM : (h + 1) * HEAD_DIM]
        q_ref[h * rows : (h + 1) * rows, :] = rotated(head, gain[...], cosine[...], sine[...], scale)


def attend_kernel(*refs, pieces, first, last, offset):
    q_ref, *kv_refs = refs[: 1 + pieces]
    ins = refs[1 + pieces : 1 + pieces + (0 if first else 2)]
    *outs, k_ref, v_ref = refs[1 + pieces + len(ins) :]
    out_ref, m_ref, a_ref = outs if last else (None, *outs)
    if first:
        m_ref[...] = jnp.full(m_ref.shape, -1e30, F32)
        a_ref[...] = jnp.zeros(a_ref.shape, F32)
    else:
        kept = slice(offset, offset + m_ref.shape[0])
        m_ref[...] = ins[0][kept]
        a_ref[...] = ins[1][kept]
    for i, ref in enumerate(kv_refs):
        k_ref[i] = ref[:, :HEAD_DIM]
        v_ref[i, :, :HEAD_DIM] = ref[:, HEAD_DIM:]
        v_ref[i, :, HEAD_DIM:] = jnp.ones((ref.shape[0], HEAD_DIM), BF16)
    sub, chunk = 128, 1024
    steps = a_ref.shape[0] // chunk

    def part(t, nothing):
        piece, base = t // steps, t % steps * chunk

        def rows(r, start=0):
            return pl.ds(pl.multiple_of(base + r, sub) + start, sub)

        def scores(r):
            return lax.dot_general(
                q_ref[rows(r, offset)], k_ref[piece], (((1,), (1,)), ((), ())), preferred_element_type=F32
            )

        following = scores(0)
        for r in range(0, chunk, sub):
            s = following
            if r + sub < chunk:
                following = scores(r + sub)
            old = m_ref[rows(r), :1]
            best = jnp.maximum(jnp.max(s, axis=1, keepdims=True), old)
            weights = jnp.exp2(s - best).astype(BF16)
            acc = jnp.dot(weights, v_ref[piece], preferred_element_type=F32)
            acc = acc + a_ref[rows(r)] * jnp.exp2(old - best)
            m_ref[rows(r)] = jnp.broadcast_to(best, (sub, HEAD_DIM))
            a_ref[rows(r)] = acc
        return nothing

    if steps * pieces == 1:
        part(0, 0)
    else:
        lax.fori_loop(0, steps * pieces, part, 0)
    if last:
        lane = lax.broadcasted_iota(jnp.int32, m_ref.shape, 1)
        out_ref[:, :HEAD_DIM] = a_ref[:, :HEAD_DIM]
        out_ref[:, HEAD_DIM:] = jnp.where(lane < 64, a_ref[:, HEAD_DIM:], m_ref[...])


def attend(q, kvs, carry, last=None):
    first, count = carry is None, kvs[0].shape[0]
    rows = q.shape[0] // (1 if last is None else 2)
    shapes = [jax.ShapeDtypeStruct((rows, n), F32) for n in ((HEAD_DIM, 2 * HEAD_DIM) if last is None else (2 * HEAD_DIM,))]
    pieces = len(kvs)
    out = pl.pallas_call(
        functools.partial(attend_kernel, pieces=pieces, first=first, last=last is not None, offset=(last or 0) * rows),
        in_specs=[WHOLE] * (1 + pieces + (0 if first else 2)),
        out_specs=[WHOLE] * len(shapes),
        out_shape=shapes,
        scratch_shapes=([] if last is None else [pltpu.VMEM((rows, HEAD_DIM), F32), pltpu.VMEM((rows, 2 * HEAD_DIM), F32)])
        + [
            pltpu.VMEM((pieces, count, HEAD_DIM), BF16),
            pltpu.VMEM((pieces, count, 2 * HEAD_DIM), BF16),
        ],
        input_output_aliases={} if first or last is not None else {1 + pieces: 0, 2 + pieces: 1},
        compiler_params=pltpu.CompilerParams(vmem_limit_bytes=40 * 2**20),
        cost_estimate=pl.CostEstimate(
            flops=8 * rows * count * HEAD_DIM * pieces, bytes_accessed=8 * 2**20, transcendentals=rows * count
        ),
        name="attend",
    )(q, *kvs, *([] if first else carry))
    return out if last is None else out[0]


def project_out_kernel(i_ref, own_ref, got_ref, column, rest, rest_got, out_ref, w_ref, at_ref):
    fill_rows(i_ref, w_ref, column, rest, rest_got)
    rows = own_ref.shape[0] // GROUP
    for h in range(GROUP):
        mine, theirs = own_ref[h * rows : (h + 1) * rows], got_ref[h * rows : (h + 1) * rows]
        best_a, best_b = mine[:, 255:256], theirs[:, 255:256]
        top = jnp.maximum(best_a, best_b)
        both = mine * jnp.exp2(best_a - top) + theirs * jnp.exp2(best_b - top)
        at_ref[:, h * HEAD_DIM : (h + 1) * HEAD_DIM] = (both[:, :HEAD_DIM] / both[:, HEAD_DIM : HEAD_DIM + 1]).astype(BF16)
    out_ref[...] = lax.dot_general(
        at_ref[...], w_ref[...], (((1,), (1,)), ((), ())), preferred_element_type=F32
    ).astype(BF16)


def tables(positions):
    lane = jnp.arange(HEAD_DIM)
    f = lane % 32
    inverse_rate = rope_base ** (-(2 * f).astype(F32) / 64)
    row = (positions // GRID_W).astype(F32)
    column = (positions % GRID_W).astype(F32)
    place = jnp.where(lane[None] < 64, row[:, None], column[:, None])
    angle = place * inverse_rate[None]
    return jnp.cos(angle), jnp.sin(angle) * jnp.where((lane // 32) % 2 == 0, -1.0, 1.0)


def from_x(column, half):
    rest = jnp.concatenate([turn(column, X, NX), shift(half, X, NX, 2)], axis=0)
    return column, rest, other_core(rest)


def local(tokens, query_weight, key_weight, value_weight, out_weight, query_gain, key_gain):
    where = jnp.stack([lax.axis_index(a) for a in (Z, X, C, Y)]).astype(jnp.int32)
    rows = tokens.shape[0] * NY
    positions = lax.axis_index(SP) * rows + jnp.arange(rows, dtype=jnp.int32)
    cosine, sine = tables(positions)
    gain_q, gain_k = query_gain[None], key_gain[None]

    kv_weight = everyone(jnp.concatenate([key_weight, value_weight], axis=1), (Z, X))
    w_own = jnp.concatenate([query_weight, out_weight.T], axis=1)
    w_other = other_core(w_own)
    slab = jnp.concatenate([w_own, w_other], axis=0)
    leaps = leap(slab, 1), leap(slab, 2), leap(slab, 3), leap(w_own, 4)
    toks = [tokens] + [shift(tokens, Y, NY, -by) for by in (1, 2, 3)]
    kv_got = other_core(kv_weight)

    kv_own, rows_in = call(
        kv_kernel, [((rows, 256), BF16), ((rows, tokens.shape[1]), BF16)],
        where, *toks, kv_weight, kv_got, gain_k, cosine, sine,
        scratch=[pltpu.VMEM((tokens.shape[1], 256), BF16)],
    )
    mine = jnp.concatenate(after(leaps, kv_own), axis=0)
    got = other_core(mine)
    q_column, q_half, wo_column, wo_half = call(
        column_kernel, [((512, 512), BF16), ((256, 512), BF16)] * 2, where, w_own, w_other, mine, got,
    )
    kv_slab = jnp.concatenate([kv_own, other_core(kv_own)], axis=0)
    kv_near, kv_far = turn(kv_slab, X, NX), shift(kv_own, X, NX, 2)
    plane = jnp.concatenate([kv_own, kv_near, kv_far], axis=0)

    (q_own,) = call(
        q_kernel, [((GROUP * rows, HEAD_DIM), BF16)],
        where, rows_in, *from_x(q_column, q_half), gain_q, cosine, sine,
        scratch=[pltpu.VMEM((tokens.shape[1], 512), BF16)],
    )
    q_all = jnp.concatenate([q_own, other_core(q_own)], axis=0)
    wo_all = from_x(*after((wo_column, wo_half), q_own))

    chain = {"a": plane, "b": other_core(plane)}
    carry, todo = None, [plane]
    for step in range(1, 5):
        for name in "ab" if step < 4 else "a":
            chain[name] = turn(chain[name], Z, NZ)
            todo.append(chain[name])
    for at_once in (todo[0:2], todo[2:4], todo[4:6]):
        carry = attend(q_all, at_once, carry)
    theirs = attend(q_all, todo[6:], carry, last=1)
    got = other_core(theirs)
    own = attend(q_all, todo[6:], carry, last=0)
    (partial,) = call(
        project_out_kernel, [((rows, tokens.shape[1]), BF16)], where, own, got, *wo_all,
        scratch=[pltpu.VMEM((2048, 512), BF16), pltpu.VMEM((rows, GROUP * HEAD_DIM), BF16)],
    )
    pieces = partial.reshape(NY, -1, partial.shape[1])
    summed = jnp.sum(lax.all_to_all(pieces, Y, 0, 0).astype(F32), axis=0)
    mixed = summed * lax.rsqrt(jnp.mean(summed * summed, axis=-1, keepdims=True) + eps)
    return mixed.astype(BF16)


def solution(mesh):
    split = Mesh(mesh.devices.reshape(NZ, NX, NC, NY), SP_TP)

    return jax.shard_map(
        local,
        mesh=split,
        in_specs=(P(SP_TP, None), P(SP, Y), P(SP, Y), P(SP, Y), P(Y, SP), P(), P()),
        out_specs=P(SP_TP, None),
        check_vma=False,
    )
```

profile of v0, /device:TPU:2, one launch (start us, length us, event | category | flops | bytes accessed | tf_op | source)
XLA Modules:
  0.0 151.5 jit_solution(5292795087158221948)
XLA Ops:
  0.0 0.8 pad_maximum_fusion.4
  0.8 0.9 broadcast_in_dim.50
  1.6 11.6 %all-to-all-start = ((bf16[32,32,256]{2,1,0:T(8,128)(2,1)}), bf16[32,32,256]{2,1,0:T(8,128)(2,1)S(1)}, u32[]{:S(2)}, u32[]{:S(2)}) async-start(bf16[32,32,256]{2,1,0:T(8,128)(2,1)} %broadcast_in_dim.50), calls=%async_computation | async-start | bytes 1048576 | tf_op jit(solution)/shard_map/all_to_all | solution.py:54
  13.2 3.1 %collective-permute-start = (bf16[64,2048]{1,0:T(8,128)(2,1)}, bf16[64,2048]{1,0:T(8,128)(2,1)S(1)}, u32[]{:S(2)}, u32[]{:S(2)}) collective-permute-start(bf16[64,2048]{1,0:T(8,128)(2,1)} %t0.1), channel_id=1, source_target_pairs={{0,3},{1,0},{2,1},{3,2},{4,7},{5,4},{6,5},{7,6},{8,11},{9,8},{10,9... | collective-permute-start | bytes 786440 | tf_op jit(solution)/shard_map/ppermute | solution.py:42
  16.3 0.6 collective-permute-start.1
  17.0 1.0 collective-permute-start.2
  17.9 0.8 pad_maximum_fusion.3.own_ref
  18.8 11.3 %all-to-all-done.own = bf16[32,32,256]{2,1,0:T(8,128)(2,1)S(1)} async-done(((bf16[32,32,256]{2,1,0:T(8,128)(2,1)}), bf16[32,32,256]{2,1,0:T(8,128)(2,1)S(1)}, u32[]{:S(2)}, u32[]{:S(2)}) %all-to-all-start) | async-done | bytes 524320 | tf_op jit(solution)/shard_map/all_to_all | solution.py:54
  30.1 0.8 pad_maximum_fusion.2
  30.9 0.7 collective-permute-start.5
  31.5 1.4 collective-permute-start.6
  32.9 1.8 %collective-permute-start.7 = (bf16[64,1024]{1,0:T(8,128)(2,1)S(1)}, bf16[64,1024]{1,0:T(8,128)(2,1)S(1)}, u32[]{:S(2)}, u32[]{:S(2)}) collective-permute-start(bf16[64,1024]{1,0:T(8,128)(2,1)S(1)} %pad_maximum_fusion.2), channel_id=1, source_target_pairs={{0,96},{4,164},{32,128},{36,196},{64,160},{68,228},{96,192},{100,4... | collective-permute-start | bytes 393224 | tf_op jit(solution)/shard_map/ppermute | solution.py:49
  34.7 0.5 sine_multiply_fusion
  35.3 3.7 %collective-permute-start.8 = (bf16[32,1024]{1,0:T(8,128)(2,1)S(1)}, bf16[32,1024]{1,0:T(8,128)(2,1)S(1)}, u32[]{:S(2)}, u32[]{:S(2)}) collective-permute-start(bf16[32,1024]{1,0:T(8,128)(2,1)S(1)} %pad_maximum_fusion.3.own_ref), channel_id=1, source_target_pairs={{0,128},{4,132},{32,160},{36,164},{64,192},{68,196},{96,224},{100,... | collective-permute-start | bytes 196616 | tf_op jit(solution)/shard_map/ppermute | solution.py:49
  39.1 1.4 shard_map.73
  40.4 4.3 %collective-permute-done.8 = bf16[32,1024]{1,0:T(8,128)(2,1)S(1)} collective-permute-done((bf16[32,1024]{1,0:T(8,128)(2,1)S(1)}, bf16[32,1024]{1,0:T(8,128)(2,1)S(1)}, u32[]{:S(2)}, u32[]{:S(2)}) %collective-permute-start.8) | collective-permute-done | bytes 65568 | tf_op jit(solution)/shard_map/ppermute | solution.py:49
  44.7 0.6 collective-permute-done.7
  45.5 0.5 collective-permute-start.14
  46.0 1.5 collective-permute-done.14
  47.5 1.5 collective-permute-start.15
  48.9 2.4 %collective-permute-start.16 = (bf16[256,256]{1,0:T(8,128)(2,1)S(1)}, bf16[256,256]{1,0:T(8,128)(2,1)S(1)}, u32[]{:S(2)}, u32[]{:S(2)}) collective-permute-start(bf16[256,256]{1,0:T(8,128)(2,1)S(1)} %get-tuple-element.24), channel_id=1, source_target_pairs={{0,16},{8,24},{16,0},{24,8},{1,17},{9,25},{17,1},{25,9},{2,18},{10... | collective-permute-start | bytes 393224 | tf_op jit(solution)/shard_map/ppermute | solution.py:42
  51.4 0.7 shard_map.74
  52.1 3.2 %collective-permute-done.15 = bf16[512,256]{1,0:T(8,128)(2,1)S(1)} collective-permute-done((bf16[512,256]{1,0:T(8,128)(2,1)S(1)}, bf16[512,256]{1,0:T(8,128)(2,1)S(1)}, u32[]{:S(2)}, u32[]{:S(2)}) %collective-permute-start.15) | collective-permute-done | bytes 262176 | tf_op jit(solution)/shard_map/ppermute | solution.py:38
  55.3 1.5 collective-permute-done.16
  57.0 2.9 %collective-permute-start.21 = (bf16[1024,256]{1,0:T(8,128)(2,1)S(1)}, bf16[1024,256]{1,0:T(8,128)(2,1)S(1)}, u32[]{:S(2)}, u32[]{:S(2)}) collective-permute-start(bf16[1024,256]{1,0:T(8,128)(2,1)S(1)} %constant_dynamic-update-slice_fusion.6.refs_1_), channel_id=1, source_target_pairs={{0,32},{4,228},{32,64},{36,4},{64,96},{68,36},{96,128},{100,68},{1... | collective-permute-start | bytes 1572872 | tf_op jit(solution)/shard_map/ppermute | solution.py:38
  59.8 2.5 %collective-permute-start.11 = (bf16[256,512]{1,0:T(8,128)(2,1)S(1)}, bf16[256,512]{1,0:T(8,128)(2,1)S(1)}, u32[]{:S(2)}, u32[]{:S(2)}) collective-permute-start(bf16[256,512]{1,0:T(8,128)(2,1)S(1)} %get-tuple-element.30), channel_id=1, source_target_pairs={{0,16},{8,24},{16,0},{24,8},{1,17},{9,25},{17,1},{25,9},{2,18},{10... | collective-permute-start | bytes 786440 | tf_op jit(solution)/shard_map/ppermute | solution.py:42
  62.4 6.8 %collective-permute-done.11 = bf16[256,512]{1,0:T(8,128)(2,1)S(1)} collective-permute-done((bf16[256,512]{1,0:T(8,128)(2,1)S(1)}, bf16[256,512]{1,0:T(8,128)(2,1)S(1)}, u32[]{:S(2)}, u32[]{:S(2)}) %collective-permute-start.11) | collective-permute-done | bytes 262176 | tf_op jit(solution)/shard_map/ppermute | solution.py:42
  69.4 1.5 collective-permute-start.18
  70.8 2.2 %collective-permute-start.22 = (bf16[1024,256]{1,0:T(8,128)(2,1)S(1)}, bf16[1024,256]{1,0:T(8,128)(2,1)S(1)}, u32[]{:S(2)}, u32[]{:S(2)}) collective-permute-start(bf16[1024,256]{1,0:T(8,128)(2,1)S(1)} %collective-permute-done.21.refs_2_), channel_id=1, source_target_pairs={{0,32},{4,228},{32,64},{36,4},{64,96},{68,36},{96,128},{100,68},{1... | collective-permute-start | bytes 1572872 | tf_op jit(solution)/shard_map/ppermute | solution.py:38
  73.0 6.8 %collective-permute-done.18.refs_1_ = bf16[1024,256]{1,0:T(8,128)(2,1)S(1)} collective-permute-done((bf16[1024,256]{1,0:T(8,128)(2,1)S(1)}, bf16[1024,256]{1,0:T(8,128)(2,1)S(1)}, u32[]{:S(2)}, u32[]{:S(2)}) %collective-permute-start.18) | collective-permute-done | bytes 524320 | tf_op jit(solution)/shard_map/ppermute | solution.py:38
  80.0 5.4 %collective-permute-done.22.refs_2_ = bf16[1024,256]{1,0:T(8,128)(2,1)S(1)} collective-permute-done((bf16[1024,256]{1,0:T(8,128)(2,1)S(1)}, bf16[1024,256]{1,0:T(8,128)(2,1)S(1)}, u32[]{:S(2)}, u32[]{:S(2)}) %collective-permute-start.22) | collective-permute-done | bytes 524320 | tf_op jit(solution)/shard_map/ppermute | solution.py:38
  85.6 1.9 %shard_map.75 = bf16[1024,128]{1,0:T(8,128)(2,1)S(1)} custom-call(s32[4]{0:T(128)S(1)} %pad_add_fusion.i_ref, bf16[256,2048]{1,0:T(8,128)(2,1)S(1)} %get-tuple-element.23.t_ref, bf16[512,512]{1,0:T(8,128)(2,1)S(1)} %get-tuple-element.29.column, bf16[768,512]{1,0:T(8,128)(2,1)S(1)} %constant_dynamic-update-slice_fusion.4.rest, ...), custom_call_target="tpu_custom_call" | custom-call | bytes 4194304 | tf_op jit(solution)/shard_map/pallas_call | solution.py:62
  87.5 0.4 collective-permute-start.13
  87.9 1.3 collective-permute-start.26
  89.2 3.6 %collective-permute-start.27 = (bf16[256,512]{1,0:T(8,128)(2,1)S(1)}, bf16[256,512]{1,0:T(8,128)(2,1)S(1)}, u32[]{:S(2)}, u32[]{:S(2)}) collective-permute-start(bf16[256,512]{1,0:T(8,128)(2,1)S(1)} %get-tuple-element.40), channel_id=1, source_target_pairs={{0,16},{8,24},{16,0},{24,8},{1,17},{9,25},{17,1},{25,9},{2,18},{10... | collective-permute-start | bytes 786440 | tf_op jit(solution)/shard_map/ppermute | solution.py:42
  92.8 2.2 %collective-permute-start.20 = (bf16[1024,256]{1,0:T(8,128)(2,1)S(1)}, bf16[1024,256]{1,0:T(8,128)(2,1)S(1)}, u32[]{:S(2)}, u32[]{:S(2)}) collective-permute-start(bf16[1024,256]{1,0:T(8,128)(2,1)S(1)} %collective-permute-done.19.refs_1_), channel_id=1, source_target_pairs={{0,32},{4,228},{32,64},{36,4},{64,96},{68,36},{96,128},{100,68},{1... | collective-permute-start | bytes 1572872 | tf_op jit(solution)/shard_map/ppermute | solution.py:38
  95.0 1.7 %collective-permute-done.23.refs_2_ = bf16[1024,256]{1,0:T(8,128)(2,1)S(1)} collective-permute-done((bf16[1024,256]{1,0:T(8,128)(2,1)S(1)}, bf16[1024,256]{1,0:T(8,128)(2,1)S(1)}, u32[]{:S(2)}, u32[]{:S(2)}) %collective-permute-start.23) | collective-permute-done | bytes 524320 | tf_op jit(solution)/shard_map/ppermute | solution.py:38
  96.7 0.2 collective-permute-start.24
  96.9 7.5 %attend.5 = (f32[2048,128]{1,0:T(8,128)S(1)}, f32[2048,256]{1,0:T(8,128)S(1)}) custom-call(bf16[2048,128]{1,0:T(8,128)(2,1)S(1)} %pad_maximum_fusion.refs_0_, bf16[1024,256]{1,0:T(8,128)(2,1)S(1)} %constant_dynamic-update-slice_fusion.6.refs_1_, bf16[1024,256]{1,0:T(8,128)(2,1)S(1)} %collective-permute-done.21.refs_2_), custom_call_target="tpu_custom_call" | custom-call | flops 4294967296 | bytes 8388608 | tf_op jit(solution)/shard_map/attend/pallas_call | solution.py:214
  104.4 7.6 %attend.6 = (f32[2048,128]{1,0:T(8,128)S(1)}, f32[2048,256]{1,0:T(8,128)S(1)}) custom-call(bf16[2048,128]{1,0:T(8,128)(2,1)S(1)} %pad_maximum_fusion.refs_0_, bf16[1024,256]{1,0:T(8,128)(2,1)S(1)} %collective-permute-done.18.refs_1_, bf16[1024,256]{1,0:T(8,128)(2,1)S(1)} %collective-permute-done.22.refs_2_, ...), custom_call_target="tpu_custom_call", output_to_operand_aliasing={{0}: (3, {}), {1}: (4, {})} | custom-call | flops 4294967296 | bytes 8388608 | tf_op jit(solution)/shard_map/attend/pallas_call | solution.py:214
  112.0 7.6 %attend.7 = (f32[2048,128]{1,0:T(8,128)S(1)}, f32[2048,256]{1,0:T(8,128)S(1)}) custom-call(bf16[2048,128]{1,0:T(8,128)(2,1)S(1)} %pad_maximum_fusion.refs_0_, bf16[1024,256]{1,0:T(8,128)(2,1)S(1)} %collective-permute-done.19.refs_1_, bf16[1024,256]{1,0:T(8,128)(2,1)S(1)} %collective-permute-done.23.refs_2_, ...), custom_call_target="tpu_custom_call", output_to_operand_aliasing={{0}: (3, {}), {1}: (4, {})} | custom-call | flops 4294967296 | bytes 8388608 | tf_op jit(solution)/shard_map/attend/pallas_call | solution.py:214
  119.7 3.8 %attend.9 = f32[1024,256]{1,0:T(8,128)S(1)} custom-call(bf16[2048,128]{1,0:T(8,128)(2,1)S(1)} %pad_maximum_fusion.refs_0_, bf16[1024,256]{1,0:T(8,128)(2,1)S(1)} %collective-permute-done.20.refs_1_, bf16[1024,256]{1,0:T(8,128)(2,1)S(1)} %collective-permute-done.24.refs_2_, f32[2048,128]{1,0:T(8,128)S(1)} %get-tuple-element.35.refs_3_, ...), custom_call_target="tpu_custom_call" | custom-call | flops 2147483648 | bytes 8388608 | tf_op jit(solution)/shard_map/attend/pallas_call | solution.py:214
  123.5 0.5 collective-permute-start.25
  124.1 0.4 collective-permute-start.28
  124.6 3.8 %attend.8.own_ref = f32[1024,256]{1,0:T(8,128)S(1)} custom-call(bf16[2048,128]{1,0:T(8,128)(2,1)S(1)} %pad_maximum_fusion.refs_0_, bf16[1024,256]{1,0:T(8,128)(2,1)S(1)} %collective-permute-done.20.refs_1_, bf16[1024,256]{1,0:T(8,128)(2,1)S(1)} %collective-permute-done.24.refs_2_, f32[2048,128]{1,0:T(8,128)S(1)} %get-tuple-element.35.refs_3_, ...), custom_call_target="tpu_custom_call" | custom-call | flops 2147483648 | bytes 8388608 | tf_op jit(solution)/shard_map/attend/pallas_call | solution.py:214
  128.4 2.0 %shard_map.76 = bf16[256,2048]{1,0:T(8,128)(2,1)S(1)} custom-call(s32[4]{0:T(128)S(1)} %pad_add_fusion.i_ref, f32[1024,256]{1,0:T(8,128)S(1)} %attend.8.own_ref, f32[1024,256]{1,0:T(8,128)S(1)} %collective-permute-done.25.got_ref, bf16[512,512]{1,0:T(8,128)(2,1)S(1)} %get-tuple-element.39.column, ...), custom_call_target="tpu_custom_call" | custom-call | bytes 4194304 | tf_op jit(solution)/shard_map/pallas_call | solution.py:62
  130.5 20.0 %all_to_all.10 = bf16[4,64,2048]{2,1,0:T(8,128)(2,1)S(1)} all-to-all(bf16[4,64,2048]{2,1,0:T(8,128)(2,1)S(1)} %bitcast.8), channel_id=1, replica_groups=mesh['sp_0'=8,'sp_1'=4,'sp_2'=2,'tp'=4] {'tp'}, dimensions={0} | all-to-all | bytes 2097152 | tf_op jit(solution)/shard_map/all_to_all | solution.py:317
  150.7 0.8 multiply_convert_fusion
  (54 shorter events, 1.5 us)
Async XLA Ops:
  0.0 39.1 %copy-start = (bf16[64,2048]{1,0:T(8,128)(2,1)S(1)}, bf16[64,2048]{1,0:T(8,128)(2,1)}, u32[]{:S(2)}) copy-start(bf16[64,2048]{1,0:T(8,128)(2,1)} %t0.1) | copy-start | bytes 786436
  0.0 39.1 %copy-start.2 = (f32[128]{0:T(128)S(1)}, f32[128]{0:T(128)}, u32[]{:S(2)}) copy-start(f32[128]{0:T(128)} %param.13) | copy-start | bytes 1540
  1.6 28.5 %all-to-all-start = ((bf16[32,32,256]{2,1,0:T(8,128)(2,1)}), bf16[32,32,256]{2,1,0:T(8,128)(2,1)S(1)}, u32[]{:S(2)}, u32[]{:S(2)}) async-start(bf16[32,32,256]{2,1,0:T(8,128)(2,1)} %broadcast_in_dim.50), calls=%async_computation | async-start | bytes 1048576 | tf_op jit(solution)/shard_map/all_to_all | solution.py:54
  13.2 18.3 %collective-permute-start = (bf16[64,2048]{1,0:T(8,128)(2,1)}, bf16[64,2048]{1,0:T(8,128)(2,1)S(1)}, u32[]{:S(2)}, u32[]{:S(2)}) collective-permute-start(bf16[64,2048]{1,0:T(8,128)(2,1)} %t0.1), channel_id=1, source_target_pairs={{0,3},{1,0},{2,1},{3,2},{4,7},{5,4},{6,5},{7,6},{8,11},{9,8},{10,9... | collective-permute-start | bytes 786440 | tf_op jit(solution)/shard_map/ppermute | solution.py:42
  16.3 16.6 %collective-permute-start.1 = (bf16[64,2048]{1,0:T(8,128)(2,1)}, bf16[64,2048]{1,0:T(8,128)(2,1)S(1)}, u32[]{:S(2)}, u32[]{:S(2)}) collective-permute-start(bf16[64,2048]{1,0:T(8,128)(2,1)} %t0.1), channel_id=1, source_target_pairs={{0,2},{1,3},{2,0},{3,1},{4,6},{5,7},{6,4},{7,5},{8,10},{9,11},{10,... | collective-permute-start | bytes 786440 | tf_op jit(solution)/shard_map/ppermute | solution.py:42
  17.0 18.3 %collective-permute-start.2 = (bf16[64,2048]{1,0:T(8,128)(2,1)}, bf16[64,2048]{1,0:T(8,128)(2,1)S(1)}, u32[]{:S(2)}, u32[]{:S(2)}) collective-permute-start(bf16[64,2048]{1,0:T(8,128)(2,1)} %t0.1), channel_id=1, source_target_pairs={{0,1},{1,2},{2,3},{3,0},{4,5},{5,6},{6,7},{7,4},{8,9},{9,10},{10,1... | collective-permute-start | bytes 786440 | tf_op jit(solution)/shard_map/ppermute | solution.py:42
  18.7 11.4 %collective-permute-start.4 = (bf16[32,1024]{1,0:T(8,128)(2,1)S(1)}, bf16[32,1024]{1,0:T(8,128)(2,1)S(1)}, u32[]{:S(2)}, u32[]{:S(2)}) collective-permute-start(bf16[32,1024]{1,0:T(8,128)(2,1)S(1)} %pad_maximum_fusion.3.own_ref), channel_id=1, source_target_pairs={{0,4},{4,0},{1,5},{5,1},{2,6},{6,2},{3,7},{7,3},{8,12},{12,8},{9,1... | collective-permute-start | bytes 196616 | tf_op jit(solution)/shard_map/ppermute | solution.py:31
  30.1 9.0 %collective-permute-start.3 = (bf16[32,32,256]{2,1,0:T(8,128)(2,1)S(1)}, bf16[32,32,256]{2,1,0:T(8,128)(2,1)S(1)}, u32[]{:S(2)}, u32[]{:S(2)}) collective-permute-start(bf16[32,32,256]{2,1,0:T(8,128)(2,1)S(1)} %all-to-all-done.own), channel_id=1, source_target_pairs={{0,4},{4,0},{1,5},{5,1},{2,6},{6,2},{3,7},{7,3},{8,12},{12,8},{9,1... | collective-permute-start | bytes 1572872 | tf_op jit(solution)/shard_map/ppermute | solution.py:31
  30.9 13.8 %collective-permute-start.5 = (bf16[64,1024]{1,0:T(8,128)(2,1)S(1)}, bf16[64,1024]{1,0:T(8,128)(2,1)S(1)}, u32[]{:S(2)}, u32[]{:S(2)}) collective-permute-start(bf16[64,1024]{1,0:T(8,128)(2,1)S(1)} %pad_maximum_fusion.2), channel_id=1, source_target_pairs={{0,32},{4,228},{32,64},{36,4},{64,96},{68,36},{96,128},{100,68},{1... | collective-permute-start | bytes 393224 | tf_op jit(solution)/shard_map/ppermute | solution.py:49
  31.5 13.2 %collective-permute-start.6 = (bf16[64,1024]{1,0:T(8,128)(2,1)S(1)}, bf16[64,1024]{1,0:T(8,128)(2,1)S(1)}, u32[]{:S(2)}, u32[]{:S(2)}) collective-permute-start(bf16[64,1024]{1,0:T(8,128)(2,1)S(1)} %pad_maximum_fusion.2), channel_id=1, source_target_pairs={{0,64},{4,196},{32,96},{36,228},{64,128},{68,4},{96,160},{100,36},... | collective-permute-start | bytes 393224 | tf_op jit(solution)/shard_map/ppermute | solution.py:49
  32.9 12.4 %collective-permute-start.7 = (bf16[64,1024]{1,0:T(8,128)(2,1)S(1)}, bf16[64,1024]{1,0:T(8,128)(2,1)S(1)}, u32[]{:S(2)}, u32[]{:S(2)}) collective-permute-start(bf16[64,1024]{1,0:T(8,128)(2,1)S(1)} %pad_maximum_fusion.2), channel_id=1, source_target_pairs={{0,96},{4,164},{32,128},{36,196},{64,160},{68,228},{96,192},{100,4... | collective-permute-start | bytes 393224 | tf_op jit(solution)/shard_map/ppermute | solution.py:49
  35.3 9.4 %collective-permute-start.8 = (bf16[32,1024]{1,0:T(8,128)(2,1)S(1)}, bf16[32,1024]{1,0:T(8,128)(2,1)S(1)}, u32[]{:S(2)}, u32[]{:S(2)}) collective-permute-start(bf16[32,1024]{1,0:T(8,128)(2,1)S(1)} %pad_maximum_fusion.3.own_ref), channel_id=1, source_target_pairs={{0,128},{4,132},{32,160},{36,164},{64,192},{68,196},{96,224},{100,... | collective-permute-start | bytes 196616 | tf_op jit(solution)/shard_map/ppermute | solution.py:49
  45.3 40.3 %copy-start.1 = (f32[128]{0:T(128)S(1)}, f32[128]{0:T(128)}, u32[]{:S(2)}) copy-start(f32[128]{0:T(128)} %param.12) | copy-start | bytes 1540
  45.4 6.0 %collective-permute-start.9 = (bf16[224,1024]{1,0:T(8,128)(2,1)S(1)}, bf16[224,1024]{1,0:T(8,128)(2,1)S(1)}, u32[]{:S(2)}, u32[]{:S(2)}) collective-permute-start(bf16[224,1024]{1,0:T(8,128)(2,1)S(1)} %constant_dynamic-update-slice_fusion.mine_ref), channel_id=1, source_target_pairs={{0,4},{4,0},{1,5},{5,1},{2,6},{6,2},{3,7},{7,3},{8,12},{12,8},{9,1... | collective-permute-start | bytes 1376264 | tf_op jit(solution)/shard_map/ppermute | solution.py:31
  45.5 2.0 %collective-permute-start.14 = (bf16[256,256]{1,0:T(8,128)(2,1)S(1)}, bf16[256,256]{1,0:T(8,128)(2,1)S(1)}, u32[]{:S(2)}, u32[]{:S(2)}) collective-permute-start(bf16[256,256]{1,0:T(8,128)(2,1)S(1)} %get-tuple-element.24), channel_id=1, source_target_pairs={{0,4},{4,0},{1,5},{5,1},{2,6},{6,2},{3,7},{7,3},{8,12},{12,8},{9,1... | collective-permute-start | bytes 393224 | tf_op jit(solution)/shard_map/ppermute | solution.py:31
  47.5 7.9 %collective-permute-start.15 = (bf16[512,256]{1,0:T(8,128)(2,1)S(1)}, bf16[512,256]{1,0:T(8,128)(2,1)S(1)}, u32[]{:S(2)}, u32[]{:S(2)}) collective-permute-start(bf16[512,256]{1,0:T(8,128)(2,1)S(1)} %pad_maximum_fusion.1), channel_id=1, source_target_pairs={{0,8},{4,28},{8,16},{12,4},{16,24},{20,12},{24,0},{28,20},{1,9},{5... | collective-permute-start | bytes 786440 | tf_op jit(solution)/shard_map/ppermute | solution.py:38
  48.9 7.9 %collective-permute-start.16 = (bf16[256,256]{1,0:T(8,128)(2,1)S(1)}, bf16[256,256]{1,0:T(8,128)(2,1)S(1)}, u32[]{:S(2)}, u32[]{:S(2)}) collective-permute-start(bf16[256,256]{1,0:T(8,128)(2,1)S(1)} %get-tuple-element.24), channel_id=1, source_target_pairs={{0,16},{8,24},{16,0},{24,8},{1,17},{9,25},{17,1},{25,9},{2,18},{10... | collective-permute-start | bytes 393224 | tf_op jit(solution)/shard_map/ppermute | solution.py:42
  52.0 10.4 %collective-permute-start.10 = (bf16[512,512]{1,0:T(8,128)(2,1)S(1)}, bf16[512,512]{1,0:T(8,128)(2,1)S(1)}, u32[]{:S(2)}, u32[]{:S(2)}) collective-permute-start(bf16[512,512]{1,0:T(8,128)(2,1)S(1)} %get-tuple-element.29.column), channel_id=1, source_target_pairs={{0,8},{4,28},{8,16},{12,4},{16,24},{20,12},{24,0},{28,20},{1,9},{5... | collective-permute-start | bytes 1572872 | tf_op jit(solution)/shard_map/ppermute | solution.py:38
  56.9 12.5 %collective-permute-start.17 = (bf16[1024,256]{1,0:T(8,128)(2,1)S(1)}, bf16[1024,256]{1,0:T(8,128)(2,1)S(1)}, u32[]{:S(2)}, u32[]{:S(2)}) collective-permute-start(bf16[1024,256]{1,0:T(8,128)(2,1)S(1)} %constant_dynamic-update-slice_fusion.6.refs_1_), channel_id=1, source_target_pairs={{0,4},{4,0},{1,5},{5,1},{2,6},{6,2},{3,7},{7,3},{8,12},{12,8},{9,1... | collective-permute-start | bytes 1572872 | tf_op jit(solution)/shard_map/ppermute | solution.py:31
  57.0 13.9 %collective-permute-start.21 = (bf16[1024,256]{1,0:T(8,128)(2,1)S(1)}, bf16[1024,256]{1,0:T(8,128)(2,1)S(1)}, u32[]{:S(2)}, u32[]{:S(2)}) collective-permute-start(bf16[1024,256]{1,0:T(8,128)(2,1)S(1)} %constant_dynamic-update-slice_fusion.6.refs_1_), channel_id=1, source_target_pairs={{0,32},{4,228},{32,64},{36,4},{64,96},{68,36},{96,128},{100,68},{1... | collective-permute-start | bytes 1572872 | tf_op jit(solution)/shard_map/ppermute | solution.py:38
  59.8 9.4 %collective-permute-start.11 = (bf16[256,512]{1,0:T(8,128)(2,1)S(1)}, bf16[256,512]{1,0:T(8,128)(2,1)S(1)}, u32[]{:S(2)}, u32[]{:S(2)}) collective-permute-start(bf16[256,512]{1,0:T(8,128)(2,1)S(1)} %get-tuple-element.30), channel_id=1, source_target_pairs={{0,16},{8,24},{16,0},{24,8},{1,17},{9,25},{17,1},{25,9},{2,18},{10... | collective-permute-start | bytes 786440 | tf_op jit(solution)/shard_map/ppermute | solution.py:42
  69.2 16.4 %collective-permute-start.12 = (bf16[768,512]{1,0:T(8,128)(2,1)S(1)}, bf16[768,512]{1,0:T(8,128)(2,1)S(1)}, u32[]{:S(2)}, u32[]{:S(2)}) collective-permute-start(bf16[768,512]{1,0:T(8,128)(2,1)S(1)} %constant_dynamic-update-slice_fusion.4.rest), channel_id=1, source_target_pairs={{0,4},{4,0},{1,5},{5,1},{2,6},{6,2},{3,7},{7,3},{8,12},{12,8},{9,1... | collective-permute-start | bytes 2359304 | tf_op jit(solution)/shard_map/ppermute | solution.py:31
  69.4 10.5 %collective-permute-start.18 = (bf16[1024,256]{1,0:T(8,128)(2,1)S(1)}, bf16[1024,256]{1,0:T(8,128)(2,1)S(1)}, u32[]{:S(2)}, u32[]{:S(2)}) collective-permute-start(bf16[1024,256]{1,0:T(8,128)(2,1)S(1)} %collective-permute-done.17), channel_id=1, source_target_pairs={{0,32},{4,228},{32,64},{36,4},{64,96},{68,36},{96,128},{100,68},{1... | collective-permute-start | bytes 1572872 | tf_op jit(solution)/shard_map/ppermute | solution.py:38
  70.8 14.6 %collective-permute-start.22 = (bf16[1024,256]{1,0:T(8,128)(2,1)S(1)}, bf16[1024,256]{1,0:T(8,128)(2,1)S(1)}, u32[]{:S(2)}, u32[]{:S(2)}) collective-permute-start(bf16[1024,256]{1,0:T(8,128)(2,1)S(1)} %collective-permute-done.21.refs_2_), channel_id=1, source_target_pairs={{0,32},{4,228},{32,64},{36,4},{64,96},{68,36},{96,128},{100,68},{1... | collective-permute-start | bytes 1572872 | tf_op jit(solution)/shard_map/ppermute | solution.py:38
  79.8 13.0 %collective-permute-start.19 = (bf16[1024,256]{1,0:T(8,128)(2,1)S(1)}, bf16[1024,256]{1,0:T(8,128)(2,1)S(1)}, u32[]{:S(2)}, u32[]{:S(2)}) collective-permute-start(bf16[1024,256]{1,0:T(8,128)(2,1)S(1)} %collective-permute-done.18.refs_1_), channel_id=1, source_target_pairs={{0,32},{4,228},{32,64},{36,4},{64,96},{68,36},{96,128},{100,68},{1... | collective-permute-start | bytes 1572872 | tf_op jit(solution)/shard_map/ppermute | solution.py:38
  85.4 11.2 %collective-permute-start.23 = (bf16[1024,256]{1,0:T(8,128)(2,1)S(1)}, bf16[1024,256]{1,0:T(8,128)(2,1)S(1)}, u32[]{:S(2)}, u32[]{:S(2)}) collective-permute-start(bf16[1024,256]{1,0:T(8,128)(2,1)S(1)} %collective-permute-done.22.refs_2_), channel_id=1, source_target_pairs={{0,32},{4,228},{32,64},{36,4},{64,96},{68,36},{96,128},{100,68},{1... | collective-permute-start | bytes 1572872 | tf_op jit(solution)/shard_map/ppermute | solution.py:38
  87.5 9.3 %collective-permute-start.13 = (bf16[1024,128]{1,0:T(8,128)(2,1)S(1)}, bf16[1024,128]{1,0:T(8,128)(2,1)S(1)}, u32[]{:S(2)}, u32[]{:S(2)}) collective-permute-start(bf16[1024,128]{1,0:T(8,128)(2,1)S(1)} %shard_map.75), channel_id=1, source_target_pairs={{0,4},{4,0},{1,5},{5,1},{2,6},{6,2},{3,7},{7,3},{8,12},{12,8},{9,1... | collective-permute-start | bytes 786440 | tf_op jit(solution)/shard_map/ppermute | solution.py:31
  87.9 36.1 %collective-permute-start.26 = (bf16[512,512]{1,0:T(8,128)(2,1)S(1)}, bf16[512,512]{1,0:T(8,128)(2,1)S(1)}, u32[]{:S(2)}, u32[]{:S(2)}) collective-permute-start(bf16[512,512]{1,0:T(8,128)(2,1)S(1)} %get-tuple-element.39.column), channel_id=1, source_target_pairs={{0,8},{4,28},{8,16},{12,4},{16,24},{20,12},{24,0},{28,20},{1,9},{5... | collective-permute-start | bytes 1572872 | tf_op jit(solution)/shard_map/ppermute | solution.py:38
  89.2 34.9 %collective-permute-start.27 = (bf16[256,512]{1,0:T(8,128)(2,1)S(1)}, bf16[256,512]{1,0:T(8,128)(2,1)S(1)}, u32[]{:S(2)}, u32[]{:S(2)}) collective-permute-start(bf16[256,512]{1,0:T(8,128)(2,1)S(1)} %get-tuple-element.40), channel_id=1, source_target_pairs={{0,16},{8,24},{16,0},{24,8},{1,17},{9,25},{17,1},{25,9},{2,18},{10... | collective-permute-start | bytes 786440 | tf_op jit(solution)/shard_map/ppermute | solution.py:42
  92.8 26.9 %collective-permute-start.20 = (bf16[1024,256]{1,0:T(8,128)(2,1)S(1)}, bf16[1024,256]{1,0:T(8,128)(2,1)S(1)}, u32[]{:S(2)}, u32[]{:S(2)}) collective-permute-start(bf16[1024,256]{1,0:T(8,128)(2,1)S(1)} %collective-permute-done.19.refs_1_), channel_id=1, source_target_pairs={{0,32},{4,228},{32,64},{36,4},{64,96},{68,36},{96,128},{100,68},{1... | collective-permute-start | bytes 1572872 | tf_op jit(solution)/shard_map/ppermute | solution.py:38
  96.7 23.0 %collective-permute-start.24 = (bf16[1024,256]{1,0:T(8,128)(2,1)S(1)}, bf16[1024,256]{1,0:T(8,128)(2,1)S(1)}, u32[]{:S(2)}, u32[]{:S(2)}) collective-permute-start(bf16[1024,256]{1,0:T(8,128)(2,1)S(1)} %collective-permute-done.23.refs_2_), channel_id=1, source_target_pairs={{0,32},{4,228},{32,64},{36,4},{64,96},{68,36},{96,128},{100,68},{1... | collective-permute-start | bytes 1572872 | tf_op jit(solution)/shard_map/ppermute | solution.py:38
  123.5 4.9 %collective-permute-start.25 = (f32[1024,256]{1,0:T(8,128)S(1)}, f32[1024,256]{1,0:T(8,128)S(1)}, u32[]{:S(2)}, u32[]{:S(2)}) collective-permute-start(f32[1024,256]{1,0:T(8,128)S(1)} %attend.9), channel_id=1, source_target_pairs={{0,4},{4,0},{1,5},{5,1},{2,6},{6,2},{3,7},{7,3},{8,12},{12,8},{9,1... | collective-permute-start | bytes 3145736 | tf_op jit(solution)/shard_map/ppermute | solution.py:31
  124.1 4.3 %collective-permute-start.28 = (bf16[768,512]{1,0:T(8,128)(2,1)S(1)}, bf16[768,512]{1,0:T(8,128)(2,1)S(1)}, u32[]{:S(2)}, u32[]{:S(2)}) collective-permute-start(bf16[768,512]{1,0:T(8,128)(2,1)S(1)} %constant_dynamic-update-slice_fusion.9.rest), channel_id=1, source_target_pairs={{0,4},{4,0},{1,5},{5,1},{2,6},{6,2},{3,7},{7,3},{8,12},{12,8},{9,1... | collective-permute-start | bytes 2359304 | tf_op jit(solution)/shard_map/ppermute | solution.py:31
where the time goes:
time: 154 us; the launch traced here: 152 us
  starting transfers between devices  46.5 us (30%)
  waiting for transfers between devices  43.2 us (28%)
  Pallas kernels  36.4 us (24%)
  blocking collectives  20 us (13%)
  other arithmetic  4.14 us (3%)
    pallas_call x5, Pallas kernels, attend(): pl.pallas_call(functools.partial(attend_kernel, pieces=pieces, first=firs...  30.4 us
    all_to_all x1, blocking collectives, local(): summed = jnp.sum(lax.all_to_all(pieces, Y, 0, 0).astype(F32), axis=0)  20 us
    ppermute x10, waiting for transfers between devices, turn(): return lax.ppermute(piece, (axis, C), pairs)  17.2 us
    ppermute x6, starting transfers between devices, shift(): lax.ppermute(piece, axis, [(i, (i + by) % count) for i in range(count)])  13.2 us
    ppermute x10, starting transfers between devices, turn(): return lax.ppermute(piece, (axis, C), pairs)  12 us
    all_to_all x1, starting transfers between devices, everyone(): lax.all_to_all(jnp.broadcast_to(piece[None], (n,) + piece.shape), axes, 0...  11.6 us
    all_to_all x1, waiting for transfers between devices, everyone(): lax.all_to_all(jnp.broadcast_to(piece[None], (n,) + piece.shape), axes, 0...  11.3 us
    ppermute x6, waiting for transfers between devices, shift(): lax.ppermute(piece, axis, [(i, (i + by) % count) for i in range(count)])  8.3 us
  transfers between devices with their start and end apart: 30, of which 10 were waited for; matrix products, arithmetic and copies ran while one was open for 2% of the time, Pallas kernels for 23%

commit v1 on v0

--- a/solution.py
+++ b/solution.py
@@ -96,6 +96,11 @@
     put(got_ref, 192, z + 4, 1 - c)
     q_half_ref[...] = q_ref[at(c, 256), :]
     o_half_ref[...] = o_ref[at(c, 256), :]
+
+
+def join_kernel(i_ref, near_ref, far_ref, out_ref):
+    out_ref[:512, :] = near_ref[...]
+    out_ref[512:, :] = far_ref[...]
 
 
 def fill_rows(i_ref, w_ref, column, rest, got):
@@ -256,8 +261,12 @@
     return jnp.cos(angle), jnp.sin(angle) * jnp.where((lane // 32) % 2 == 0, -1.0, 1.0)
 
 
-def from_x(column, half):
-    rest = jnp.concatenate([turn(column, X, NX), shift(half, X, NX, 2)], axis=0)
+def start_x(column, half):
+    return column, turn(column, X, NX), shift(half, X, NX, 2)
+
+
+def finish_x(where, column, near, far):
+    (rest,) = call(join_kernel, [((768, near.shape[1]), BF16)], where, near, far)
     return column, rest, other_core(rest)
 
 
@@ -272,7 +281,8 @@
     w_own = jnp.concatenate([query_weight, out_weight.T], axis=1)
     w_other = other_core(w_own)
     slab = jnp.concatenate([w_own, w_other], axis=0)
-    leaps = leap(slab, 1), leap(slab, 2), leap(slab, 3), leap(w_own, 4)
+    leaps = leap(slab, 1), leap(slab, 2), leap(slab, 3)
+    leaps += (leap(w_own, 4),)
     toks = [tokens] + [shift(tokens, Y, NY, -by) for by in (1, 2, 3)]
     kv_got = other_core(kv_weight)
 
@@ -286,17 +296,16 @@
     q_column, q_half, wo_column, wo_half = call(
         column_kernel, [((512, 512), BF16), ((256, 512), BF16)] * 2, where, w_own, w_other, mine, got,
     )
-    kv_slab = jnp.concatenate([kv_own, other_core(kv_own)], axis=0)
-    kv_near, kv_far = turn(kv_slab, X, NX), shift(kv_own, X, NX, 2)
-    plane = jnp.concatenate([kv_own, kv_near, kv_far], axis=0)
+    parts = [shift(kv_own, X, NX, by) for by in (2, 1, 3)]
+    plane = jnp.concatenate([kv_own, *parts], axis=0)
 
     (q_own,) = call(
         q_kernel, [((GROUP * rows, HEAD_DIM), BF16)],
-        where, rows_in, *from_x(q_column, q_half), gain_q, cosine, sine,
+        where, rows_in, *finish_x(where, *start_x(q_column, q_half)), gain_q, cosine, sine,
         scratch=[pltpu.VMEM((tokens.shape[1], 512), BF16)],
     )
     q_all = jnp.concatenate([q_own, other_core(q_own)], axis=0)
-    wo_all = from_x(*after((wo_column, wo_half), q_own))
+    wo_column, *wo_parts = start_x(wo_column, wo_half)
 
     chain = {"a": plane, "b": other_core(plane)}
     carry, todo = None, [plane]
@@ -304,8 +313,10 @@
         for name in "ab" if step < 4 else "a":
             chain[name] = turn(chain[name], Z, NZ)
             todo.append(chain[name])
-    for at_once in (todo[0:2], todo[2:4], todo[4:6]):
+    for i, at_once in enumerate((todo[0:2], todo[2:4], todo[4:6])):
         carry = attend(q_all, at_once, carry)
+        if i == 1:
+            wo_all = finish_x(where, wo_column, *wo_parts)
     theirs = attend(q_all, todo[6:], carry, last=1)
     got = other_core(theirs)
     own = attend(q_all, todo[6:], carry, last=0)

time: 154 us -> 159 us (1.032)
  the two profiles are of different devices: /device:TPU:2 before, /device:TPU:32 now
where the time goes in v1:
time: 159 us
  waiting for transfers between devices  48.4 us (30%)
  starting transfers between devices  47.2 us (30%)
  Pallas kernels  37.9 us (24%)
  blocking collectives  19.6 us (12%)
  other arithmetic  4.12 us (3%)
    pallas_call x5, Pallas kernels, attend(): pl.pallas_call(functools.partial(attend_kernel, pieces=pieces, first=firs...  30.8 us
    all_to_all x1, blocking collectives, local(): summed = jnp.sum(lax.all_to_all(pieces, Y, 0, 0).astype(F32), axis=0)  19.6 us
    ppermute x8, waiting for transfers between devices, shift(): lax.ppermute(piece, axis, [(i, (i + by) % count) for i in range(count)])  15.4 us
    ppermute x9, waiting for transfers between devices, turn(): return lax.ppermute(piece, (axis, C), pairs)  14.9 us
    ppermute x9, starting transfers between devices, turn(): return lax.ppermute(piece, (axis, C), pairs)  13.5 us
    ppermute x8, starting transfers between devices, shift(): lax.ppermute(piece, axis, [(i, (i + by) % count) for i in range(count)])  13 us
    all_to_all x1, waiting for transfers between devices, everyone(): lax.all_to_all(jnp.broadcast_to(piece[None], (n,) + piece.shape), axes, 0...  11.7 us
    all_to_all x1, starting transfers between devices, everyone(): lax.all_to_all(jnp.broadcast_to(piece[None], (n,) + piece.shape), axes, 0...  11.2 us
  transfers between devices with their start and end apart: 30, of which 10 were waited for; matrix products, arithmetic and copies ran while one was open for 1% of the time, Pallas kernels for 23%

profile of v1, /device:TPU:32, one launch (start us, length us, event | category | flops | bytes accessed | tf_op | source)
XLA Modules:
  0.0 158.5 jit_solution(1079050799238258578)
XLA Ops:
  0.0 0.8 pad_maximum_fusion.3
  0.8 0.9 broadcast_in_dim.50
  1.6 11.2 %all-to-all-start = ((bf16[32,32,256]{2,1,0:T(8,128)(2,1)}), bf16[32,32,256]{2,1,0:T(8,128)(2,1)S(1)}, u32[]{:S(2)}, u32[]{:S(2)}) async-start(bf16[32,32,256]{2,1,0:T(8,128)(2,1)} %broadcast_in_dim.50), calls=%async_computation | async-start | bytes 1048576 | tf_op jit(solution)/shard_map/all_to_all | solution.py:54
  12.8 3.1 %collective-permute-start = (bf16[64,2048]{1,0:T(8,128)(2,1)}, bf16[64,2048]{1,0:T(8,128)(2,1)S(1)}, u32[]{:S(2)}, u32[]{:S(2)}) collective-permute-start(bf16[64,2048]{1,0:T(8,128)(2,1)} %t0.1), channel_id=1, source_target_pairs={{0,3},{1,0},{2,1},{3,2},{4,7},{5,4},{6,5},{7,6},{8,11},{9,8},{10,9... | collective-permute-start | bytes 786440 | tf_op jit(solution)/shard_map/ppermute | solution.py:42
  15.9 0.6 collective-permute-start.1
  16.5 1.0 collective-permute-start.2
  17.5 0.8 pad_maximum_fusion.2.own_ref
  18.3 11.7 %all-to-all-done.own = bf16[32,32,256]{2,1,0:T(8,128)(2,1)S(1)} async-done(((bf16[32,32,256]{2,1,0:T(8,128)(2,1)}), bf16[32,32,256]{2,1,0:T(8,128)(2,1)S(1)}, u32[]{:S(2)}, u32[]{:S(2)}) %all-to-all-start) | async-done | bytes 524320 | tf_op jit(solution)/shard_map/all_to_all | solution.py:54
  30.0 0.8 pad_maximum_fusion.1
  30.8 1.2 collective-permute-start.5
  32.0 0.6 collective-permute-start.6
  32.6 1.9 %collective-permute-start.7 = (bf16[64,1024]{1,0:T(8,128)(2,1)S(1)}, bf16[64,1024]{1,0:T(8,128)(2,1)S(1)}, u32[]{:S(2)}, u32[]{:S(2)}) collective-permute-start(bf16[64,1024]{1,0:T(8,128)(2,1)S(1)} %pad_maximum_fusion.1), channel_id=1, source_target_pairs={{0,96},{4,164},{32,128},{36,196},{64,160},{68,228},{96,192},{100,4... | collective-permute-start | bytes 393224 | tf_op jit(solution)/shard_map/ppermute | solution.py:49
  34.5 0.5 sine_multiply_fusion
  35.1 4.3 %collective-permute-start.8 = (bf16[32,1024]{1,0:T(8,128)(2,1)S(1)}, bf16[32,1024]{1,0:T(8,128)(2,1)S(1)}, u32[]{:S(2)}, u32[]{:S(2)}) collective-permute-start(bf16[32,1024]{1,0:T(8,128)(2,1)S(1)} %pad_maximum_fusion.2.own_ref), channel_id=1, source_target_pairs={{0,128},{4,132},{32,160},{36,164},{64,192},{68,196},{96,224},{100,... | collective-permute-start | bytes 196616 | tf_op jit(solution)/shard_map/ppermute | solution.py:49
  39.4 1.4 shard_map.73
  40.8 4.9 %collective-permute-done.8 = bf16[32,1024]{1,0:T(8,128)(2,1)S(1)} collective-permute-done((bf16[32,1024]{1,0:T(8,128)(2,1)S(1)}, bf16[32,1024]{1,0:T(8,128)(2,1)S(1)}, u32[]{:S(2)}, u32[]{:S(2)}) %collective-permute-start.8) | collective-permute-done | bytes 65568 | tf_op jit(solution)/shard_map/ppermute | solution.py:49
  45.7 1.5 collective-permute-done.7
  47.7 1.5 collective-permute-start.14
  49.2 0.6 collective-permute-start.15
  49.7 2.7 %collective-permute-start.16 = (bf16[256,256]{1,0:T(8,128)(2,1)S(1)}, bf16[256,256]{1,0:T(8,128)(2,1)S(1)}, u32[]{:S(2)}, u32[]{:S(2)}) collective-permute-start(bf16[256,256]{1,0:T(8,128)(2,1)S(1)} %get-tuple-element.22), channel_id=1, source_target_pairs={{0,24},{8,0},{16,8},{24,16},{1,25},{9,1},{17,9},{25,17},{2,26},{10... | collective-permute-start | bytes 393224 | tf_op jit(solution)/shard_map/ppermute | solution.py:42
  52.5 3.0 %collective-permute-done.14 = bf16[256,256]{1,0:T(8,128)(2,1)S(1)} collective-permute-done((bf16[256,256]{1,0:T(8,128)(2,1)S(1)}, bf16[256,256]{1,0:T(8,128)(2,1)S(1)}, u32[]{:S(2)}, u32[]{:S(2)}) %collective-permute-start.14) | collective-permute-done | bytes 131104 | tf_op jit(solution)/shard_map/ppermute | solution.py:42
  55.5 2.1 %collective-permute-done.15 = bf16[256,256]{1,0:T(8,128)(2,1)S(1)} collective-permute-done((bf16[256,256]{1,0:T(8,128)(2,1)S(1)}, bf16[256,256]{1,0:T(8,128)(2,1)S(1)}, u32[]{:S(2)}, u32[]{:S(2)}) %collective-permute-start.15) | collective-permute-done | bytes 131104 | tf_op jit(solution)/shard_map/ppermute | solution.py:42
  57.6 0.7 shard_map.74
  58.7 2.4 %collective-permute-start.21 = (bf16[1024,256]{1,0:T(8,128)(2,1)S(1)}, bf16[1024,256]{1,0:T(8,128)(2,1)S(1)}, u32[]{:S(2)}, u32[]{:S(2)}) collective-permute-start(bf16[1024,256]{1,0:T(8,128)(2,1)S(1)} %constant_dynamic-update-slice_fusion.4.refs_1_), channel_id=1, source_target_pairs={{0,32},{4,228},{32,64},{36,4},{64,96},{68,36},{96,128},{100,68},{1... | collective-permute-start | bytes 1572872 | tf_op jit(solution)/shard_map/ppermute | solution.py:38
  61.2 1.8 %collective-permute-start.11 = (bf16[256,512]{1,0:T(8,128)(2,1)S(1)}, bf16[256,512]{1,0:T(8,128)(2,1)S(1)}, u32[]{:S(2)}, u32[]{:S(2)}) collective-permute-start(bf16[256,512]{1,0:T(8,128)(2,1)S(1)} %get-tuple-element.28), channel_id=1, source_target_pairs={{0,16},{8,24},{16,0},{24,8},{1,17},{9,25},{17,1},{25,9},{2,18},{10... | collective-permute-start | bytes 786440 | tf_op jit(solution)/shard_map/ppermute | solution.py:42
  63.0 10.3 %collective-permute-done.11.far_ref = bf16[256,512]{1,0:T(8,128)(2,1)S(1)} collective-permute-done((bf16[256,512]{1,0:T(8,128)(2,1)S(1)}, bf16[256,512]{1,0:T(8,128)(2,1)S(1)}, u32[]{:S(2)}, u32[]{:S(2)}) %collective-permute-start.11) | collective-permute-done | bytes 262176 | tf_op jit(solution)/shard_map/ppermute | solution.py:42
  73.3 1.1 collective-permute-done.10.near_ref
  74.4 0.6 shard_map.75.rest
  75.1 2.3 %collective-permute-start.18 = (bf16[1024,256]{1,0:T(8,128)(2,1)S(1)}, bf16[1024,256]{1,0:T(8,128)(2,1)S(1)}, u32[]{:S(2)}, u32[]{:S(2)}) collective-permute-start(bf16[1024,256]{1,0:T(8,128)(2,1)S(1)} %collective-permute-done.17), channel_id=1, source_target_pairs={{0,32},{4,228},{32,64},{36,4},{64,96},{68,36},{96,128},{100,68},{1... | collective-permute-start | bytes 1572872 | tf_op jit(solution)/shard_map/ppermute | solution.py:38
  77.5 6.9 %collective-permute-done.18.refs_1_ = bf16[1024,256]{1,0:T(8,128)(2,1)S(1)} collective-permute-done((bf16[1024,256]{1,0:T(8,128)(2,1)S(1)}, bf16[1024,256]{1,0:T(8,128)(2,1)S(1)}, u32[]{:S(2)}, u32[]{:S(2)}) %collective-permute-start.18) | collective-permute-done | bytes 524320 | tf_op jit(solution)/shard_map/ppermute | solution.py:38
  84.3 2.2 %collective-permute-start.19 = (bf16[1024,256]{1,0:T(8,128)(2,1)S(1)}, bf16[1024,256]{1,0:T(8,128)(2,1)S(1)}, u32[]{:S(2)}, u32[]{:S(2)}) collective-permute-start(bf16[1024,256]{1,0:T(8,128)(2,1)S(1)} %collective-permute-done.18.refs_1_), channel_id=1, source_target_pairs={{0,32},{4,228},{32,64},{36,4},{64,96},{68,36},{96,128},{100,68},{1... | collective-permute-start | bytes 1572872 | tf_op jit(solution)/shard_map/ppermute | solution.py:38
  86.5 3.4 %collective-permute-done.22.refs_2_ = bf16[1024,256]{1,0:T(8,128)(2,1)S(1)} collective-permute-done((bf16[1024,256]{1,0:T(8,128)(2,1)S(1)}, bf16[1024,256]{1,0:T(8,128)(2,1)S(1)}, u32[]{:S(2)}, u32[]{:S(2)}) %collective-permute-start.22) | collective-permute-done | bytes 524320 | tf_op jit(solution)/shard_map/ppermute | solution.py:38
  90.0 2.2 %collective-permute-start.23 = (bf16[1024,256]{1,0:T(8,128)(2,1)S(1)}, bf16[1024,256]{1,0:T(8,128)(2,1)S(1)}, u32[]{:S(2)}, u32[]{:S(2)}) collective-permute-start(bf16[1024,256]{1,0:T(8,128)(2,1)S(1)} %collective-permute-done.22.refs_2_), channel_id=1, source_target_pairs={{0,32},{4,228},{32,64},{36,4},{64,96},{68,36},{96,128},{100,68},{1... | collective-permute-start | bytes 1572872 | tf_op jit(solution)/shard_map/ppermute | solution.py:38
  92.2 1.9 %shard_map.76 = bf16[1024,128]{1,0:T(8,128)(2,1)S(1)} custom-call(s32[4]{0:T(128)S(1)} %pad_add_fusion.i_ref, bf16[256,2048]{1,0:T(8,128)(2,1)S(1)} %get-tuple-element.21.t_ref, bf16[512,512]{1,0:T(8,128)(2,1)S(1)} %get-tuple-element.27.column, bf16[768,512]{1,0:T(8,128)(2,1)S(1)} %shard_map.75.rest, bf16[768,512]{1,0:T(8,128)(2,1)S(1)} %collective-permute-done.12.got, ...), custom_call_target="tpu_custom_call" | custom-call | bytes 4194304 | tf_op jit(solution)/shard_map/pallas_call | solution.py:62
  94.3 1.7 %collective-permute-start.27 = (bf16[256,512]{1,0:T(8,128)(2,1)S(1)}, bf16[256,512]{1,0:T(8,128)(2,1)S(1)}, u32[]{:S(2)}, u32[]{:S(2)}) collective-permute-start(bf16[256,512]{1,0:T(8,128)(2,1)S(1)} %get-tuple-element.36), channel_id=1, source_target_pairs={{0,16},{8,24},{16,0},{24,8},{1,17},{9,25},{17,1},{25,9},{2,18},{10... | collective-permute-start | bytes 786440 | tf_op jit(solution)/shard_map/ppermute | solution.py:42
  96.0 1.8 %collective-permute-start.20 = (bf16[1024,256]{1,0:T(8,128)(2,1)S(1)}, bf16[1024,256]{1,0:T(8,128)(2,1)S(1)}, u32[]{:S(2)}, u32[]{:S(2)}) collective-permute-start(bf16[1024,256]{1,0:T(8,128)(2,1)S(1)} %collective-permute-done.19.refs_1_), channel_id=1, source_target_pairs={{0,32},{4,228},{32,64},{36,4},{64,96},{68,36},{96,128},{100,68},{1... | collective-permute-start | bytes 1572872 | tf_op jit(solution)/shard_map/ppermute | solution.py:38
  97.8 3.4 %collective-permute-done.23.refs_2_ = bf16[1024,256]{1,0:T(8,128)(2,1)S(1)} collective-permute-done((bf16[1024,256]{1,0:T(8,128)(2,1)S(1)}, bf16[1024,256]{1,0:T(8,128)(2,1)S(1)}, u32[]{:S(2)}, u32[]{:S(2)}) %collective-permute-start.23) | collective-permute-done | bytes 524320 | tf_op jit(solution)/shard_map/ppermute | solution.py:38
  101.2 2.2 %collective-permute-start.24 = (bf16[1024,256]{1,0:T(8,128)(2,1)S(1)}, bf16[1024,256]{1,0:T(8,128)(2,1)S(1)}, u32[]{:S(2)}, u32[]{:S(2)}) collective-permute-start(bf16[1024,256]{1,0:T(8,128)(2,1)S(1)} %collective-permute-done.23.refs_2_), channel_id=1, source_target_pairs={{0,32},{4,228},{32,64},{36,4},{64,96},{68,36},{96,128},{100,68},{1... | collective-permute-start | bytes 1572872 | tf_op jit(solution)/shard_map/ppermute | solution.py:38
  103.4 7.6 %attend.5 = (f32[2048,128]{1,0:T(8,128)S(1)}, f32[2048,256]{1,0:T(8,128)S(1)}) custom-call(bf16[2048,128]{1,0:T(8,128)(2,1)S(1)} %pad_maximum_fusion.refs_0_, bf16[1024,256]{1,0:T(8,128)(2,1)S(1)} %constant_dynamic-update-slice_fusion.4.refs_1_, bf16[1024,256]{1,0:T(8,128)(2,1)S(1)} %collective-permute-done.21.refs_2_), custom_call_target="tpu_custom_call" | custom-call | flops 4294967296 | bytes 8388608 | tf_op jit(solution)/shard_map/attend/pallas_call | solution.py:219
  111.0 7.8 %attend.6 = (f32[2048,128]{1,0:T(8,128)S(1)}, f32[2048,256]{1,0:T(8,128)S(1)}) custom-call(bf16[2048,128]{1,0:T(8,128)(2,1)S(1)} %pad_maximum_fusion.refs_0_, bf16[1024,256]{1,0:T(8,128)(2,1)S(1)} %collective-permute-done.18.refs_1_, bf16[1024,256]{1,0:T(8,128)(2,1)S(1)} %collective-permute-done.22.refs_2_, ...), custom_call_target="tpu_custom_call", output_to_operand_aliasing={{0}: (3, {}), {1}: (4, {})} | custom-call | flops 4294967296 | bytes 8388608 | tf_op jit(solution)/shard_map/attend/pallas_call | solution.py:219
  118.8 7.8 %attend.7 = (f32[2048,128]{1,0:T(8,128)S(1)}, f32[2048,256]{1,0:T(8,128)S(1)}) custom-call(bf16[2048,128]{1,0:T(8,128)(2,1)S(1)} %pad_maximum_fusion.refs_0_, bf16[1024,256]{1,0:T(8,128)(2,1)S(1)} %collective-permute-done.19.refs_1_, bf16[1024,256]{1,0:T(8,128)(2,1)S(1)} %collective-permute-done.23.refs_2_, ...), custom_call_target="tpu_custom_call", output_to_operand_aliasing={{0}: (3, {}), {1}: (4, {})} | custom-call | flops 4294967296 | bytes 8388608 | tf_op jit(solution)/shard_map/attend/pallas_call | solution.py:219
  126.6 3.8 %attend.9 = f32[1024,256]{1,0:T(8,128)S(1)} custom-call(bf16[2048,128]{1,0:T(8,128)(2,1)S(1)} %pad_maximum_fusion.refs_0_, bf16[1024,256]{1,0:T(8,128)(2,1)S(1)} %collective-permute-done.20.refs_1_, bf16[1024,256]{1,0:T(8,128)(2,1)S(1)} %collective-permute-done.24.refs_2_, f32[2048,128]{1,0:T(8,128)S(1)} %get-tuple-element.33.refs_3_, ...), custom_call_target="tpu_custom_call" | custom-call | flops 2147483648 | bytes 8388608 | tf_op jit(solution)/shard_map/attend/pallas_call | solution.py:219
  130.5 0.6 shard_map.77.rest
  131.1 0.8 collective-permute-start.28
  132.0 3.8 %attend.8.own_ref = f32[1024,256]{1,0:T(8,128)S(1)} custom-call(bf16[2048,128]{1,0:T(8,128)(2,1)S(1)} %pad_maximum_fusion.refs_0_, bf16[1024,256]{1,0:T(8,128)(2,1)S(1)} %collective-permute-done.20.refs_1_, bf16[1024,256]{1,0:T(8,128)(2,1)S(1)} %collective-permute-done.24.refs_2_, f32[2048,128]{1,0:T(8,128)S(1)} %get-tuple-element.33.refs_3_, ...), custom_call_target="tpu_custom_call" | custom-call | flops 2147483648 | bytes 8388608 | tf_op jit(solution)/shard_map/attend/pallas_call | solution.py:219
  135.8 2.0 %shard_map.78 = bf16[256,2048]{1,0:T(8,128)(2,1)S(1)} custom-call(s32[4]{0:T(128)S(1)} %pad_add_fusion.i_ref, f32[1024,256]{1,0:T(8,128)S(1)} %attend.8.own_ref, f32[1024,256]{1,0:T(8,128)S(1)} %collective-permute-done.25.got_ref, bf16[512,512]{1,0:T(8,128)(2,1)S(1)} %get-tuple-element.35.column, bf16[768,512]{1,0:T(8,128)(2,1)S(1)} %shard_map.77.rest, ...), custom_call_target="tpu_custom_call" | custom-call | bytes 4194304 | tf_op jit(solution)/shard_map/pallas_call | solution.py:62
  137.9 19.6 %all_to_all.10 = bf16[4,64,2048]{2,1,0:T(8,128)(2,1)S(1)} all-to-all(bf16[4,64,2048]{2,1,0:T(8,128)(2,1)S(1)} %bitcast.8), channel_id=1, replica_groups=mesh['sp_0'=8,'sp_1'=4,'sp_2'=2,'tp'=4] {'tp'}, dimensions={0} | all-to-all | bytes 2097152 | tf_op jit(solution)/shard_map/all_to_all | solution.py:328
  157.7 0.8 multiply_convert_fusion
  (52 shorter events, 1.8 us)
Async XLA Ops:
  0.0 39.4 %copy-start = (bf16[64,2048]{1,0:T(8,128)(2,1)S(1)}, bf16[64,2048]{1,0:T(8,128)(2,1)}, u32[]{:S(2)}) copy-start(bf16[64,2048]{1,0:T(8,128)(2,1)} %t0.1) | copy-start | bytes 786436
  0.0 39.4 %copy-start.2 = (f32[128]{0:T(128)S(1)}, f32[128]{0:T(128)}, u32[]{:S(2)}) copy-start(f32[128]{0:T(128)} %param.13) | copy-start | bytes 1540
  1.6 28.4 %all-to-all-start = ((bf16[32,32,256]{2,1,0:T(8,128)(2,1)}), bf16[32,32,256]{2,1,0:T(8,128)(2,1)S(1)}, u32[]{:S(2)}, u32[]{:S(2)}) async-start(bf16[32,32,256]{2,1,0:T(8,128)(2,1)} %broadcast_in_dim.50), calls=%async_computation | async-start | bytes 1048576 | tf_op jit(solution)/shard_map/all_to_all | solution.py:54
  12.8 19.2 %collective-permute-start = (bf16[64,2048]{1,0:T(8,128)(2,1)}, bf16[64,2048]{1,0:T(8,128)(2,1)S(1)}, u32[]{:S(2)}, u32[]{:S(2)}) collective-permute-start(bf16[64,2048]{1,0:T(8,128)(2,1)} %t0.1), channel_id=1, source_target_pairs={{0,3},{1,0},{2,1},{3,2},{4,7},{5,4},{6,5},{7,6},{8,11},{9,8},{10,9... | collective-permute-start | bytes 786440 | tf_op jit(solution)/shard_map/ppermute | solution.py:42
  15.9 16.7 %collective-permute-start.1 = (bf16[64,2048]{1,0:T(8,128)(2,1)}, bf16[64,2048]{1,0:T(8,128)(2,1)S(1)}, u32[]{:S(2)}, u32[]{:S(2)}) collective-permute-start(bf16[64,2048]{1,0:T(8,128)(2,1)} %t0.1), channel_id=1, source_target_pairs={{0,2},{1,3},{2,0},{3,1},{4,6},{5,7},{6,4},{7,5},{8,10},{9,11},{10,... | collective-permute-start | bytes 786440 | tf_op jit(solution)/shard_map/ppermute | solution.py:42
  16.5 18.5 %collective-permute-start.2 = (bf16[64,2048]{1,0:T(8,128)(2,1)}, bf16[64,2048]{1,0:T(8,128)(2,1)S(1)}, u32[]{:S(2)}, u32[]{:S(2)}) collective-permute-start(bf16[64,2048]{1,0:T(8,128)(2,1)} %t0.1), channel_id=1, source_target_pairs={{0,1},{1,2},{2,3},{3,0},{4,5},{5,6},{6,7},{7,4},{8,9},{9,10},{10,1... | collective-permute-start | bytes 786440 | tf_op jit(solution)/shard_map/ppermute | solution.py:42
  18.3 11.7 %collective-permute-start.4 = (bf16[32,1024]{1,0:T(8,128)(2,1)S(1)}, bf16[32,1024]{1,0:T(8,128)(2,1)S(1)}, u32[]{:S(2)}, u32[]{:S(2)}) collective-permute-start(bf16[32,1024]{1,0:T(8,128)(2,1)S(1)} %pad_maximum_fusion.2.own_ref), channel_id=1, source_target_pairs={{0,4},{4,0},{1,5},{5,1},{2,6},{6,2},{3,7},{7,3},{8,12},{12,8},{9,1... | collective-permute-start | bytes 196616 | tf_op jit(solution)/shard_map/ppermute | solution.py:31
  30.0 9.4 %collective-permute-start.3 = (bf16[32,32,256]{2,1,0:T(8,128)(2,1)S(1)}, bf16[32,32,256]{2,1,0:T(8,128)(2,1)S(1)}, u32[]{:S(2)}, u32[]{:S(2)}) collective-permute-start(bf16[32,32,256]{2,1,0:T(8,128)(2,1)S(1)} %all-to-all-done.own), channel_id=1, source_target_pairs={{0,4},{4,0},{1,5},{5,1},{2,6},{6,2},{3,7},{7,3},{8,12},{12,8},{9,1... | collective-permute-start | bytes 1572872 | tf_op jit(solution)/shard_map/ppermute | solution.py:31
  30.8 14.9 %collective-permute-start.5 = (bf16[64,1024]{1,0:T(8,128)(2,1)S(1)}, bf16[64,1024]{1,0:T(8,128)(2,1)S(1)}, u32[]{:S(2)}, u32[]{:S(2)}) collective-permute-start(bf16[64,1024]{1,0:T(8,128)(2,1)S(1)} %pad_maximum_fusion.1), channel_id=1, source_target_pairs={{0,32},{4,228},{32,64},{36,4},{64,96},{68,36},{96,128},{100,68},{1... | collective-permute-start | bytes 393224 | tf_op jit(solution)/shard_map/ppermute | solution.py:49
  32.0 13.7 %collective-permute-start.6 = (bf16[64,1024]{1,0:T(8,128)(2,1)S(1)}, bf16[64,1024]{1,0:T(8,128)(2,1)S(1)}, u32[]{:S(2)}, u32[]{:S(2)}) collective-permute-start(bf16[64,1024]{1,0:T(8,128)(2,1)S(1)} %pad_maximum_fusion.1), channel_id=1, source_target_pairs={{0,64},{4,196},{32,96},{36,228},{64,128},{68,4},{96,160},{100,36},... | collective-permute-start | bytes 393224 | tf_op jit(solution)/shard_map/ppermute | solution.py:49
  32.6 14.6 %collective-permute-start.7 = (bf16[64,1024]{1,0:T(8,128)(2,1)S(1)}, bf16[64,1024]{1,0:T(8,128)(2,1)S(1)}, u32[]{:S(2)}, u32[]{:S(2)}) collective-permute-start(bf16[64,1024]{1,0:T(8,128)(2,1)S(1)} %pad_maximum_fusion.1), channel_id=1, source_target_pairs={{0,96},{4,164},{32,128},{36,196},{64,160},{68,228},{96,192},{100,4... | collective-permute-start | bytes 393224 | tf_op jit(solution)/shard_map/ppermute | solution.py:49
  35.1 10.6 %collective-permute-start.8 = (bf16[32,1024]{1,0:T(8,128)(2,1)S(1)}, bf16[32,1024]{1,0:T(8,128)(2,1)S(1)}, u32[]{:S(2)}, u32[]{:S(2)}) collective-permute-start(bf16[32,1024]{1,0:T(8,128)(2,1)S(1)} %pad_maximum_fusion.2.own_ref), channel_id=1, source_target_pairs={{0,128},{4,132},{32,160},{36,164},{64,192},{68,196},{96,224},{100,... | collective-permute-start | bytes 196616 | tf_op jit(solution)/shard_map/ppermute | solution.py:49
  47.2 44.9 %copy-start.1 = (f32[128]{0:T(128)S(1)}, f32[128]{0:T(128)}, u32[]{:S(2)}) copy-start(f32[128]{0:T(128)} %param.12) | copy-start | bytes 1540
  47.3 10.3 %collective-permute-start.9 = (bf16[224,1024]{1,0:T(8,128)(2,1)S(1)}, bf16[224,1024]{1,0:T(8,128)(2,1)S(1)}, u32[]{:S(2)}, u32[]{:S(2)}) collective-permute-start(bf16[224,1024]{1,0:T(8,128)(2,1)S(1)} %constant_dynamic-update-slice_fusion.mine_ref), channel_id=1, source_target_pairs={{0,4},{4,0},{1,5},{5,1},{2,6},{6,2},{3,7},{7,3},{8,12},{12,8},{9,1... | collective-permute-start | bytes 1376264 | tf_op jit(solution)/shard_map/ppermute | solution.py:31
  47.7 7.9 %collective-permute-start.14 = (bf16[256,256]{1,0:T(8,128)(2,1)S(1)}, bf16[256,256]{1,0:T(8,128)(2,1)S(1)}, u32[]{:S(2)}, u32[]{:S(2)}) collective-permute-start(bf16[256,256]{1,0:T(8,128)(2,1)S(1)} %get-tuple-element.22), channel_id=1, source_target_pairs={{0,16},{8,24},{16,0},{24,8},{1,17},{9,25},{17,1},{25,9},{2,18},{10... | collective-permute-start | bytes 393224 | tf_op jit(solution)/shard_map/ppermute | solution.py:42
  49.2 8.4 %collective-permute-start.15 = (bf16[256,256]{1,0:T(8,128)(2,1)S(1)}, bf16[256,256]{1,0:T(8,128)(2,1)S(1)}, u32[]{:S(2)}, u32[]{:S(2)}) collective-permute-start(bf16[256,256]{1,0:T(8,128)(2,1)S(1)} %get-tuple-element.22), channel_id=1, source_target_pairs={{0,8},{8,16},{16,24},{24,0},{1,9},{9,17},{17,25},{25,1},{2,10},{10... | collective-permute-start | bytes 393224 | tf_op jit(solution)/shard_map/ppermute | solution.py:42
  49.7 8.9 %collective-permute-start.16 = (bf16[256,256]{1,0:T(8,128)(2,1)S(1)}, bf16[256,256]{1,0:T(8,128)(2,1)S(1)}, u32[]{:S(2)}, u32[]{:S(2)}) collective-permute-start(bf16[256,256]{1,0:T(8,128)(2,1)S(1)} %get-tuple-element.22), channel_id=1, source_target_pairs={{0,24},{8,0},{16,8},{24,16},{1,25},{9,1},{17,9},{25,17},{2,26},{10... | collective-permute-start | bytes 393224 | tf_op jit(solution)/shard_map/ppermute | solution.py:42
  58.3 16.1 %collective-permute-start.10 = (bf16[512,512]{1,0:T(8,128)(2,1)S(1)}, bf16[512,512]{1,0:T(8,128)(2,1)S(1)}, u32[]{:S(2)}, u32[]{:S(2)}) collective-permute-start(bf16[512,512]{1,0:T(8,128)(2,1)S(1)} %get-tuple-element.27.column), channel_id=1, source_target_pairs={{0,8},{4,28},{8,16},{12,4},{16,24},{20,12},{24,0},{28,20},{1,9},{5... | collective-permute-start | bytes 1572872 | tf_op jit(solution)/shard_map/ppermute | solution.py:38
  58.6 16.5 %collective-permute-start.17 = (bf16[1024,256]{1,0:T(8,128)(2,1)S(1)}, bf16[1024,256]{1,0:T(8,128)(2,1)S(1)}, u32[]{:S(2)}, u32[]{:S(2)}) collective-permute-start(bf16[1024,256]{1,0:T(8,128)(2,1)S(1)} %constant_dynamic-update-slice_fusion.4.refs_1_), channel_id=1, source_target_pairs={{0,4},{4,0},{1,5},{5,1},{2,6},{6,2},{3,7},{7,3},{8,12},{12,8},{9,1... | collective-permute-start | bytes 1572872 | tf_op jit(solution)/shard_map/ppermute | solution.py:31
  58.7 18.6 %collective-permute-start.21 = (bf16[1024,256]{1,0:T(8,128)(2,1)S(1)}, bf16[1024,256]{1,0:T(8,128)(2,1)S(1)}, u32[]{:S(2)}, u32[]{:S(2)}) collective-permute-start(bf16[1024,256]{1,0:T(8,128)(2,1)S(1)} %constant_dynamic-update-slice_fusion.4.refs_1_), channel_id=1, source_target_pairs={{0,32},{4,228},{32,64},{36,4},{64,96},{68,36},{96,128},{100,68},{1... | collective-permute-start | bytes 1572872 | tf_op jit(solution)/shard_map/ppermute | solution.py:38
  61.2 12.1 %collective-permute-start.11 = (bf16[256,512]{1,0:T(8,128)(2,1)S(1)}, bf16[256,512]{1,0:T(8,128)(2,1)S(1)}, u32[]{:S(2)}, u32[]{:S(2)}) collective-permute-start(bf16[256,512]{1,0:T(8,128)(2,1)S(1)} %get-tuple-element.28), channel_id=1, source_target_pairs={{0,16},{8,24},{16,0},{24,8},{1,17},{9,25},{17,1},{25,9},{2,18},{10... | collective-permute-start | bytes 786440 | tf_op jit(solution)/shard_map/ppermute | solution.py:42
  75.0 17.2 %collective-permute-start.12 = (bf16[768,512]{1,0:T(8,128)(2,1)S(1)}, bf16[768,512]{1,0:T(8,128)(2,1)S(1)}, u32[]{:S(2)}, u32[]{:S(2)}) collective-permute-start(bf16[768,512]{1,0:T(8,128)(2,1)S(1)} %shard_map.75.rest), channel_id=1, source_target_pairs={{0,4},{4,0},{1,5},{5,1},{2,6},{6,2},{3,7},{7,3},{8,12},{12,8},{9,1... | collective-permute-start | bytes 2359304 | tf_op jit(solution)/shard_map/ppermute | solution.py:31
  75.1 9.3 %collective-permute-start.18 = (bf16[1024,256]{1,0:T(8,128)(2,1)S(1)}, bf16[1024,256]{1,0:T(8,128)(2,1)S(1)}, u32[]{:S(2)}, u32[]{:S(2)}) collective-permute-start(bf16[1024,256]{1,0:T(8,128)(2,1)S(1)} %collective-permute-done.17), channel_id=1, source_target_pairs={{0,32},{4,228},{32,64},{36,4},{64,96},{68,36},{96,128},{100,68},{1... | collective-permute-start | bytes 1572872 | tf_op jit(solution)/shard_map/ppermute | solution.py:38
  77.4 12.6 %collective-permute-start.22 = (bf16[1024,256]{1,0:T(8,128)(2,1)S(1)}, bf16[1024,256]{1,0:T(8,128)(2,1)S(1)}, u32[]{:S(2)}, u32[]{:S(2)}) collective-permute-start(bf16[1024,256]{1,0:T(8,128)(2,1)S(1)} %collective-permute-done.21.refs_2_), channel_id=1, source_target_pairs={{0,32},{4,228},{32,64},{36,4},{64,96},{68,36},{96,128},{100,68},{1... | collective-permute-start | bytes 1572872 | tf_op jit(solution)/shard_map/ppermute | solution.py:38
  84.3 11.6 %collective-permute-start.19 = (bf16[1024,256]{1,0:T(8,128)(2,1)S(1)}, bf16[1024,256]{1,0:T(8,128)(2,1)S(1)}, u32[]{:S(2)}, u32[]{:S(2)}) collective-permute-start(bf16[1024,256]{1,0:T(8,128)(2,1)S(1)} %collective-permute-done.18.refs_1_), channel_id=1, source_target_pairs={{0,32},{4,228},{32,64},{36,4},{64,96},{68,36},{96,128},{100,68},{1... | collective-permute-start | bytes 1572872 | tf_op jit(solution)/shard_map/ppermute | solution.py:38
  90.0 11.2 %collective-permute-start.23 = (bf16[1024,256]{1,0:T(8,128)(2,1)S(1)}, bf16[1024,256]{1,0:T(8,128)(2,1)S(1)}, u32[]{:S(2)}, u32[]{:S(2)}) collective-permute-start(bf16[1024,256]{1,0:T(8,128)(2,1)S(1)} %collective-permute-done.22.refs_2_), channel_id=1, source_target_pairs={{0,32},{4,228},{32,64},{36,4},{64,96},{68,36},{96,128},{100,68},{1... | collective-permute-start | bytes 1572872 | tf_op jit(solution)/shard_map/ppermute | solution.py:38
  94.1 9.3 %collective-permute-start.13 = (bf16[1024,128]{1,0:T(8,128)(2,1)S(1)}, bf16[1024,128]{1,0:T(8,128)(2,1)S(1)}, u32[]{:S(2)}, u32[]{:S(2)}) collective-permute-start(bf16[1024,128]{1,0:T(8,128)(2,1)S(1)} %shard_map.76), channel_id=1, source_target_pairs={{0,4},{4,0},{1,5},{5,1},{2,6},{6,2},{3,7},{7,3},{8,12},{12,8},{9,1... | collective-permute-start | bytes 786440 | tf_op jit(solution)/shard_map/ppermute | solution.py:31
  94.2 36.3 %collective-permute-start.26 = (bf16[512,512]{1,0:T(8,128)(2,1)S(1)}, bf16[512,512]{1,0:T(8,128)(2,1)S(1)}, u32[]{:S(2)}, u32[]{:S(2)}) collective-permute-start(bf16[512,512]{1,0:T(8,128)(2,1)S(1)} %get-tuple-element.35.column), channel_id=1, source_target_pairs={{0,8},{4,28},{8,16},{12,4},{16,24},{20,12},{24,0},{28,20},{1,9},{5... | collective-permute-start | bytes 1572872 | tf_op jit(solution)/shard_map/ppermute | solution.py:38
  94.3 36.2 %collective-permute-start.27 = (bf16[256,512]{1,0:T(8,128)(2,1)S(1)}, bf16[256,512]{1,0:T(8,128)(2,1)S(1)}, u32[]{:S(2)}, u32[]{:S(2)}) collective-permute-start(bf16[256,512]{1,0:T(8,128)(2,1)S(1)} %get-tuple-element.36), channel_id=1, source_target_pairs={{0,16},{8,24},{16,0},{24,8},{1,17},{9,25},{17,1},{25,9},{2,18},{10... | collective-permute-start | bytes 786440 | tf_op jit(solution)/shard_map/ppermute | solution.py:42
  96.0 30.6 %collective-permute-start.20 = (bf16[1024,256]{1,0:T(8,128)(2,1)S(1)}, bf16[1024,256]{1,0:T(8,128)(2,1)S(1)}, u32[]{:S(2)}, u32[]{:S(2)}) collective-permute-start(bf16[1024,256]{1,0:T(8,128)(2,1)S(1)} %collective-permute-done.19.refs_1_), channel_id=1, source_target_pairs={{0,32},{4,228},{32,64},{36,4},{64,96},{68,36},{96,128},{100,68},{1... | collective-permute-start | bytes 1572872 | tf_op jit(solution)/shard_map/ppermute | solution.py:38
  101.2 25.4 %collective-permute-start.24 = (bf16[1024,256]{1,0:T(8,128)(2,1)S(1)}, bf16[1024,256]{1,0:T(8,128)(2,1)S(1)}, u32[]{:S(2)}, u32[]{:S(2)}) collective-permute-start(bf16[1024,256]{1,0:T(8,128)(2,1)S(1)} %collective-permute-done.23.refs_2_), channel_id=1, source_target_pairs={{0,32},{4,228},{32,64},{36,4},{64,96},{68,36},{96,128},{100,68},{1... | collective-permute-start | bytes 1572872 | tf_op jit(solution)/shard_map/ppermute | solution.py:38
  130.4 5.4 %collective-permute-start.25 = (f32[1024,256]{1,0:T(8,128)S(1)}, f32[1024,256]{1,0:T(8,128)S(1)}, u32[]{:S(2)}, u32[]{:S(2)}) collective-permute-start(f32[1024,256]{1,0:T(8,128)S(1)} %attend.9), channel_id=1, source_target_pairs={{0,4},{4,0},{1,5},{5,1},{2,6},{6,2},{3,7},{7,3},{8,12},{12,8},{9,1... | collective-permute-start | bytes 3145736 | tf_op jit(solution)/shard_map/ppermute | solution.py:31
  131.1 4.7 %collective-permute-start.28 = (bf16[768,512]{1,0:T(8,128)(2,1)S(1)}, bf16[768,512]{1,0:T(8,128)(2,1)S(1)}, u32[]{:S(2)}, u32[]{:S(2)}) collective-permute-start(bf16[768,512]{1,0:T(8,128)(2,1)S(1)} %shard_map.77.rest), channel_id=1, source_target_pairs={{0,4},{4,0},{1,5},{5,1},{2,6},{6,2},{3,7},{7,3},{8,12},{12,8},{9,1... | collective-permute-start | bytes 2359304 | tf_op jit(solution)/shard_map/ppermute | solution.py:31

commit v2 on v1

--- a/solution.py
+++ b/solution.py
@@ -161,54 +161,43 @@
     q_ref, *kv_refs = refs[: 1 + pieces]
     ins = refs[1 + pieces : 1 + pieces + (0 if first else 2)]
     *outs, k_ref, v_ref = refs[1 + pieces + len(ins) :]
-    out_ref, m_ref, a_ref = outs if last else (None, *outs)
-    if first:
-        m_ref[...] = jnp.full(m_ref.shape, -1e30, F32)
-        a_ref[...] = jnp.zeros(a_ref.shape, F32)
-    else:
-        kept = slice(offset, offset + m_ref.shape[0])
-        m_ref[...] = ins[0][kept]
-        a_ref[...] = ins[1][kept]
     for i, ref in enumerate(kv_refs):
-        k_ref[i] = ref[:, :HEAD_DIM]
-        v_ref[i, :, :HEAD_DIM] = ref[:, HEAD_DIM:]
-        v_ref[i, :, HEAD_DIM:] = jnp.ones((ref.shape[0], HEAD_DIM), BF16)
-    sub, chunk = 128, 1024
-    steps = a_ref.shape[0] // chunk
+        keys = slice(i * ref.shape[0], (i + 1) * ref.shape[0])
+        k_ref[:, keys] = ref[:, :HEAD_DIM].T
+        v_ref[keys, :HEAD_DIM] = ref[:, HEAD_DIM:]
+    v_ref[:, HEAD_DIM:] = jnp.ones((v_ref.shape[0], HEAD_DIM), BF16)
+    sub, chunk = 128, 512
+    lane = lax.broadcasted_iota(jnp.int32, (sub, HEAD_DIM), 1)
 
     def part(t, nothing):
-        piece, base = t // steps, t % steps * chunk
-
         def rows(r, start=0):
-            return pl.ds(pl.multiple_of(base + r, sub) + start, sub)
+            return pl.ds(pl.multiple_of(t * chunk + r, sub) + start, sub)
 
         def scores(r):
-            return lax.dot_general(
-                q_ref[rows(r, offset)], k_ref[piece], (((1,), (1,)), ((), ())), preferred_element_type=F32
-            )
+            return jnp.dot(q_ref[rows(r, offset)], k_ref[...], preferred_element_type=F32)
 
         following = scores(0)
         for r in range(0, chunk, sub):
             s = following
             if r + sub < chunk:
                 following = scores(r + sub)
-            old = m_ref[rows(r), :1]
-            best = jnp.maximum(jnp.max(s, axis=1, keepdims=True), old)
+            best = jnp.max(s, axis=1, keepdims=True)
+            if not first:
+                old = ins[0][rows(r, offset), :1]
+                best = jnp.maximum(best, old)
             weights = jnp.exp2(s - best).astype(BF16)
-            acc = jnp.dot(weights, v_ref[piece], preferred_element_type=F32)
-            acc = acc + a_ref[rows(r)] * jnp.exp2(old - best)
-            m_ref[rows(r)] = jnp.broadcast_to(best, (sub, HEAD_DIM))
-            a_ref[rows(r)] = acc
+            acc = jnp.dot(weights, v_ref[...], preferred_element_type=F32)
+            if not first:
+                acc = acc + ins[1][rows(r, offset)] * jnp.exp2(old - best)
+            if last:
+                outs[0][rows(r), :HEAD_DIM] = acc[:, :HEAD_DIM]
+                outs[0][rows(r), HEAD_DIM:] = jnp.where(lane < 64, acc[:, HEAD_DIM:], best)
+            else:
+                outs[0][rows(r)] = jnp.broadcast_to(best, (sub, HEAD_DIM))
+                outs[1][rows(r)] = acc
         return nothing
 
-    if steps * pieces == 1:
-        part(0, 0)
-    else:
-        lax.fori_loop(0, steps * pieces, part, 0)
-    if last:
-        lane = lax.broadcasted_iota(jnp.int32, m_ref.shape, 1)
-        out_ref[:, :HEAD_DIM] = a_ref[:, :HEAD_DIM]
-        out_ref[:, HEAD_DIM:] = jnp.where(lane < 64, a_ref[:, HEAD_DIM:], m_ref[...])
+    lax.fori_loop(0, outs[0].shape[0] // chunk, part, 0)
 
 
 def attend(q, kvs, carry, last=None):
@@ -221,10 +210,9 @@
         in_specs=[WHOLE] * (1 + pieces + (0 if first else 2)),
         out_specs=[WHOLE] * len(shapes),
         out_shape=shapes,
-        scratch_shapes=([] if last is None else [pltpu.VMEM((rows, HEAD_DIM), F32), pltpu.VMEM((rows, 2 * HEAD_DIM), F32)])
-        + [
-            pltpu.VMEM((pieces, count, HEAD_DIM), BF16),
-            pltpu.VMEM((pieces, count, 2 * HEAD_DIM), BF16),
+        scratch_shapes=[
+            pltpu.VMEM((HEAD_DIM, pieces * count), BF16),
+            pltpu.VMEM((pieces * count, 2 * HEAD_DIM), BF16),
         ],
         input_output_aliases={} if first or last is not None else {1 + pieces: 0, 2 + pieces: 1},
         compiler_params=pltpu.CompilerParams(vmem_limit_bytes=40 * 2**20),
@@ -262,7 +250,8 @@
 
 
 def start_x(column, half):
-    return column, turn(column, X, NX), shift(half, X, NX, 2)
+    near = turn(column, X, NX)
+    return column, near, shift(half, X, NX, 2)
 
 
 def finish_x(where, column, near, far):

time: 159 us -> 154 us (0.969)
  Pallas kernels: 37.9 us -> 33.6 us
    pallas_call x5, Pallas kernels: 30.8 us -> 26.5 us  [attend(): pl.pallas_call(functools.partial(attend_kernel, pieces=pieces, first=firs...]
  transfers between devices with their start and end apart: 30 -> 30, of which waited for: 10 -> 10; matrix products, arithmetic and copies ran while one was open for 1% -> 1% of each run, Pallas kernels for 23% -> 21%
where the time goes in v2:
time: 154 us
  waiting for transfers between devices  48.4 us (31%)
  starting transfers between devices  47 us (31%)
  Pallas kernels  33.6 us (22%)
  blocking collectives  19.5 us (13%)
  other arithmetic  4.12 us (3%)
    pallas_call x5, Pallas kernels, attend(): pl.pallas_call(functools.partial(attend_kernel, pieces=pieces, first=firs...  26.5 us
    all_to_all x1, blocking collectives, local(): summed = jnp.sum(lax.all_to_all(pieces, Y, 0, 0).astype(F32), axis=0)  19.5 us
    ppermute x8, waiting for transfers between devices, shift(): lax.ppermute(piece, axis, [(i, (i + by) % count) for i in range(count)])  15.4 us
    ppermute x9, waiting for transfers between devices, turn(): return lax.ppermute(piece, (axis, C), pairs)  14.9 us
    ppermute x9, starting transfers between devices, turn(): return lax.ppermute(piece, (axis, C), pairs)  13.5 us
    ppermute x8, starting transfers between devices, shift(): lax.ppermute(piece, axis, [(i, (i + by) % count) for i in range(count)])  13 us
    all_to_all x1, waiting for transfers between devices, everyone(): lax.all_to_all(jnp.broadcast_to(piece[None], (n,) + piece.shape), axes, 0...  11.7 us
    all_to_all x1, starting transfers between devices, everyone(): lax.all_to_all(jnp.broadcast_to(piece[None], (n,) + piece.shape), axes, 0...  11.2 us
  transfers between devices with their start and end apart: 30, of which 10 were waited for; matrix products, arithmetic and copies ran while one was open for 1% of the time, Pallas kernels for 21%

profile of v2, /device:TPU:32, one launch (start us, length us, event | category | flops | bytes accessed | tf_op | source)
XLA Modules:
  0.0 153.9 jit_solution(15603098514191975794)
XLA Ops:
  0.0 0.8 pad_maximum_fusion.3
  0.8 0.9 broadcast_in_dim.50
  1.6 11.2 %all-to-all-start = ((bf16[32,32,256]{2,1,0:T(8,128)(2,1)}), bf16[32,32,256]{2,1,0:T(8,128)(2,1)S(1)}, u32[]{:S(2)}, u32[]{:S(2)}) async-start(bf16[32,32,256]{2,1,0:T(8,128)(2,1)} %broadcast_in_dim.50), calls=%async_computation | async-start | bytes 1048576 | tf_op jit(solution)/shard_map/all_to_all | solution.py:54
  12.8 3.1 %collective-permute-start = (bf16[64,2048]{1,0:T(8,128)(2,1)}, bf16[64,2048]{1,0:T(8,128)(2,1)S(1)}, u32[]{:S(2)}, u32[]{:S(2)}) collective-permute-start(bf16[64,2048]{1,0:T(8,128)(2,1)} %t0.1), channel_id=1, source_target_pairs={{0,3},{1,0},{2,1},{3,2},{4,7},{5,4},{6,5},{7,6},{8,11},{9,8},{10,9... | collective-permute-start | bytes 786440 | tf_op jit(solution)/shard_map/ppermute | solution.py:42
  15.9 0.6 collective-permute-start.1
  16.5 1.0 collective-permute-start.2
  17.5 0.8 pad_maximum_fusion.2.own_ref
  18.3 11.7 %all-to-all-done.own = bf16[32,32,256]{2,1,0:T(8,128)(2,1)S(1)} async-done(((bf16[32,32,256]{2,1,0:T(8,128)(2,1)}), bf16[32,32,256]{2,1,0:T(8,128)(2,1)S(1)}, u32[]{:S(2)}, u32[]{:S(2)}) %all-to-all-start) | async-done | bytes 524320 | tf_op jit(solution)/shard_map/all_to_all | solution.py:54
  30.0 0.8 pad_maximum_fusion.1
  30.8 1.2 collective-permute-start.5
  32.0 0.6 collective-permute-start.6
  32.6 1.9 %collective-permute-start.7 = (bf16[64,1024]{1,0:T(8,128)(2,1)S(1)}, bf16[64,1024]{1,0:T(8,128)(2,1)S(1)}, u32[]{:S(2)}, u32[]{:S(2)}) collective-permute-start(bf16[64,1024]{1,0:T(8,128)(2,1)S(1)} %pad_maximum_fusion.1), channel_id=1, source_target_pairs={{0,96},{4,164},{32,128},{36,196},{64,160},{68,228},{96,192},{100,4... | collective-permute-start | bytes 393224 | tf_op jit(solution)/shard_map/ppermute | solution.py:49
  34.5 0.5 sine_multiply_fusion
  35.1 4.3 %collective-permute-start.8 = (bf16[32,1024]{1,0:T(8,128)(2,1)S(1)}, bf16[32,1024]{1,0:T(8,128)(2,1)S(1)}, u32[]{:S(2)}, u32[]{:S(2)}) collective-permute-start(bf16[32,1024]{1,0:T(8,128)(2,1)S(1)} %pad_maximum_fusion.2.own_ref), channel_id=1, source_target_pairs={{0,128},{4,132},{32,160},{36,164},{64,192},{68,196},{96,224},{100,... | collective-permute-start | bytes 196616 | tf_op jit(solution)/shard_map/ppermute | solution.py:49
  39.4 1.4 shard_map.73
  40.8 4.9 %collective-permute-done.8 = bf16[32,1024]{1,0:T(8,128)(2,1)S(1)} collective-permute-done((bf16[32,1024]{1,0:T(8,128)(2,1)S(1)}, bf16[32,1024]{1,0:T(8,128)(2,1)S(1)}, u32[]{:S(2)}, u32[]{:S(2)}) %collective-permute-start.8) | collective-permute-done | bytes 65568 | tf_op jit(solution)/shard_map/ppermute | solution.py:49
  45.7 1.5 collective-permute-done.7
  47.7 1.5 collective-permute-start.14
  49.2 0.6 collective-permute-start.15
  49.7 2.7 %collective-permute-start.16 = (bf16[256,256]{1,0:T(8,128)(2,1)S(1)}, bf16[256,256]{1,0:T(8,128)(2,1)S(1)}, u32[]{:S(2)}, u32[]{:S(2)}) collective-permute-start(bf16[256,256]{1,0:T(8,128)(2,1)S(1)} %get-tuple-element.22), channel_id=1, source_target_pairs={{0,24},{8,0},{16,8},{24,16},{1,25},{9,1},{17,9},{25,17},{2,26},{10... | collective-permute-start | bytes 393224 | tf_op jit(solution)/shard_map/ppermute | solution.py:42
  52.5 3.0 %collective-permute-done.14 = bf16[256,256]{1,0:T(8,128)(2,1)S(1)} collective-permute-done((bf16[256,256]{1,0:T(8,128)(2,1)S(1)}, bf16[256,256]{1,0:T(8,128)(2,1)S(1)}, u32[]{:S(2)}, u32[]{:S(2)}) %collective-permute-start.14) | collective-permute-done | bytes 131104 | tf_op jit(solution)/shard_map/ppermute | solution.py:42
  55.5 2.1 %collective-permute-done.15 = bf16[256,256]{1,0:T(8,128)(2,1)S(1)} collective-permute-done((bf16[256,256]{1,0:T(8,128)(2,1)S(1)}, bf16[256,256]{1,0:T(8,128)(2,1)S(1)}, u32[]{:S(2)}, u32[]{:S(2)}) %collective-permute-start.15) | collective-permute-done | bytes 131104 | tf_op jit(solution)/shard_map/ppermute | solution.py:42
  57.6 0.7 shard_map.74
  58.7 2.4 %collective-permute-start.21 = (bf16[1024,256]{1,0:T(8,128)(2,1)S(1)}, bf16[1024,256]{1,0:T(8,128)(2,1)S(1)}, u32[]{:S(2)}, u32[]{:S(2)}) collective-permute-start(bf16[1024,256]{1,0:T(8,128)(2,1)S(1)} %constant_dynamic-update-slice_fusion.4.refs_1_), channel_id=1, source_target_pairs={{0,32},{4,228},{32,64},{36,4},{64,96},{68,36},{96,128},{100,68},{1... | collective-permute-start | bytes 1572872 | tf_op jit(solution)/shard_map/ppermute | solution.py:38
  61.2 1.8 %collective-permute-start.11 = (bf16[256,512]{1,0:T(8,128)(2,1)S(1)}, bf16[256,512]{1,0:T(8,128)(2,1)S(1)}, u32[]{:S(2)}, u32[]{:S(2)}) collective-permute-start(bf16[256,512]{1,0:T(8,128)(2,1)S(1)} %get-tuple-element.28), channel_id=1, source_target_pairs={{0,16},{8,24},{16,0},{24,8},{1,17},{9,25},{17,1},{25,9},{2,18},{10... | collective-permute-start | bytes 786440 | tf_op jit(solution)/shard_map/ppermute | solution.py:42
  63.0 10.3 %collective-permute-done.11.far_ref = bf16[256,512]{1,0:T(8,128)(2,1)S(1)} collective-permute-done((bf16[256,512]{1,0:T(8,128)(2,1)S(1)}, bf16[256,512]{1,0:T(8,128)(2,1)S(1)}, u32[]{:S(2)}, u32[]{:S(2)}) %collective-permute-start.11) | collective-permute-done | bytes 262176 | tf_op jit(solution)/shard_map/ppermute | solution.py:42
  73.3 1.1 collective-permute-done.10.near_ref
  74.4 0.6 shard_map.75.rest
  75.1 2.3 %collective-permute-start.18 = (bf16[1024,256]{1,0:T(8,128)(2,1)S(1)}, bf16[1024,256]{1,0:T(8,128)(2,1)S(1)}, u32[]{:S(2)}, u32[]{:S(2)}) collective-permute-start(bf16[1024,256]{1,0:T(8,128)(2,1)S(1)} %collective-permute-done.17), channel_id=1, source_target_pairs={{0,32},{4,228},{32,64},{36,4},{64,96},{68,36},{96,128},{100,68},{1... | collective-permute-start | bytes 1572872 | tf_op jit(solution)/shard_map/ppermute | solution.py:38
  77.5 6.9 %collective-permute-done.18.refs_1_ = bf16[1024,256]{1,0:T(8,128)(2,1)S(1)} collective-permute-done((bf16[1024,256]{1,0:T(8,128)(2,1)S(1)}, bf16[1024,256]{1,0:T(8,128)(2,1)S(1)}, u32[]{:S(2)}, u32[]{:S(2)}) %collective-permute-start.18) | collective-permute-done | bytes 524320 | tf_op jit(solution)/shard_map/ppermute | solution.py:38
  84.3 2.2 %collective-permute-start.19 = (bf16[1024,256]{1,0:T(8,128)(2,1)S(1)}, bf16[1024,256]{1,0:T(8,128)(2,1)S(1)}, u32[]{:S(2)}, u32[]{:S(2)}) collective-permute-start(bf16[1024,256]{1,0:T(8,128)(2,1)S(1)} %collective-permute-done.18.refs_1_), channel_id=1, source_target_pairs={{0,32},{4,228},{32,64},{36,4},{64,96},{68,36},{96,128},{100,68},{1... | collective-permute-start | bytes 1572872 | tf_op jit(solution)/shard_map/ppermute | solution.py:38
  86.5 3.4 %collective-permute-done.22.refs_2_ = bf16[1024,256]{1,0:T(8,128)(2,1)S(1)} collective-permute-done((bf16[1024,256]{1,0:T(8,128)(2,1)S(1)}, bf16[1024,256]{1,0:T(8,128)(2,1)S(1)}, u32[]{:S(2)}, u32[]{:S(2)}) %collective-permute-start.22) | collective-permute-done | bytes 524320 | tf_op jit(solution)/shard_map/ppermute | solution.py:38
  90.0 2.2 %collective-permute-start.23 = (bf16[1024,256]{1,0:T(8,128)(2,1)S(1)}, bf16[1024,256]{1,0:T(8,128)(2,1)S(1)}, u32[]{:S(2)}, u32[]{:S(2)}) collective-permute-start(bf16[1024,256]{1,0:T(8,128)(2,1)S(1)} %collective-permute-done.22.refs_2_), channel_id=1, source_target_pairs={{0,32},{4,228},{32,64},{36,4},{64,96},{68,36},{96,128},{100,68},{1... | collective-permute-start | bytes 1572872 | tf_op jit(solution)/shard_map/ppermute | solution.py:38
  92.2 1.9 %shard_map.76 = bf16[1024,128]{1,0:T(8,128)(2,1)S(1)} custom-call(s32[4]{0:T(128)S(1)} %pad_add_fusion.i_ref, bf16[256,2048]{1,0:T(8,128)(2,1)S(1)} %get-tuple-element.21.t_ref, bf16[512,512]{1,0:T(8,128)(2,1)S(1)} %get-tuple-element.27.column, bf16[768,512]{1,0:T(8,128)(2,1)S(1)} %shard_map.75.rest, bf16[768,512]{1,0:T(8,128)(2,1)S(1)} %collective-permute-done.12.got, ...), custom_call_target="tpu_custom_call" | custom-call | bytes 4194304 | tf_op jit(solution)/shard_map/pallas_call | solution.py:62
  94.3 1.7 %collective-permute-start.27 = (bf16[256,512]{1,0:T(8,128)(2,1)S(1)}, bf16[256,512]{1,0:T(8,128)(2,1)S(1)}, u32[]{:S(2)}, u32[]{:S(2)}) collective-permute-start(bf16[256,512]{1,0:T(8,128)(2,1)S(1)} %get-tuple-element.36), channel_id=1, source_target_pairs={{0,16},{8,24},{16,0},{24,8},{1,17},{9,25},{17,1},{25,9},{2,18},{10... | collective-permute-start | bytes 786440 | tf_op jit(solution)/shard_map/ppermute | solution.py:42
  96.0 1.8 %collective-permute-start.20 = (bf16[1024,256]{1,0:T(8,128)(2,1)S(1)}, bf16[1024,256]{1,0:T(8,128)(2,1)S(1)}, u32[]{:S(2)}, u32[]{:S(2)}) collective-permute-start(bf16[1024,256]{1,0:T(8,128)(2,1)S(1)} %collective-permute-done.19.refs_1_), channel_id=1, source_target_pairs={{0,32},{4,228},{32,64},{36,4},{64,96},{68,36},{96,128},{100,68},{1... | collective-permute-start | bytes 1572872 | tf_op jit(solution)/shard_map/ppermute | solution.py:38
  97.8 3.4 %collective-permute-done.23.refs_2_ = bf16[1024,256]{1,0:T(8,128)(2,1)S(1)} collective-permute-done((bf16[1024,256]{1,0:T(8,128)(2,1)S(1)}, bf16[1024,256]{1,0:T(8,128)(2,1)S(1)}, u32[]{:S(2)}, u32[]{:S(2)}) %collective-permute-start.23) | collective-permute-done | bytes 524320 | tf_op jit(solution)/shard_map/ppermute | solution.py:38
  101.2 2.2 %collective-permute-start.24 = (bf16[1024,256]{1,0:T(8,128)(2,1)S(1)}, bf16[1024,256]{1,0:T(8,128)(2,1)S(1)}, u32[]{:S(2)}, u32[]{:S(2)}) collective-permute-start(bf16[1024,256]{1,0:T(8,128)(2,1)S(1)} %collective-permute-done.23.refs_2_), channel_id=1, source_target_pairs={{0,32},{4,228},{32,64},{36,4},{64,96},{68,36},{96,128},{100,68},{1... | collective-permute-start | bytes 1572872 | tf_op jit(solution)/shard_map/ppermute | solution.py:38
  103.4 6.3 %attend.5 = (f32[2048,128]{1,0:T(8,128)S(1)}, f32[2048,256]{1,0:T(8,128)S(1)}) custom-call(bf16[2048,128]{1,0:T(8,128)(2,1)S(1)} %pad_maximum_fusion.refs_0_, bf16[1024,256]{1,0:T(8,128)(2,1)S(1)} %constant_dynamic-update-slice_fusion.4.refs_1_, bf16[1024,256]{1,0:T(8,128)(2,1)S(1)} %collective-permute-done.21.refs_2_), custom_call_target="tpu_custom_call" | custom-call | flops 4294967296 | bytes 8388608 | tf_op jit(solution)/shard_map/attend/pallas_call | solution.py:208
  109.7 6.6 %attend.6 = (f32[2048,128]{1,0:T(8,128)S(1)}, f32[2048,256]{1,0:T(8,128)S(1)}) custom-call(bf16[2048,128]{1,0:T(8,128)(2,1)S(1)} %pad_maximum_fusion.refs_0_, bf16[1024,256]{1,0:T(8,128)(2,1)S(1)} %collective-permute-done.18.refs_1_, bf16[1024,256]{1,0:T(8,128)(2,1)S(1)} %collective-permute-done.22.refs_2_, ...), custom_call_target="tpu_custom_call", output_to_operand_aliasing={{0}: (3, {}), {1}: (4, {})} | custom-call | flops 4294967296 | bytes 8388608 | tf_op jit(solution)/shard_map/attend/pallas_call | solution.py:208
  116.3 6.6 %attend.7 = (f32[2048,128]{1,0:T(8,128)S(1)}, f32[2048,256]{1,0:T(8,128)S(1)}) custom-call(bf16[2048,128]{1,0:T(8,128)(2,1)S(1)} %pad_maximum_fusion.refs_0_, bf16[1024,256]{1,0:T(8,128)(2,1)S(1)} %collective-permute-done.19.refs_1_, bf16[1024,256]{1,0:T(8,128)(2,1)S(1)} %collective-permute-done.23.refs_2_, ...), custom_call_target="tpu_custom_call", output_to_operand_aliasing={{0}: (3, {}), {1}: (4, {})} | custom-call | flops 4294967296 | bytes 8388608 | tf_op jit(solution)/shard_map/attend/pallas_call | solution.py:208
  122.9 3.5 %attend.9 = f32[1024,256]{1,0:T(8,128)S(1)} custom-call(bf16[2048,128]{1,0:T(8,128)(2,1)S(1)} %pad_maximum_fusion.refs_0_, bf16[1024,256]{1,0:T(8,128)(2,1)S(1)} %collective-permute-done.20.refs_1_, bf16[1024,256]{1,0:T(8,128)(2,1)S(1)} %collective-permute-done.24.refs_2_, f32[2048,128]{1,0:T(8,128)S(1)} %get-tuple-element.33.refs_3_, ...), custom_call_target="tpu_custom_call" | custom-call | flops 2147483648 | bytes 8388608 | tf_op jit(solution)/shard_map/attend/pallas_call | solution.py:208
  126.6 0.6 shard_map.77.rest
  127.2 0.6 collective-permute-start.28
  127.7 3.5 %attend.8.own_ref = f32[1024,256]{1,0:T(8,128)S(1)} custom-call(bf16[2048,128]{1,0:T(8,128)(2,1)S(1)} %pad_maximum_fusion.refs_0_, bf16[1024,256]{1,0:T(8,128)(2,1)S(1)} %collective-permute-done.20.refs_1_, bf16[1024,256]{1,0:T(8,128)(2,1)S(1)} %collective-permute-done.24.refs_2_, f32[2048,128]{1,0:T(8,128)S(1)} %get-tuple-element.33.refs_3_, ...), custom_call_target="tpu_custom_call" | custom-call | flops 2147483648 | bytes 8388608 | tf_op jit(solution)/shard_map/attend/pallas_call | solution.py:208
  131.3 2.0 %shard_map.78 = bf16[256,2048]{1,0:T(8,128)(2,1)S(1)} custom-call(s32[4]{0:T(128)S(1)} %pad_add_fusion.i_ref, f32[1024,256]{1,0:T(8,128)S(1)} %attend.8.own_ref, f32[1024,256]{1,0:T(8,128)S(1)} %collective-permute-done.25.got_ref, bf16[512,512]{1,0:T(8,128)(2,1)S(1)} %get-tuple-element.35.column, bf16[768,512]{1,0:T(8,128)(2,1)S(1)} %shard_map.77.rest, ...), custom_call_target="tpu_custom_call" | custom-call | bytes 4194304 | tf_op jit(solution)/shard_map/pallas_call | solution.py:62
  133.3 19.5 %all_to_all.10 = bf16[4,64,2048]{2,1,0:T(8,128)(2,1)S(1)} all-to-all(bf16[4,64,2048]{2,1,0:T(8,128)(2,1)S(1)} %bitcast.8), channel_id=1, replica_groups=mesh['sp_0'=8,'sp_1'=4,'sp_2'=2,'tp'=4] {'tp'}, dimensions={0} | all-to-all | bytes 2097152 | tf_op jit(solution)/shard_map/all_to_all | solution.py:317
  153.1 0.8 multiply_convert_fusion
  (52 shorter events, 1.8 us)
Async XLA Ops:
  0.0 39.4 %copy-start = (bf16[64,2048]{1,0:T(8,128)(2,1)S(1)}, bf16[64,2048]{1,0:T(8,128)(2,1)}, u32[]{:S(2)}) copy-start(bf16[64,2048]{1,0:T(8,128)(2,1)} %t0.1) | copy-start | bytes 786436
  0.0 39.4 %copy-start.2 = (f32[128]{0:T(128)S(1)}, f32[128]{0:T(128)}, u32[]{:S(2)}) copy-start(f32[128]{0:T(128)} %param.13) | copy-start | bytes 1540
  1.6 28.4 %all-to-all-start = ((bf16[32,32,256]{2,1,0:T(8,128)(2,1)}), bf16[32,32,256]{2,1,0:T(8,128)(2,1)S(1)}, u32[]{:S(2)}, u32[]{:S(2)}) async-start(bf16[32,32,256]{2,1,0:T(8,128)(2,1)} %broadcast_in_dim.50), calls=%async_computation | async-start | bytes 1048576 | tf_op jit(solution)/shard_map/all_to_all | solution.py:54
  12.8 19.2 %collective-permute-start = (bf16[64,2048]{1,0:T(8,128)(2,1)}, bf16[64,2048]{1,0:T(8,128)(2,1)S(1)}, u32[]{:S(2)}, u32[]{:S(2)}) collective-permute-start(bf16[64,2048]{1,0:T(8,128)(2,1)} %t0.1), channel_id=1, source_target_pairs={{0,3},{1,0},{2,1},{3,2},{4,7},{5,4},{6,5},{7,6},{8,11},{9,8},{10,9... | collective-permute-start | bytes 786440 | tf_op jit(solution)/shard_map/ppermute | solution.py:42
  15.9 16.7 %collective-permute-start.1 = (bf16[64,2048]{1,0:T(8,128)(2,1)}, bf16[64,2048]{1,0:T(8,128)(2,1)S(1)}, u32[]{:S(2)}, u32[]{:S(2)}) collective-permute-start(bf16[64,2048]{1,0:T(8,128)(2,1)} %t0.1), channel_id=1, source_target_pairs={{0,2},{1,3},{2,0},{3,1},{4,6},{5,7},{6,4},{7,5},{8,10},{9,11},{10,... | collective-permute-start | bytes 786440 | tf_op jit(solution)/shard_map/ppermute | solution.py:42
  16.5 18.5 %collective-permute-start.2 = (bf16[64,2048]{1,0:T(8,128)(2,1)}, bf16[64,2048]{1,0:T(8,128)(2,1)S(1)}, u32[]{:S(2)}, u32[]{:S(2)}) collective-permute-start(bf16[64,2048]{1,0:T(8,128)(2,1)} %t0.1), channel_id=1, source_target_pairs={{0,1},{1,2},{2,3},{3,0},{4,5},{5,6},{6,7},{7,4},{8,9},{9,10},{10,1... | collective-permute-start | bytes 786440 | tf_op jit(solution)/shard_map/ppermute | solution.py:42
  18.3 11.7 %collective-permute-start.4 = (bf16[32,1024]{1,0:T(8,128)(2,1)S(1)}, bf16[32,1024]{1,0:T(8,128)(2,1)S(1)}, u32[]{:S(2)}, u32[]{:S(2)}) collective-permute-start(bf16[32,1024]{1,0:T(8,128)(2,1)S(1)} %pad_maximum_fusion.2.own_ref), channel_id=1, source_target_pairs={{0,4},{4,0},{1,5},{5,1},{2,6},{6,2},{3,7},{7,3},{8,12},{12,8},{9,1... | collective-permute-start | bytes 196616 | tf_op jit(solution)/shard_map/ppermute | solution.py:31
  30.0 9.4 %collective-permute-start.3 = (bf16[32,32,256]{2,1,0:T(8,128)(2,1)S(1)}, bf16[32,32,256]{2,1,0:T(8,128)(2,1)S(1)}, u32[]{:S(2)}, u32[]{:S(2)}) collective-permute-start(bf16[32,32,256]{2,1,0:T(8,128)(2,1)S(1)} %all-to-all-done.own), channel_id=1, source_target_pairs={{0,4},{4,0},{1,5},{5,1},{2,6},{6,2},{3,7},{7,3},{8,12},{12,8},{9,1... | collective-permute-start | bytes 1572872 | tf_op jit(solution)/shard_map/ppermute | solution.py:31
  30.8 14.9 %collective-permute-start.5 = (bf16[64,1024]{1,0:T(8,128)(2,1)S(1)}, bf16[64,1024]{1,0:T(8,128)(2,1)S(1)}, u32[]{:S(2)}, u32[]{:S(2)}) collective-permute-start(bf16[64,1024]{1,0:T(8,128)(2,1)S(1)} %pad_maximum_fusion.1), channel_id=1, source_target_pairs={{0,32},{4,228},{32,64},{36,4},{64,96},{68,36},{96,128},{100,68},{1... | collective-permute-start | bytes 393224 | tf_op jit(solution)/shard_map/ppermute | solution.py:49
  32.0 13.7 %collective-permute-start.6 = (bf16[64,1024]{1,0:T(8,128)(2,1)S(1)}, bf16[64,1024]{1,0:T(8,128)(2,1)S(1)}, u32[]{:S(2)}, u32[]{:S(2)}) collective-permute-start(bf16[64,1024]{1,0:T(8,128)(2,1)S(1)} %pad_maximum_fusion.1), channel_id=1, source_target_pairs={{0,64},{4,196},{32,96},{36,228},{64,128},{68,4},{96,160},{100,36},... | collective-permute-start | bytes 393224 | tf_op jit(solution)/shard_map/ppermute | solution.py:49
  32.6 14.6 %collective-permute-start.7 = (bf16[64,1024]{1,0:T(8,128)(2,1)S(1)}, bf16[64,1024]{1,0:T(8,128)(2,1)S(1)}, u32[]{:S(2)}, u32[]{:S(2)}) collective-permute-start(bf16[64,1024]{1,0:T(8,128)(2,1)S(1)} %pad_maximum_fusion.1), channel_id=1, source_target_pairs={{0,96},{4,164},{32,128},{36,196},{64,160},{68,228},{96,192},{100,4... | collective-permute-start | bytes 393224 | tf_op jit(solution)/shard_map/ppermute | solution.py:49
  35.1 10.6 %collective-permute-start.8 = (bf16[32,1024]{1,0:T(8,128)(2,1)S(1)}, bf16[32,1024]{1,0:T(8,128)(2,1)S(1)}, u32[]{:S(2)}, u32[]{:S(2)}) collective-permute-start(bf16[32,1024]{1,0:T(8,128)(2,1)S(1)} %pad_maximum_fusion.2.own_ref), channel_id=1, source_target_pairs={{0,128},{4,132},{32,160},{36,164},{64,192},{68,196},{96,224},{100,... | collective-permute-start | bytes 196616 | tf_op jit(solution)/shard_map/ppermute | solution.py:49
  47.2 44.9 %copy-start.1 = (f32[128]{0:T(128)S(1)}, f32[128]{0:T(128)}, u32[]{:S(2)}) copy-start(f32[128]{0:T(128)} %param.12) | copy-start | bytes 1540
  47.3 10.3 %collective-permute-start.9 = (bf16[224,1024]{1,0:T(8,128)(2,1)S(1)}, bf16[224,1024]{1,0:T(8,128)(2,1)S(1)}, u32[]{:S(2)}, u32[]{:S(2)}) collective-permute-start(bf16[224,1024]{1,0:T(8,128)(2,1)S(1)} %constant_dynamic-update-slice_fusion.mine_ref), channel_id=1, source_target_pairs={{0,4},{4,0},{1,5},{5,1},{2,6},{6,2},{3,7},{7,3},{8,12},{12,8},{9,1... | collective-permute-start | bytes 1376264 | tf_op jit(solution)/shard_map/ppermute | solution.py:31
  47.7 7.9 %collective-permute-start.14 = (bf16[256,256]{1,0:T(8,128)(2,1)S(1)}, bf16[256,256]{1,0:T(8,128)(2,1)S(1)}, u32[]{:S(2)}, u32[]{:S(2)}) collective-permute-start(bf16[256,256]{1,0:T(8,128)(2,1)S(1)} %get-tuple-element.22), channel_id=1, source_target_pairs={{0,16},{8,24},{16,0},{24,8},{1,17},{9,25},{17,1},{25,9},{2,18},{10... | collective-permute-start | bytes 393224 | tf_op jit(solution)/shard_map/ppermute | solution.py:42
  49.2 8.4 %collective-permute-start.15 = (bf16[256,256]{1,0:T(8,128)(2,1)S(1)}, bf16[256,256]{1,0:T(8,128)(2,1)S(1)}, u32[]{:S(2)}, u32[]{:S(2)}) collective-permute-start(bf16[256,256]{1,0:T(8,128)(2,1)S(1)} %get-tuple-element.22), channel_id=1, source_target_pairs={{0,8},{8,16},{16,24},{24,0},{1,9},{9,17},{17,25},{25,1},{2,10},{10... | collective-permute-start | bytes 393224 | tf_op jit(solution)/shard_map/ppermute | solution.py:42
  49.7 8.9 %collective-permute-start.16 = (bf16[256,256]{1,0:T(8,128)(2,1)S(1)}, bf16[256,256]{1,0:T(8,128)(2,1)S(1)}, u32[]{:S(2)}, u32[]{:S(2)}) collective-permute-start(bf16[256,256]{1,0:T(8,128)(2,1)S(1)} %get-tuple-element.22), channel_id=1, source_target_pairs={{0,24},{8,0},{16,8},{24,16},{1,25},{9,1},{17,9},{25,17},{2,26},{10... | collective-permute-start | bytes 393224 | tf_op jit(solution)/shard_map/ppermute | solution.py:42
  58.3 16.1 %collective-permute-start.10 = (bf16[512,512]{1,0:T(8,128)(2,1)S(1)}, bf16[512,512]{1,0:T(8,128)(2,1)S(1)}, u32[]{:S(2)}, u32[]{:S(2)}) collective-permute-start(bf16[512,512]{1,0:T(8,128)(2,1)S(1)} %get-tuple-element.27.column), channel_id=1, source_target_pairs={{0,8},{4,28},{8,16},{12,4},{16,24},{20,12},{24,0},{28,20},{1,9},{5... | collective-permute-start | bytes 1572872 | tf_op jit(solution)/shard_map/ppermute | solution.py:38
  58.6 16.5 %collective-permute-start.17 = (bf16[1024,256]{1,0:T(8,128)(2,1)S(1)}, bf16[1024,256]{1,0:T(8,128)(2,1)S(1)}, u32[]{:S(2)}, u32[]{:S(2)}) collective-permute-start(bf16[1024,256]{1,0:T(8,128)(2,1)S(1)} %constant_dynamic-update-slice_fusion.4.refs_1_), channel_id=1, source_target_pairs={{0,4},{4,0},{1,5},{5,1},{2,6},{6,2},{3,7},{7,3},{8,12},{12,8},{9,1... | collective-permute-start | bytes 1572872 | tf_op jit(solution)/shard_map/ppermute | solution.py:31
  58.7 18.6 %collective-permute-start.21 = (bf16[1024,256]{1,0:T(8,128)(2,1)S(1)}, bf16[1024,256]{1,0:T(8,128)(2,1)S(1)}, u32[]{:S(2)}, u32[]{:S(2)}) collective-permute-start(bf16[1024,256]{1,0:T(8,128)(2,1)S(1)} %constant_dynamic-update-slice_fusion.4.refs_1_), channel_id=1, source_target_pairs={{0,32},{4,228},{32,64},{36,4},{64,96},{68,36},{96,128},{100,68},{1... | collective-permute-start | bytes 1572872 | tf_op jit(solution)/shard_map/ppermute | solution.py:38
  61.2 12.1 %collective-permute-start.11 = (bf16[256,512]{1,0:T(8,128)(2,1)S(1)}, bf16[256,512]{1,0:T(8,128)(2,1)S(1)}, u32[]{:S(2)}, u32[]{:S(2)}) collective-permute-start(bf16[256,512]{1,0:T(8,128)(2,1)S(1)} %get-tuple-element.28), channel_id=1, source_target_pairs={{0,16},{8,24},{16,0},{24,8},{1,17},{9,25},{17,1},{25,9},{2,18},{10... | collective-permute-start | bytes 786440 | tf_op jit(solution)/shard_map/ppermute | solution.py:42
  75.0 17.2 %collective-permute-start.12 = (bf16[768,512]{1,0:T(8,128)(2,1)S(1)}, bf16[768,512]{1,0:T(8,128)(2,1)S(1)}, u32[]{:S(2)}, u32[]{:S(2)}) collective-permute-start(bf16[768,512]{1,0:T(8,128)(2,1)S(1)} %shard_map.75.rest), channel_id=1, source_target_pairs={{0,4},{4,0},{1,5},{5,1},{2,6},{6,2},{3,7},{7,3},{8,12},{12,8},{9,1... | collective-permute-start | bytes 2359304 | tf_op jit(solution)/shard_map/ppermute | solution.py:31
  75.1 9.3 %collective-permute-start.18 = (bf16[1024,256]{1,0:T(8,128)(2,1)S(1)}, bf16[1024,256]{1,0:T(8,128)(2,1)S(1)}, u32[]{:S(2)}, u32[]{:S(2)}) collective-permute-start(bf16[1024,256]{1,0:T(8,128)(2,1)S(1)} %collective-permute-done.17), channel_id=1, source_target_pairs={{0,32},{4,228},{32,64},{36,4},{64,96},{68,36},{96,128},{100,68},{1... | collective-permute-start | bytes 1572872 | tf_op jit(solution)/shard_map/ppermute | solution.py:38
  77.4 12.6 %collective-permute-start.22 = (bf16[1024,256]{1,0:T(8,128)(2,1)S(1)}, bf16[1024,256]{1,0:T(8,128)(2,1)S(1)}, u32[]{:S(2)}, u32[]{:S(2)}) collective-permute-start(bf16[1024,256]{1,0:T(8,128)(2,1)S(1)} %collective-permute-done.21.refs_2_), channel_id=1, source_target_pairs={{0,32},{4,228},{32,64},{36,4},{64,96},{68,36},{96,128},{100,68},{1... | collective-permute-start | bytes 1572872 | tf_op jit(solution)/shard_map/ppermute | solution.py:38
  84.3 11.6 %collective-permute-start.19 = (bf16[1024,256]{1,0:T(8,128)(2,1)S(1)}, bf16[1024,256]{1,0:T(8,128)(2,1)S(1)}, u32[]{:S(2)}, u32[]{:S(2)}) collective-permute-start(bf16[1024,256]{1,0:T(8,128)(2,1)S(1)} %collective-permute-done.18.refs_1_), channel_id=1, source_target_pairs={{0,32},{4,228},{32,64},{36,4},{64,96},{68,36},{96,128},{100,68},{1... | collective-permute-start | bytes 1572872 | tf_op jit(solution)/shard_map/ppermute | solution.py:38
  90.0 11.2 %collective-permute-start.23 = (bf16[1024,256]{1,0:T(8,128)(2,1)S(1)}, bf16[1024,256]{1,0:T(8,128)(2,1)S(1)}, u32[]{:S(2)}, u32[]{:S(2)}) collective-permute-start(bf16[1024,256]{1,0:T(8,128)(2,1)S(1)} %collective-permute-done.22.refs_2_), channel_id=1, source_target_pairs={{0,32},{4,228},{32,64},{36,4},{64,96},{68,36},{96,128},{100,68},{1... | collective-permute-start | bytes 1572872 | tf_op jit(solution)/shard_map/ppermute | solution.py:38
  94.1 9.3 %collective-permute-start.13 = (bf16[1024,128]{1,0:T(8,128)(2,1)S(1)}, bf16[1024,128]{1,0:T(8,128)(2,1)S(1)}, u32[]{:S(2)}, u32[]{:S(2)}) collective-permute-start(bf16[1024,128]{1,0:T(8,128)(2,1)S(1)} %shard_map.76), channel_id=1, source_target_pairs={{0,4},{4,0},{1,5},{5,1},{2,6},{6,2},{3,7},{7,3},{8,12},{12,8},{9,1... | collective-permute-start | bytes 786440 | tf_op jit(solution)/shard_map/ppermute | solution.py:31
  94.2 32.4 %collective-permute-start.26 = (bf16[512,512]{1,0:T(8,128)(2,1)S(1)}, bf16[512,512]{1,0:T(8,128)(2,1)S(1)}, u32[]{:S(2)}, u32[]{:S(2)}) collective-permute-start(bf16[512,512]{1,0:T(8,128)(2,1)S(1)} %get-tuple-element.35.column), channel_id=1, source_target_pairs={{0,8},{4,28},{8,16},{12,4},{16,24},{20,12},{24,0},{28,20},{1,9},{5... | collective-permute-start | bytes 1572872 | tf_op jit(solution)/shard_map/ppermute | solution.py:38
  94.3 32.3 %collective-permute-start.27 = (bf16[256,512]{1,0:T(8,128)(2,1)S(1)}, bf16[256,512]{1,0:T(8,128)(2,1)S(1)}, u32[]{:S(2)}, u32[]{:S(2)}) collective-permute-start(bf16[256,512]{1,0:T(8,128)(2,1)S(1)} %get-tuple-element.36), channel_id=1, source_target_pairs={{0,16},{8,24},{16,0},{24,8},{1,17},{9,25},{17,1},{25,9},{2,18},{10... | collective-permute-start | bytes 786440 | tf_op jit(solution)/shard_map/ppermute | solution.py:42
  96.0 26.9 %collective-permute-start.20 = (bf16[1024,256]{1,0:T(8,128)(2,1)S(1)}, bf16[1024,256]{1,0:T(8,128)(2,1)S(1)}, u32[]{:S(2)}, u32[]{:S(2)}) collective-permute-start(bf16[1024,256]{1,0:T(8,128)(2,1)S(1)} %collective-permute-done.19.refs_1_), channel_id=1, source_target_pairs={{0,32},{4,228},{32,64},{36,4},{64,96},{68,36},{96,128},{100,68},{1... | collective-permute-start | bytes 1572872 | tf_op jit(solution)/shard_map/ppermute | solution.py:38
  101.2 21.7 %collective-permute-start.24 = (bf16[1024,256]{1,0:T(8,128)(2,1)S(1)}, bf16[1024,256]{1,0:T(8,128)(2,1)S(1)}, u32[]{:S(2)}, u32[]{:S(2)}) collective-permute-start(bf16[1024,256]{1,0:T(8,128)(2,1)S(1)} %collective-permute-done.23.refs_2_), channel_id=1, source_target_pairs={{0,32},{4,228},{32,64},{36,4},{64,96},{68,36},{96,128},{100,68},{1... | collective-permute-start | bytes 1572872 | tf_op jit(solution)/shard_map/ppermute | solution.py:38
  126.4 4.8 %collective-permute-start.25 = (f32[1024,256]{1,0:T(8,128)S(1)}, f32[1024,256]{1,0:T(8,128)S(1)}, u32[]{:S(2)}, u32[]{:S(2)}) collective-permute-start(f32[1024,256]{1,0:T(8,128)S(1)} %attend.9), channel_id=1, source_target_pairs={{0,4},{4,0},{1,5},{5,1},{2,6},{6,2},{3,7},{7,3},{8,12},{12,8},{9,1... | collective-permute-start | bytes 3145736 | tf_op jit(solution)/shard_map/ppermute | solution.py:31
  127.2 4.1 %collective-permute-start.28 = (bf16[768,512]{1,0:T(8,128)(2,1)S(1)}, bf16[768,512]{1,0:T(8,128)(2,1)S(1)}, u32[]{:S(2)}, u32[]{:S(2)}) collective-permute-start(bf16[768,512]{1,0:T(8,128)(2,1)S(1)} %shard_map.77.rest), channel_id=1, source_target_pairs={{0,4},{4,0},{1,5},{5,1},{2,6},{6,2},{3,7},{7,3},{8,12},{12,8},{9,1... | collective-permute-start | bytes 2359304 | tf_op jit(solution)/shard_map/ppermute | solution.py:31

commit v3 on v2

--- a/solution.py
+++ b/solution.py
@@ -157,7 +157,7 @@
         q_ref[h * rows : (h + 1) * rows, :] = rotated(head, gain[...], cosine[...], sine[...], scale)
 
 
-def attend_kernel(*refs, pieces, first, last, offset):
+def attend_kernel(*refs, pieces, chunk, first, last, offset):
     q_ref, *kv_refs = refs[: 1 + pieces]
     ins = refs[1 + pieces : 1 + pieces + (0 if first else 2)]
     *outs, k_ref, v_ref = refs[1 + pieces + len(ins) :]
@@ -166,7 +166,7 @@
         k_ref[:, keys] = ref[:, :HEAD_DIM].T
         v_ref[keys, :HEAD_DIM] = ref[:, HEAD_DIM:]
     v_ref[:, HEAD_DIM:] = jnp.ones((v_ref.shape[0], HEAD_DIM), BF16)
-    sub, chunk = 128, 512
+    sub = 128
     lane = lax.broadcasted_iota(jnp.int32, (sub, HEAD_DIM), 1)
 
     def part(t, nothing):
@@ -200,13 +200,13 @@
     lax.fori_loop(0, outs[0].shape[0] // chunk, part, 0)
 
 
-def attend(q, kvs, carry, last=None):
+def attend(q, kvs, carry, chunk, last=None):
     first, count = carry is None, kvs[0].shape[0]
     rows = q.shape[0] // (1 if last is None else 2)
     shapes = [jax.ShapeDtypeStruct((rows, n), F32) for n in ((HEAD_DIM, 2 * HEAD_DIM) if last is None else (2 * HEAD_DIM,))]
     pieces = len(kvs)
     out = pl.pallas_call(
-        functools.partial(attend_kernel, pieces=pieces, first=first, last=last is not None, offset=(last or 0) * rows),
+        functools.partial(attend_kernel, pieces=pieces, chunk=chunk, first=first, last=last is not None, offset=(last or 0) * rows),
         in_specs=[WHOLE] * (1 + pieces + (0 if first else 2)),
         out_specs=[WHOLE] * len(shapes),
         out_shape=shapes,
@@ -302,13 +302,13 @@
         for name in "ab" if step < 4 else "a":
             chain[name] = turn(chain[name], Z, NZ)
             todo.append(chain[name])
-    for i, at_once in enumerate((todo[0:2], todo[2:4], todo[4:6])):
-        carry = attend(q_all, at_once, carry)
+    for i, at_once in enumerate((todo[0:2], todo[2:3], todo[3:5], todo[5:7])):
+        carry = attend(q_all, at_once, carry, 1024 if i in (1, 3) else 512)
         if i == 1:
             wo_all = finish_x(where, wo_column, *wo_parts)
-    theirs = attend(q_all, todo[6:], carry, last=1)
+    theirs = attend(q_all, todo[7:], carry, 1024, last=1)
     got = other_core(theirs)
-    own = attend(q_all, todo[6:], carry, last=0)
+    own = attend(q_all, todo[7:], carry, 1024, last=0)
     (partial,) = call(
         project_out_kernel, [((rows, tokens.shape[1]), BF16)], where, own, got, *wo_all,
         scratch=[pltpu.VMEM((2048, 512), BF16), pltpu.VMEM((rows, GROUP * HEAD_DIM), BF16)],

time: 154 us -> 154 us (level)
    pallas_call x5 -> x6, Pallas kernels: 26.5 us -> 25.6 us  [attend(): pl.pallas_call(functools.partial(attend_kernel, pieces=pieces, chunk=chun...]
  transfers between devices with their start and end apart: 30 -> 30, of which waited for: 10 -> 11; matrix products, arithmetic and copies ran while one was open for 1% -> 1% of each run, Pallas kernels for 21% -> 20%
where the time goes in v3:
time: 154 us
  waiting for transfers between devices  49 us (32%)
  starting transfers between devices  47.2 us (31%)
  Pallas kernels  32.7 us (21%)
  blocking collectives  19.6 us (13%)
  other arithmetic  4.12 us (3%)
    pallas_call x6, Pallas kernels, attend(): pl.pallas_call(functools.partial(attend_kernel, pieces=pieces, chunk=chun...  25.6 us
    all_to_all x1, blocking collectives, local(): summed = jnp.sum(lax.all_to_all(pieces, Y, 0, 0).astype(F32), axis=0)  19.6 us
    ppermute x8, waiting for transfers between devices, shift(): lax.ppermute(piece, axis, [(i, (i + by) % count) for i in range(count)])  15.4 us
    ppermute x9, waiting for transfers between devices, turn(): return lax.ppermute(piece, (axis, C), pairs)  14.9 us
    ppermute x9, starting transfers between devices, turn(): return lax.ppermute(piece, (axis, C), pairs)  13.5 us
    ppermute x8, starting transfers between devices, shift(): lax.ppermute(piece, axis, [(i, (i + by) % count) for i in range(count)])  13 us
    all_to_all x1, waiting for transfers between devices, everyone(): lax.all_to_all(jnp.broadcast_to(piece[None], (n,) + piece.shape), axes, 0...  11.7 us
    all_to_all x1, starting transfers between devices, everyone(): lax.all_to_all(jnp.broadcast_to(piece[None], (n,) + piece.shape), axes, 0...  11.2 us
  transfers between devices with their start and end apart: 30, of which 11 were waited for; matrix products, arithmetic and copies ran while one was open for 1% of the time, Pallas kernels for 20%

profile of v3, /device:TPU:32, one launch (start us, length us, event | category | flops | bytes accessed | tf_op | source)
XLA Modules:
  0.0 154.0 jit_solution(8128756647975449074)
XLA Ops:
  0.0 0.8 pad_maximum_fusion.3
  0.8 0.9 broadcast_in_dim.50
  1.6 11.2 %all-to-all-start = ((bf16[32,32,256]{2,1,0:T(8,128)(2,1)}), bf16[32,32,256]{2,1,0:T(8,128)(2,1)S(1)}, u32[]{:S(2)}, u32[]{:S(2)}) async-start(bf16[32,32,256]{2,1,0:T(8,128)(2,1)} %broadcast_in_dim.50), calls=%async_computation | async-start | bytes 1048576 | tf_op jit(solution)/shard_map/all_to_all | solution.py:54
  12.8 3.1 %collective-permute-start = (bf16[64,2048]{1,0:T(8,128)(2,1)}, bf16[64,2048]{1,0:T(8,128)(2,1)S(1)}, u32[]{:S(2)}, u32[]{:S(2)}) collective-permute-start(bf16[64,2048]{1,0:T(8,128)(2,1)} %t0.1), channel_id=1, source_target_pairs={{0,3},{1,0},{2,1},{3,2},{4,7},{5,4},{6,5},{7,6},{8,11},{9,8},{10,9... | collective-permute-start | bytes 786440 | tf_op jit(solution)/shard_map/ppermute | solution.py:42
  15.9 0.6 collective-permute-start.1
  16.5 1.0 collective-permute-start.2
  17.5 0.8 pad_maximum_fusion.2.own_ref
  18.3 11.7 %all-to-all-done.own = bf16[32,32,256]{2,1,0:T(8,128)(2,1)S(1)} async-done(((bf16[32,32,256]{2,1,0:T(8,128)(2,1)}), bf16[32,32,256]{2,1,0:T(8,128)(2,1)S(1)}, u32[]{:S(2)}, u32[]{:S(2)}) %all-to-all-start) | async-done | bytes 524320 | tf_op jit(solution)/shard_map/all_to_all | solution.py:54
  30.0 0.8 pad_maximum_fusion.1
  30.8 1.2 collective-permute-start.5
  32.0 0.6 collective-permute-start.6
  32.6 1.9 %collective-permute-start.7 = (bf16[64,1024]{1,0:T(8,128)(2,1)S(1)}, bf16[64,1024]{1,0:T(8,128)(2,1)S(1)}, u32[]{:S(2)}, u32[]{:S(2)}) collective-permute-start(bf16[64,1024]{1,0:T(8,128)(2,1)S(1)} %pad_maximum_fusion.1), channel_id=1, source_target_pairs={{0,96},{4,164},{32,128},{36,196},{64,160},{68,228},{96,192},{100,4... | collective-permute-start | bytes 393224 | tf_op jit(solution)/shard_map/ppermute | solution.py:49
  35.1 4.3 %collective-permute-start.8 = (bf16[32,1024]{1,0:T(8,128)(2,1)S(1)}, bf16[32,1024]{1,0:T(8,128)(2,1)S(1)}, u32[]{:S(2)}, u32[]{:S(2)}) collective-permute-start(bf16[32,1024]{1,0:T(8,128)(2,1)S(1)} %pad_maximum_fusion.2.own_ref), channel_id=1, source_target_pairs={{0,128},{4,132},{32,160},{36,164},{64,192},{68,196},{96,224},{100,... | collective-permute-start | bytes 196616 | tf_op jit(solution)/shard_map/ppermute | solution.py:49
  39.4 1.4 shard_map.73
  40.8 4.9 %collective-permute-done.8 = bf16[32,1024]{1,0:T(8,128)(2,1)S(1)} collective-permute-done((bf16[32,1024]{1,0:T(8,128)(2,1)S(1)}, bf16[32,1024]{1,0:T(8,128)(2,1)S(1)}, u32[]{:S(2)}, u32[]{:S(2)}) %collective-permute-start.8) | collective-permute-done | bytes 65568 | tf_op jit(solution)/shard_map/ppermute | solution.py:49
  45.7 1.5 collective-permute-done.7
  47.6 1.5 collective-permute-start.14
  49.2 0.6 collective-permute-start.15
  49.7 2.7 %collective-permute-start.16 = (bf16[256,256]{1,0:T(8,128)(2,1)S(1)}, bf16[256,256]{1,0:T(8,128)(2,1)S(1)}, u32[]{:S(2)}, u32[]{:S(2)}) collective-permute-start(bf16[256,256]{1,0:T(8,128)(2,1)S(1)} %get-tuple-element.24), channel_id=1, source_target_pairs={{0,24},{8,0},{16,8},{24,16},{1,25},{9,1},{17,9},{25,17},{2,26},{10... | collective-permute-start | bytes 393224 | tf_op jit(solution)/shard_map/ppermute | solution.py:42
  52.5 3.0 %collective-permute-done.14 = bf16[256,256]{1,0:T(8,128)(2,1)S(1)} collective-permute-done((bf16[256,256]{1,0:T(8,128)(2,1)S(1)}, bf16[256,256]{1,0:T(8,128)(2,1)S(1)}, u32[]{:S(2)}, u32[]{:S(2)}) %collective-permute-start.14) | collective-permute-done | bytes 131104 | tf_op jit(solution)/shard_map/ppermute | solution.py:42
  55.5 2.1 %collective-permute-done.15 = bf16[256,256]{1,0:T(8,128)(2,1)S(1)} collective-permute-done((bf16[256,256]{1,0:T(8,128)(2,1)S(1)}, bf16[256,256]{1,0:T(8,128)(2,1)S(1)}, u32[]{:S(2)}, u32[]{:S(2)}) %collective-permute-start.15) | collective-permute-done | bytes 131104 | tf_op jit(solution)/shard_map/ppermute | solution.py:42
  57.6 0.7 shard_map.74
  58.7 2.4 %collective-permute-start.17 = (bf16[1024,256]{1,0:T(8,128)(2,1)S(1)}, bf16[1024,256]{1,0:T(8,128)(2,1)S(1)}, u32[]{:S(2)}, u32[]{:S(2)}) collective-permute-start(bf16[1024,256]{1,0:T(8,128)(2,1)S(1)} %constant_dynamic-update-slice_fusion.4.refs_1_), channel_id=1, source_target_pairs={{0,32},{4,228},{32,64},{36,4},{64,96},{68,36},{96,128},{100,68},{1... | collective-permute-start | bytes 1572872 | tf_op jit(solution)/shard_map/ppermute | solution.py:38
  61.1 1.8 %collective-permute-start.11 = (bf16[256,512]{1,0:T(8,128)(2,1)S(1)}, bf16[256,512]{1,0:T(8,128)(2,1)S(1)}, u32[]{:S(2)}, u32[]{:S(2)}) collective-permute-start(bf16[256,512]{1,0:T(8,128)(2,1)S(1)} %get-tuple-element.30), channel_id=1, source_target_pairs={{0,16},{8,24},{16,0},{24,8},{1,17},{9,25},{17,1},{25,9},{2,18},{10... | collective-permute-start | bytes 786440 | tf_op jit(solution)/shard_map/ppermute | solution.py:42
  63.0 10.3 %collective-permute-done.11.far_ref = bf16[256,512]{1,0:T(8,128)(2,1)S(1)} collective-permute-done((bf16[256,512]{1,0:T(8,128)(2,1)S(1)}, bf16[256,512]{1,0:T(8,128)(2,1)S(1)}, u32[]{:S(2)}, u32[]{:S(2)}) %collective-permute-start.11) | collective-permute-done | bytes 262176 | tf_op jit(solution)/shard_map/ppermute | solution.py:42
  73.3 1.1 collective-permute-done.10.near_ref
  74.4 0.6 shard_map.75.rest
  75.1 2.3 %collective-permute-start.22 = (bf16[1024,256]{1,0:T(8,128)(2,1)S(1)}, bf16[1024,256]{1,0:T(8,128)(2,1)S(1)}, u32[]{:S(2)}, u32[]{:S(2)}) collective-permute-start(bf16[1024,256]{1,0:T(8,128)(2,1)S(1)} %collective-permute-done.21), channel_id=1, source_target_pairs={{0,32},{4,228},{32,64},{36,4},{64,96},{68,36},{96,128},{100,68},{1... | collective-permute-start | bytes 1572872 | tf_op jit(solution)/shard_map/ppermute | solution.py:38
  77.4 6.9 %collective-permute-done.22.refs_1_ = bf16[1024,256]{1,0:T(8,128)(2,1)S(1)} collective-permute-done((bf16[1024,256]{1,0:T(8,128)(2,1)S(1)}, bf16[1024,256]{1,0:T(8,128)(2,1)S(1)}, u32[]{:S(2)}, u32[]{:S(2)}) %collective-permute-start.22) | collective-permute-done | bytes 524320 | tf_op jit(solution)/shard_map/ppermute | solution.py:38
  84.3 2.2 %collective-permute-start.23 = (bf16[1024,256]{1,0:T(8,128)(2,1)S(1)}, bf16[1024,256]{1,0:T(8,128)(2,1)S(1)}, u32[]{:S(2)}, u32[]{:S(2)}) collective-permute-start(bf16[1024,256]{1,0:T(8,128)(2,1)S(1)} %collective-permute-done.22.refs_1_), channel_id=1, source_target_pairs={{0,32},{4,228},{32,64},{36,4},{64,96},{68,36},{96,128},{100,68},{1... | collective-permute-start | bytes 1572872 | tf_op jit(solution)/shard_map/ppermute | solution.py:38
  86.5 3.4 %collective-permute-done.18.refs_1_ = bf16[1024,256]{1,0:T(8,128)(2,1)S(1)} collective-permute-done((bf16[1024,256]{1,0:T(8,128)(2,1)S(1)}, bf16[1024,256]{1,0:T(8,128)(2,1)S(1)}, u32[]{:S(2)}, u32[]{:S(2)}) %collective-permute-start.18) | collective-permute-done | bytes 524320 | tf_op jit(solution)/shard_map/ppermute | solution.py:38
  90.0 2.2 %collective-permute-start.19 = (bf16[1024,256]{1,0:T(8,128)(2,1)S(1)}, bf16[1024,256]{1,0:T(8,128)(2,1)S(1)}, u32[]{:S(2)}, u32[]{:S(2)}) collective-permute-start(bf16[1024,256]{1,0:T(8,128)(2,1)S(1)} %collective-permute-done.18.refs_1_), channel_id=1, source_target_pairs={{0,32},{4,228},{32,64},{36,4},{64,96},{68,36},{96,128},{100,68},{1... | collective-permute-start | bytes 1572872 | tf_op jit(solution)/shard_map/ppermute | solution.py:38
  92.2 1.9 %shard_map.76 = bf16[1024,128]{1,0:T(8,128)(2,1)S(1)} custom-call(s32[4]{0:T(128)S(1)} %pad_add_fusion.i_ref, bf16[256,2048]{1,0:T(8,128)(2,1)S(1)} %get-tuple-element.23.t_ref, bf16[512,512]{1,0:T(8,128)(2,1)S(1)} %get-tuple-element.29.column, bf16[768,512]{1,0:T(8,128)(2,1)S(1)} %shard_map.75.rest, bf16[768,512]{1,0:T(8,128)(2,1)S(1)} %collective-permute-done.12.got, ...), custom_call_target="tpu_custom_call" | custom-call | bytes 4194304 | tf_op jit(solution)/shard_map/pallas_call | solution.py:62
  94.3 1.7 %collective-permute-start.27 = (bf16[256,512]{1,0:T(8,128)(2,1)S(1)}, bf16[256,512]{1,0:T(8,128)(2,1)S(1)}, u32[]{:S(2)}, u32[]{:S(2)}) collective-permute-start(bf16[256,512]{1,0:T(8,128)(2,1)S(1)} %get-tuple-element.40), channel_id=1, source_target_pairs={{0,16},{8,24},{16,0},{24,8},{1,17},{9,25},{17,1},{25,9},{2,18},{10... | collective-permute-start | bytes 786440 | tf_op jit(solution)/shard_map/ppermute | solution.py:42
  96.0 1.8 %collective-permute-start.24 = (bf16[1024,256]{1,0:T(8,128)(2,1)S(1)}, bf16[1024,256]{1,0:T(8,128)(2,1)S(1)}, u32[]{:S(2)}, u32[]{:S(2)}) collective-permute-start(bf16[1024,256]{1,0:T(8,128)(2,1)S(1)} %collective-permute-done.23.refs_2_), channel_id=1, source_target_pairs={{0,32},{4,228},{32,64},{36,4},{64,96},{68,36},{96,128},{100,68},{1... | collective-permute-start | bytes 1572872 | tf_op jit(solution)/shard_map/ppermute | solution.py:38
  97.8 3.4 %collective-permute-done.19.refs_1_ = bf16[1024,256]{1,0:T(8,128)(2,1)S(1)} collective-permute-done((bf16[1024,256]{1,0:T(8,128)(2,1)S(1)}, bf16[1024,256]{1,0:T(8,128)(2,1)S(1)}, u32[]{:S(2)}, u32[]{:S(2)}) %collective-permute-start.19) | collective-permute-done | bytes 524320 | tf_op jit(solution)/shard_map/ppermute | solution.py:38
  101.2 2.2 %collective-permute-start.20 = (bf16[1024,256]{1,0:T(8,128)(2,1)S(1)}, bf16[1024,256]{1,0:T(8,128)(2,1)S(1)}, u32[]{:S(2)}, u32[]{:S(2)}) collective-permute-start(bf16[1024,256]{1,0:T(8,128)(2,1)S(1)} %collective-permute-done.19.refs_1_), channel_id=1, source_target_pairs={{0,32},{4,228},{32,64},{36,4},{64,96},{68,36},{96,128},{100,68},{1... | collective-permute-start | bytes 1572872 | tf_op jit(solution)/shard_map/ppermute | solution.py:38
  103.4 6.3 %attend.6 = (f32[2048,128]{1,0:T(8,128)S(1)}, f32[2048,256]{1,0:T(8,128)S(1)}) custom-call(bf16[2048,128]{1,0:T(8,128)(2,1)S(1)} %pad_maximum_fusion.refs_0_, bf16[1024,256]{1,0:T(8,128)(2,1)S(1)} %constant_dynamic-update-slice_fusion.4.refs_1_, bf16[1024,256]{1,0:T(8,128)(2,1)S(1)} %collective-permute-done.17.refs_2_), custom_call_target="tpu_custom_call" | custom-call | flops 4294967296 | bytes 8388608 | tf_op jit(solution)/shard_map/attend/pallas_call | solution.py:208
  109.7 3.4 %attend.7 = (f32[2048,128]{1,0:T(8,128)S(1)}, f32[2048,256]{1,0:T(8,128)S(1)}) custom-call(bf16[2048,128]{1,0:T(8,128)(2,1)S(1)} %pad_maximum_fusion.refs_0_, bf16[1024,256]{1,0:T(8,128)(2,1)S(1)} %collective-permute-done.22.refs_1_, f32[2048,128]{1,0:T(8,128)S(1)} %get-tuple-element.31.refs_2_, ...), custom_call_target="tpu_custom_call", output_to_operand_aliasing={{0}: (2, {}), {1}: (3, {})} | custom-call | flops 2147483648 | bytes 8388608 | tf_op jit(solution)/shard_map/attend/pallas_call | solution.py:208
  113.1 6.5 %attend.8 = (f32[2048,128]{1,0:T(8,128)S(1)}, f32[2048,256]{1,0:T(8,128)S(1)}) custom-call(bf16[2048,128]{1,0:T(8,128)(2,1)S(1)} %pad_maximum_fusion.refs_0_, bf16[1024,256]{1,0:T(8,128)(2,1)S(1)} %collective-permute-done.18.refs_1_, bf16[1024,256]{1,0:T(8,128)(2,1)S(1)} %collective-permute-done.23.refs_2_, ...), custom_call_target="tpu_custom_call", output_to_operand_aliasing={{0}: (3, {}), {1}: (4, {})} | custom-call | flops 4294967296 | bytes 8388608 | tf_op jit(solution)/shard_map/attend/pallas_call | solution.py:208
  119.6 5.9 %attend.9 = (f32[2048,128]{1,0:T(8,128)S(1)}, f32[2048,256]{1,0:T(8,128)S(1)}) custom-call(bf16[2048,128]{1,0:T(8,128)(2,1)S(1)} %pad_maximum_fusion.refs_0_, bf16[1024,256]{1,0:T(8,128)(2,1)S(1)} %collective-permute-done.19.refs_1_, bf16[1024,256]{1,0:T(8,128)(2,1)S(1)} %collective-permute-done.24.refs_2_, ...), custom_call_target="tpu_custom_call", output_to_operand_aliasing={{0}: (3, {}), {1}: (4, {})} | custom-call | flops 4294967296 | bytes 8388608 | tf_op jit(solution)/shard_map/attend/pallas_call | solution.py:208
  125.5 1.7 %attend.11 = f32[1024,256]{1,0:T(8,128)S(1)} custom-call(bf16[2048,128]{1,0:T(8,128)(2,1)S(1)} %pad_maximum_fusion.refs_0_, bf16[1024,256]{1,0:T(8,128)(2,1)S(1)} %collective-permute-done.20.refs_1_, f32[2048,128]{1,0:T(8,128)S(1)} %get-tuple-element.37.refs_2_, f32[2048,256]{1,0:T(8,128)S(1)} %get-tuple-element.38.refs_3_), custom_call_target="tpu_custom_call" | custom-call | flops 1073741824 | bytes 8388608 | tf_op jit(solution)/shard_map/attend/pallas_call | solution.py:208
  127.4 0.6 shard_map.77.rest
  128.0 0.8 collective-permute-start.28
  128.8 1.7 %attend.10.own_ref = f32[1024,256]{1,0:T(8,128)S(1)} custom-call(bf16[2048,128]{1,0:T(8,128)(2,1)S(1)} %pad_maximum_fusion.refs_0_, bf16[1024,256]{1,0:T(8,128)(2,1)S(1)} %collective-permute-done.20.refs_1_, f32[2048,128]{1,0:T(8,128)S(1)} %get-tuple-element.37.refs_2_, f32[2048,256]{1,0:T(8,128)S(1)} %get-tuple-element.38.refs_3_), custom_call_target="tpu_custom_call" | custom-call | flops 1073741824 | bytes 8388608 | tf_op jit(solution)/shard_map/attend/pallas_call | solution.py:208
  131.2 2.0 %shard_map.78 = bf16[256,2048]{1,0:T(8,128)(2,1)S(1)} custom-call(s32[4]{0:T(128)S(1)} %pad_add_fusion.i_ref, f32[1024,256]{1,0:T(8,128)S(1)} %attend.10.own_ref, f32[1024,256]{1,0:T(8,128)S(1)} %collective-permute-done.25.got_ref, bf16[512,512]{1,0:T(8,128)(2,1)S(1)} %get-tuple-element.39.column, bf16[768,512]{1,0:T(8,128)(2,1)S(1)} %shard_map.77.rest, ...), custom_call_target="tpu_custom_call" | custom-call | bytes 4194304 | tf_op jit(solution)/shard_map/pallas_call | solution.py:62
  133.2 19.6 %all_to_all.10 = bf16[4,64,2048]{2,1,0:T(8,128)(2,1)S(1)} all-to-all(bf16[4,64,2048]{2,1,0:T(8,128)(2,1)S(1)} %bitcast.8), channel_id=1, replica_groups=mesh['sp_0'=8,'sp_1'=4,'sp_2'=2,'tp'=4] {'tp'}, dimensions={0} | all-to-all | bytes 2097152 | tf_op jit(solution)/shard_map/all_to_all | solution.py:317
  153.2 0.8 multiply_convert_fusion
  (53 shorter events, 2.9 us)
Async XLA Ops:
  0.0 39.4 %copy-start = (bf16[64,2048]{1,0:T(8,128)(2,1)S(1)}, bf16[64,2048]{1,0:T(8,128)(2,1)}, u32[]{:S(2)}) copy-start(bf16[64,2048]{1,0:T(8,128)(2,1)} %t0.1) | copy-start | bytes 786436
  0.0 39.4 %copy-start.2 = (f32[128]{0:T(128)S(1)}, f32[128]{0:T(128)}, u32[]{:S(2)}) copy-start(f32[128]{0:T(128)} %param.13) | copy-start | bytes 1540
  1.6 28.4 %all-to-all-start = ((bf16[32,32,256]{2,1,0:T(8,128)(2,1)}), bf16[32,32,256]{2,1,0:T(8,128)(2,1)S(1)}, u32[]{:S(2)}, u32[]{:S(2)}) async-start(bf16[32,32,256]{2,1,0:T(8,128)(2,1)} %broadcast_in_dim.50), calls=%async_computation | async-start | bytes 1048576 | tf_op jit(solution)/shard_map/all_to_all | solution.py:54
  12.8 19.2 %collective-permute-start = (bf16[64,2048]{1,0:T(8,128)(2,1)}, bf16[64,2048]{1,0:T(8,128)(2,1)S(1)}, u32[]{:S(2)}, u32[]{:S(2)}) collective-permute-start(bf16[64,2048]{1,0:T(8,128)(2,1)} %t0.1), channel_id=1, source_target_pairs={{0,3},{1,0},{2,1},{3,2},{4,7},{5,4},{6,5},{7,6},{8,11},{9,8},{10,9... | collective-permute-start | bytes 786440 | tf_op jit(solution)/shard_map/ppermute | solution.py:42
  15.9 16.7 %collective-permute-start.1 = (bf16[64,2048]{1,0:T(8,128)(2,1)}, bf16[64,2048]{1,0:T(8,128)(2,1)S(1)}, u32[]{:S(2)}, u32[]{:S(2)}) collective-permute-start(bf16[64,2048]{1,0:T(8,128)(2,1)} %t0.1), channel_id=1, source_target_pairs={{0,2},{1,3},{2,0},{3,1},{4,6},{5,7},{6,4},{7,5},{8,10},{9,11},{10,... | collective-permute-start | bytes 786440 | tf_op jit(solution)/shard_map/ppermute | solution.py:42
  16.5 18.5 %collective-permute-start.2 = (bf16[64,2048]{1,0:T(8,128)(2,1)}, bf16[64,2048]{1,0:T(8,128)(2,1)S(1)}, u32[]{:S(2)}, u32[]{:S(2)}) collective-permute-start(bf16[64,2048]{1,0:T(8,128)(2,1)} %t0.1), channel_id=1, source_target_pairs={{0,1},{1,2},{2,3},{3,0},{4,5},{5,6},{6,7},{7,4},{8,9},{9,10},{10,1... | collective-permute-start | bytes 786440 | tf_op jit(solution)/shard_map/ppermute | solution.py:42
  18.3 11.7 %collective-permute-start.4 = (bf16[32,1024]{1,0:T(8,128)(2,1)S(1)}, bf16[32,1024]{1,0:T(8,128)(2,1)S(1)}, u32[]{:S(2)}, u32[]{:S(2)}) collective-permute-start(bf16[32,1024]{1,0:T(8,128)(2,1)S(1)} %pad_maximum_fusion.2.own_ref), channel_id=1, source_target_pairs={{0,4},{4,0},{1,5},{5,1},{2,6},{6,2},{3,7},{7,3},{8,12},{12,8},{9,1... | collective-permute-start | bytes 196616 | tf_op jit(solution)/shard_map/ppermute | solution.py:31
  30.0 9.4 %collective-permute-start.3 = (bf16[32,32,256]{2,1,0:T(8,128)(2,1)S(1)}, bf16[32,32,256]{2,1,0:T(8,128)(2,1)S(1)}, u32[]{:S(2)}, u32[]{:S(2)}) collective-permute-start(bf16[32,32,256]{2,1,0:T(8,128)(2,1)S(1)} %all-to-all-done.own), channel_id=1, source_target_pairs={{0,4},{4,0},{1,5},{5,1},{2,6},{6,2},{3,7},{7,3},{8,12},{12,8},{9,1... | collective-permute-start | bytes 1572872 | tf_op jit(solution)/shard_map/ppermute | solution.py:31
  30.8 14.9 %collective-permute-start.5 = (bf16[64,1024]{1,0:T(8,128)(2,1)S(1)}, bf16[64,1024]{1,0:T(8,128)(2,1)S(1)}, u32[]{:S(2)}, u32[]{:S(2)}) collective-permute-start(bf16[64,1024]{1,0:T(8,128)(2,1)S(1)} %pad_maximum_fusion.1), channel_id=1, source_target_pairs={{0,32},{4,228},{32,64},{36,4},{64,96},{68,36},{96,128},{100,68},{1... | collective-permute-start | bytes 393224 | tf_op jit(solution)/shard_map/ppermute | solution.py:49
  32.0 13.7 %collective-permute-start.6 = (bf16[64,1024]{1,0:T(8,128)(2,1)S(1)}, bf16[64,1024]{1,0:T(8,128)(2,1)S(1)}, u32[]{:S(2)}, u32[]{:S(2)}) collective-permute-start(bf16[64,1024]{1,0:T(8,128)(2,1)S(1)} %pad_maximum_fusion.1), channel_id=1, source_target_pairs={{0,64},{4,196},{32,96},{36,228},{64,128},{68,4},{96,160},{100,36},... | collective-permute-start | bytes 393224 | tf_op jit(solution)/shard_map/ppermute | solution.py:49
  32.6 14.6 %collective-permute-start.7 = (bf16[64,1024]{1,0:T(8,128)(2,1)S(1)}, bf16[64,1024]{1,0:T(8,128)(2,1)S(1)}, u32[]{:S(2)}, u32[]{:S(2)}) collective-permute-start(bf16[64,1024]{1,0:T(8,128)(2,1)S(1)} %pad_maximum_fusion.1), channel_id=1, source_target_pairs={{0,96},{4,164},{32,128},{36,196},{64,160},{68,228},{96,192},{100,4... | collective-permute-start | bytes 393224 | tf_op jit(solution)/shard_map/ppermute | solution.py:49
  35.1 10.6 %collective-permute-start.8 = (bf16[32,1024]{1,0:T(8,128)(2,1)S(1)}, bf16[32,1024]{1,0:T(8,128)(2,1)S(1)}, u32[]{:S(2)}, u32[]{:S(2)}) collective-permute-start(bf16[32,1024]{1,0:T(8,128)(2,1)S(1)} %pad_maximum_fusion.2.own_ref), channel_id=1, source_target_pairs={{0,128},{4,132},{32,160},{36,164},{64,192},{68,196},{96,224},{100,... | collective-permute-start | bytes 196616 | tf_op jit(solution)/shard_map/ppermute | solution.py:49
  47.2 44.9 %copy-start.1 = (f32[128]{0:T(128)S(1)}, f32[128]{0:T(128)}, u32[]{:S(2)}) copy-start(f32[128]{0:T(128)} %param.12) | copy-start | bytes 1540
  47.3 10.3 %collective-permute-start.9 = (bf16[224,1024]{1,0:T(8,128)(2,1)S(1)}, bf16[224,1024]{1,0:T(8,128)(2,1)S(1)}, u32[]{:S(2)}, u32[]{:S(2)}) collective-permute-start(bf16[224,1024]{1,0:T(8,128)(2,1)S(1)} %constant_dynamic-update-slice_fusion.mine_ref), channel_id=1, source_target_pairs={{0,4},{4,0},{1,5},{5,1},{2,6},{6,2},{3,7},{7,3},{8,12},{12,8},{9,1... | collective-permute-start | bytes 1376264 | tf_op jit(solution)/shard_map/ppermute | solution.py:31
  47.6 7.9 %collective-permute-start.14 = (bf16[256,256]{1,0:T(8,128)(2,1)S(1)}, bf16[256,256]{1,0:T(8,128)(2,1)S(1)}, u32[]{:S(2)}, u32[]{:S(2)}) collective-permute-start(bf16[256,256]{1,0:T(8,128)(2,1)S(1)} %get-tuple-element.24), channel_id=1, source_target_pairs={{0,16},{8,24},{16,0},{24,8},{1,17},{9,25},{17,1},{25,9},{2,18},{10... | collective-permute-start | bytes 393224 | tf_op jit(solution)/shard_map/ppermute | solution.py:42
  49.2 8.4 %collective-permute-start.15 = (bf16[256,256]{1,0:T(8,128)(2,1)S(1)}, bf16[256,256]{1,0:T(8,128)(2,1)S(1)}, u32[]{:S(2)}, u32[]{:S(2)}) collective-permute-start(bf16[256,256]{1,0:T(8,128)(2,1)S(1)} %get-tuple-element.24), channel_id=1, source_target_pairs={{0,8},{8,16},{16,24},{24,0},{1,9},{9,17},{17,25},{25,1},{2,10},{10... | collective-permute-start | bytes 393224 | tf_op jit(solution)/shard_map/ppermute | solution.py:42
  49.7 8.9 %collective-permute-start.16 = (bf16[256,256]{1,0:T(8,128)(2,1)S(1)}, bf16[256,256]{1,0:T(8,128)(2,1)S(1)}, u32[]{:S(2)}, u32[]{:S(2)}) collective-permute-start(bf16[256,256]{1,0:T(8,128)(2,1)S(1)} %get-tuple-element.24), channel_id=1, source_target_pairs={{0,24},{8,0},{16,8},{24,16},{1,25},{9,1},{17,9},{25,17},{2,26},{10... | collective-permute-start | bytes 393224 | tf_op jit(solution)/shard_map/ppermute | solution.py:42
  58.3 16.1 %collective-permute-start.10 = (bf16[512,512]{1,0:T(8,128)(2,1)S(1)}, bf16[512,512]{1,0:T(8,128)(2,1)S(1)}, u32[]{:S(2)}, u32[]{:S(2)}) collective-permute-start(bf16[512,512]{1,0:T(8,128)(2,1)S(1)} %get-tuple-element.29.column), channel_id=1, source_target_pairs={{0,8},{4,28},{8,16},{12,4},{16,24},{20,12},{24,0},{28,20},{1,9},{5... | collective-permute-start | bytes 1572872 | tf_op jit(solution)/shard_map/ppermute | solution.py:38
  58.6 16.5 %collective-permute-start.21 = (bf16[1024,256]{1,0:T(8,128)(2,1)S(1)}, bf16[1024,256]{1,0:T(8,128)(2,1)S(1)}, u32[]{:S(2)}, u32[]{:S(2)}) collective-permute-start(bf16[1024,256]{1,0:T(8,128)(2,1)S(1)} %constant_dynamic-update-slice_fusion.4.refs_1_), channel_id=1, source_target_pairs={{0,4},{4,0},{1,5},{5,1},{2,6},{6,2},{3,7},{7,3},{8,12},{12,8},{9,1... | collective-permute-start | bytes 1572872 | tf_op jit(solution)/shard_map/ppermute | solution.py:31
  58.7 18.6 %collective-permute-start.17 = (bf16[1024,256]{1,0:T(8,128)(2,1)S(1)}, bf16[1024,256]{1,0:T(8,128)(2,1)S(1)}, u32[]{:S(2)}, u32[]{:S(2)}) collective-permute-start(bf16[1024,256]{1,0:T(8,128)(2,1)S(1)} %constant_dynamic-update-slice_fusion.4.refs_1_), channel_id=1, source_target_pairs={{0,32},{4,228},{32,64},{36,4},{64,96},{68,36},{96,128},{100,68},{1... | collective-permute-start | bytes 1572872 | tf_op jit(solution)/shard_map/ppermute | solution.py:38
  61.1 12.1 %collective-permute-start.11 = (bf16[256,512]{1,0:T(8,128)(2,1)S(1)}, bf16[256,512]{1,0:T(8,128)(2,1)S(1)}, u32[]{:S(2)}, u32[]{:S(2)}) collective-permute-start(bf16[256,512]{1,0:T(8,128)(2,1)S(1)} %get-tuple-element.30), channel_id=1, source_target_pairs={{0,16},{8,24},{16,0},{24,8},{1,17},{9,25},{17,1},{25,9},{2,18},{10... | collective-permute-start | bytes 786440 | tf_op jit(solution)/shard_map/ppermute | solution.py:42
  75.0 17.2 %collective-permute-start.12 = (bf16[768,512]{1,0:T(8,128)(2,1)S(1)}, bf16[768,512]{1,0:T(8,128)(2,1)S(1)}, u32[]{:S(2)}, u32[]{:S(2)}) collective-permute-start(bf16[768,512]{1,0:T(8,128)(2,1)S(1)} %shard_map.75.rest), channel_id=1, source_target_pairs={{0,4},{4,0},{1,5},{5,1},{2,6},{6,2},{3,7},{7,3},{8,12},{12,8},{9,1... | collective-permute-start | bytes 2359304 | tf_op jit(solution)/shard_map/ppermute | solution.py:31
  75.1 9.3 %collective-permute-start.22 = (bf16[1024,256]{1,0:T(8,128)(2,1)S(1)}, bf16[1024,256]{1,0:T(8,128)(2,1)S(1)}, u32[]{:S(2)}, u32[]{:S(2)}) collective-permute-start(bf16[1024,256]{1,0:T(8,128)(2,1)S(1)} %collective-permute-done.21), channel_id=1, source_target_pairs={{0,32},{4,228},{32,64},{36,4},{64,96},{68,36},{96,128},{100,68},{1... | collective-permute-start | bytes 1572872 | tf_op jit(solution)/shard_map/ppermute | solution.py:38
  77.4 12.6 %collective-permute-start.18 = (bf16[1024,256]{1,0:T(8,128)(2,1)S(1)}, bf16[1024,256]{1,0:T(8,128)(2,1)S(1)}, u32[]{:S(2)}, u32[]{:S(2)}) collective-permute-start(bf16[1024,256]{1,0:T(8,128)(2,1)S(1)} %collective-permute-done.17.refs_2_), channel_id=1, source_target_pairs={{0,32},{4,228},{32,64},{36,4},{64,96},{68,36},{96,128},{100,68},{1... | collective-permute-start | bytes 1572872 | tf_op jit(solution)/shard_map/ppermute | solution.py:38
  84.3 11.6 %collective-permute-start.23 = (bf16[1024,256]{1,0:T(8,128)(2,1)S(1)}, bf16[1024,256]{1,0:T(8,128)(2,1)S(1)}, u32[]{:S(2)}, u32[]{:S(2)}) collective-permute-start(bf16[1024,256]{1,0:T(8,128)(2,1)S(1)} %collective-permute-done.22.refs_1_), channel_id=1, source_target_pairs={{0,32},{4,228},{32,64},{36,4},{64,96},{68,36},{96,128},{100,68},{1... | collective-permute-start | bytes 1572872 | tf_op jit(solution)/shard_map/ppermute | solution.py:38
  90.0 11.2 %collective-permute-start.19 = (bf16[1024,256]{1,0:T(8,128)(2,1)S(1)}, bf16[1024,256]{1,0:T(8,128)(2,1)S(1)}, u32[]{:S(2)}, u32[]{:S(2)}) collective-permute-start(bf16[1024,256]{1,0:T(8,128)(2,1)S(1)} %collective-permute-done.18.refs_1_), channel_id=1, source_target_pairs={{0,32},{4,228},{32,64},{36,4},{64,96},{68,36},{96,128},{100,68},{1... | collective-permute-start | bytes 1572872 | tf_op jit(solution)/shard_map/ppermute | solution.py:38
  94.1 9.3 %collective-permute-start.13 = (bf16[1024,128]{1,0:T(8,128)(2,1)S(1)}, bf16[1024,128]{1,0:T(8,128)(2,1)S(1)}, u32[]{:S(2)}, u32[]{:S(2)}) collective-permute-start(bf16[1024,128]{1,0:T(8,128)(2,1)S(1)} %shard_map.76), channel_id=1, source_target_pairs={{0,4},{4,0},{1,5},{5,1},{2,6},{6,2},{3,7},{7,3},{8,12},{12,8},{9,1... | collective-permute-start | bytes 786440 | tf_op jit(solution)/shard_map/ppermute | solution.py:31
  94.2 33.2 %collective-permute-start.26 = (bf16[512,512]{1,0:T(8,128)(2,1)S(1)}, bf16[512,512]{1,0:T(8,128)(2,1)S(1)}, u32[]{:S(2)}, u32[]{:S(2)}) collective-permute-start(bf16[512,512]{1,0:T(8,128)(2,1)S(1)} %get-tuple-element.39.column), channel_id=1, source_target_pairs={{0,8},{4,28},{8,16},{12,4},{16,24},{20,12},{24,0},{28,20},{1,9},{5... | collective-permute-start | bytes 1572872 | tf_op jit(solution)/shard_map/ppermute | solution.py:38
  94.3 33.1 %collective-permute-start.27 = (bf16[256,512]{1,0:T(8,128)(2,1)S(1)}, bf16[256,512]{1,0:T(8,128)(2,1)S(1)}, u32[]{:S(2)}, u32[]{:S(2)}) collective-permute-start(bf16[256,512]{1,0:T(8,128)(2,1)S(1)} %get-tuple-element.40), channel_id=1, source_target_pairs={{0,16},{8,24},{16,0},{24,8},{1,17},{9,25},{17,1},{25,9},{2,18},{10... | collective-permute-start | bytes 786440 | tf_op jit(solution)/shard_map/ppermute | solution.py:42
  96.0 23.7 %collective-permute-start.24 = (bf16[1024,256]{1,0:T(8,128)(2,1)S(1)}, bf16[1024,256]{1,0:T(8,128)(2,1)S(1)}, u32[]{:S(2)}, u32[]{:S(2)}) collective-permute-start(bf16[1024,256]{1,0:T(8,128)(2,1)S(1)} %collective-permute-done.23.refs_2_), channel_id=1, source_target_pairs={{0,32},{4,228},{32,64},{36,4},{64,96},{68,36},{96,128},{100,68},{1... | collective-permute-start | bytes 1572872 | tf_op jit(solution)/shard_map/ppermute | solution.py:38
  101.2 24.3 %collective-permute-start.20 = (bf16[1024,256]{1,0:T(8,128)(2,1)S(1)}, bf16[1024,256]{1,0:T(8,128)(2,1)S(1)}, u32[]{:S(2)}, u32[]{:S(2)}) collective-permute-start(bf16[1024,256]{1,0:T(8,128)(2,1)S(1)} %collective-permute-done.19.refs_1_), channel_id=1, source_target_pairs={{0,32},{4,228},{32,64},{36,4},{64,96},{68,36},{96,128},{100,68},{1... | collective-permute-start | bytes 1572872 | tf_op jit(solution)/shard_map/ppermute | solution.py:38
  127.3 3.9 %collective-permute-start.25 = (f32[1024,256]{1,0:T(8,128)S(1)}, f32[1024,256]{1,0:T(8,128)S(1)}, u32[]{:S(2)}, u32[]{:S(2)}) collective-permute-start(f32[1024,256]{1,0:T(8,128)S(1)} %attend.11), channel_id=1, source_target_pairs={{0,4},{4,0},{1,5},{5,1},{2,6},{6,2},{3,7},{7,3},{8,12},{12,8},{9,1... | collective-permute-start | bytes 3145736 | tf_op jit(solution)/shard_map/ppermute | solution.py:31
  128.0 3.1 %collective-permute-start.28 = (bf16[768,512]{1,0:T(8,128)(2,1)S(1)}, bf16[768,512]{1,0:T(8,128)(2,1)S(1)}, u32[]{:S(2)}, u32[]{:S(2)}) collective-permute-start(bf16[768,512]{1,0:T(8,128)(2,1)S(1)} %shard_map.77.rest), channel_id=1, source_target_pairs={{0,4},{4,0},{1,5},{5,1},{2,6},{6,2},{3,7},{7,3},{8,12},{12,8},{9,1... | collective-permute-start | bytes 2359304 | tf_op jit(solution)/shard_map/ppermute | solution.py:31

commit v4 on v3

--- a/solution.py
+++ b/solution.py
@@ -224,8 +224,11 @@
     return out if last is None else out[0]
 
 
-def project_out_kernel(i_ref, own_ref, got_ref, column, rest, rest_got, out_ref, w_ref, at_ref):
-    fill_rows(i_ref, w_ref, column, rest, rest_got)
+def fill_kernel(i_ref, column, rest, got, w_ref):
+    fill_rows(i_ref, w_ref, column, rest, got)
+
+
+def project_out_kernel(i_ref, own_ref, got_ref, w_ref, out_ref, at_ref):
     rows = own_ref.shape[0] // GROUP
     for h in range(GROUP):
         mine, theirs = own_ref[h * rows : (h + 1) * rows], got_ref[h * rows : (h + 1) * rows]
@@ -309,9 +312,10 @@
     theirs = attend(q_all, todo[7:], carry, 1024, last=1)
     got = other_core(theirs)
     own = attend(q_all, todo[7:], carry, 1024, last=0)
+    (wo_rows,) = call(fill_kernel, [((tokens.shape[1], GROUP * HEAD_DIM), BF16)], where, *wo_all)
     (partial,) = call(
-        project_out_kernel, [((rows, tokens.shape[1]), BF16)], where, own, got, *wo_all,
-        scratch=[pltpu.VMEM((2048, 512), BF16), pltpu.VMEM((rows, GROUP * HEAD_DIM), BF16)],
+        project_out_kernel, [((rows, tokens.shape[1]), BF16)], where, own, got, wo_rows,
+        scratch=[pltpu.VMEM((rows, GROUP * HEAD_DIM), BF16)],
     )
     pieces = partial.reshape(NY, -1, partial.shape[1])
     summed = jnp.sum(lax.all_to_all(pieces, Y, 0, 0).astype(F32), axis=0)

time: 154 us -> 158 us (1.026)
  waiting for transfers between devices: 49 us -> 50.8 us
  Pallas kernels: 32.7 us -> 34.3 us
    ppermute x8, waiting for transfers between devices: 0.59 us -> 2.34 us  [other_core(): return lax.ppermute(piece, C, [(0, 1), (1, 0)])]
    pallas_call x6 -> x7, Pallas kernels: 7.18 us -> 7.77 us  [call(): pl.pallas_call(kernel, in_specs=[SCALARS] + [WHOLE] * (len(args) - 1), ou...]
  transfers between devices with their start and end apart: 30 -> 30, of which waited for: 11 -> 11; matrix products, arithmetic and copies ran while one was open for 1% -> 1% of each run, Pallas kernels for 20% -> 21%
where the time goes in v4:
time: 158 us; the launch traced here: 157 us
  waiting for transfers between devices  50.8 us (32%)
  starting transfers between devices  47.2 us (30%)
  Pallas kernels  34.3 us (22%)
  blocking collectives  19.7 us (12%)
  other arithmetic  4.12 us (3%)
    pallas_call x6, Pallas kernels, attend(): pl.pallas_call(functools.partial(attend_kernel, pieces=pieces, chunk=chun...  26.5 us
    all_to_all x1, blocking collectives, local(): summed = jnp.sum(lax.all_to_all(pieces, Y, 0, 0).astype(F32), axis=0)  19.7 us
    ppermute x8, waiting for transfers between devices, shift(): lax.ppermute(piece, axis, [(i, (i + by) % count) for i in range(count)])  15.4 us
    ppermute x9, waiting for transfers between devices, turn(): return lax.ppermute(piece, (axis, C), pairs)  14.9 us
    ppermute x9, starting transfers between devices, turn(): return lax.ppermute(piece, (axis, C), pairs)  13.5 us
    ppermute x8, starting transfers between devices, shift(): lax.ppermute(piece, axis, [(i, (i + by) % count) for i in range(count)])  13 us
    all_to_all x1, waiting for transfers between devices, everyone(): lax.all_to_all(jnp.broadcast_to(piece[None], (n,) + piece.shape), axes, 0...  11.7 us
    all_to_all x1, starting transfers between devices, everyone(): lax.all_to_all(jnp.broadcast_to(piece[None], (n,) + piece.shape), axes, 0...  11.2 us
  transfers between devices with their start and end apart: 30, of which 11 were waited for; matrix products, arithmetic and copies ran while one was open for 1% of the time, Pallas kernels for 21%

profile of v4, /device:TPU:32, one launch (start us, length us, event | category | flops | bytes accessed | tf_op | source)
XLA Modules:
  0.0 157.3 jit_solution(14748879430849840340)
XLA Ops:
  0.0 0.8 pad_maximum_fusion.3
  0.8 0.9 broadcast_in_dim.50
  1.6 11.2 %all-to-all-start = ((bf16[32,32,256]{2,1,0:T(8,128)(2,1)}), bf16[32,32,256]{2,1,0:T(8,128)(2,1)S(1)}, u32[]{:S(2)}, u32[]{:S(2)}) async-start(bf16[32,32,256]{2,1,0:T(8,128)(2,1)} %broadcast_in_dim.50), calls=%async_computation | async-start | bytes 1048576 | tf_op jit(solution)/shard_map/all_to_all | solution.py:54
  12.8 3.1 %collective-permute-start = (bf16[64,2048]{1,0:T(8,128)(2,1)}, bf16[64,2048]{1,0:T(8,128)(2,1)S(1)}, u32[]{:S(2)}, u32[]{:S(2)}) collective-permute-start(bf16[64,2048]{1,0:T(8,128)(2,1)} %t0.1), channel_id=1, source_target_pairs={{0,3},{1,0},{2,1},{3,2},{4,7},{5,4},{6,5},{7,6},{8,11},{9,8},{10,9... | collective-permute-start | bytes 786440 | tf_op jit(solution)/shard_map/ppermute | solution.py:42
  15.9 0.6 collective-permute-start.1
  16.5 1.0 collective-permute-start.2
  17.5 0.8 pad_maximum_fusion.2.own_ref
  18.3 11.7 %all-to-all-done.own = bf16[32,32,256]{2,1,0:T(8,128)(2,1)S(1)} async-done(((bf16[32,32,256]{2,1,0:T(8,128)(2,1)}), bf16[32,32,256]{2,1,0:T(8,128)(2,1)S(1)}, u32[]{:S(2)}, u32[]{:S(2)}) %all-to-all-start) | async-done | bytes 524320 | tf_op jit(solution)/shard_map/all_to_all | solution.py:54
  30.0 0.8 pad_maximum_fusion.1
  30.8 1.2 collective-permute-start.5
  32.0 0.6 collective-permute-start.6
  32.6 1.9 %collective-permute-start.7 = (bf16[64,1024]{1,0:T(8,128)(2,1)S(1)}, bf16[64,1024]{1,0:T(8,128)(2,1)S(1)}, u32[]{:S(2)}, u32[]{:S(2)}) collective-permute-start(bf16[64,1024]{1,0:T(8,128)(2,1)S(1)} %pad_maximum_fusion.1), channel_id=1, source_target_pairs={{0,96},{4,164},{32,128},{36,196},{64,160},{68,228},{96,192},{100,4... | collective-permute-start | bytes 393224 | tf_op jit(solution)/shard_map/ppermute | solution.py:49
  35.1 4.3 %collective-permute-start.8 = (bf16[32,1024]{1,0:T(8,128)(2,1)S(1)}, bf16[32,1024]{1,0:T(8,128)(2,1)S(1)}, u32[]{:S(2)}, u32[]{:S(2)}) collective-permute-start(bf16[32,1024]{1,0:T(8,128)(2,1)S(1)} %pad_maximum_fusion.2.own_ref), channel_id=1, source_target_pairs={{0,128},{4,132},{32,160},{36,164},{64,192},{68,196},{96,224},{100,... | collective-permute-start | bytes 196616 | tf_op jit(solution)/shard_map/ppermute | solution.py:49
  39.4 1.4 shard_map.73
  40.8 4.9 %collective-permute-done.8 = bf16[32,1024]{1,0:T(8,128)(2,1)S(1)} collective-permute-done((bf16[32,1024]{1,0:T(8,128)(2,1)S(1)}, bf16[32,1024]{1,0:T(8,128)(2,1)S(1)}, u32[]{:S(2)}, u32[]{:S(2)}) %collective-permute-start.8) | collective-permute-done | bytes 65568 | tf_op jit(solution)/shard_map/ppermute | solution.py:49
  45.7 1.5 collective-permute-done.7
  47.6 1.5 collective-permute-start.14
  49.7 2.7 %collective-permute-start.16 = (bf16[256,256]{1,0:T(8,128)(2,1)S(1)}, bf16[256,256]{1,0:T(8,128)(2,1)S(1)}, u32[]{:S(2)}, u32[]{:S(2)}) collective-permute-start(bf16[256,256]{1,0:T(8,128)(2,1)S(1)} %get-tuple-element.24), channel_id=1, source_target_pairs={{0,24},{8,0},{16,8},{24,16},{1,25},{9,1},{17,9},{25,17},{2,26},{10... | collective-permute-start | bytes 393224 | tf_op jit(solution)/shard_map/ppermute | solution.py:42
  52.5 3.0 %collective-permute-done.14 = bf16[256,256]{1,0:T(8,128)(2,1)S(1)} collective-permute-done((bf16[256,256]{1,0:T(8,128)(2,1)S(1)}, bf16[256,256]{1,0:T(8,128)(2,1)S(1)}, u32[]{:S(2)}, u32[]{:S(2)}) %collective-permute-start.14) | collective-permute-done | bytes 131104 | tf_op jit(solution)/shard_map/ppermute | solution.py:42
  55.5 2.1 %collective-permute-done.15 = bf16[256,256]{1,0:T(8,128)(2,1)S(1)} collective-permute-done((bf16[256,256]{1,0:T(8,128)(2,1)S(1)}, bf16[256,256]{1,0:T(8,128)(2,1)S(1)}, u32[]{:S(2)}, u32[]{:S(2)}) %collective-permute-start.15) | collective-permute-done | bytes 131104 | tf_op jit(solution)/shard_map/ppermute | solution.py:42
  57.6 0.7 shard_map.74
  58.7 2.4 %collective-permute-start.17 = (bf16[1024,256]{1,0:T(8,128)(2,1)S(1)}, bf16[1024,256]{1,0:T(8,128)(2,1)S(1)}, u32[]{:S(2)}, u32[]{:S(2)}) collective-permute-start(bf16[1024,256]{1,0:T(8,128)(2,1)S(1)} %constant_dynamic-update-slice_fusion.4.refs_1_), channel_id=1, source_target_pairs={{0,32},{4,228},{32,64},{36,4},{64,96},{68,36},{96,128},{100,68},{1... | collective-permute-start | bytes 1572872 | tf_op jit(solution)/shard_map/ppermute | solution.py:38
  61.1 1.8 %collective-permute-start.11 = (bf16[256,512]{1,0:T(8,128)(2,1)S(1)}, bf16[256,512]{1,0:T(8,128)(2,1)S(1)}, u32[]{:S(2)}, u32[]{:S(2)}) collective-permute-start(bf16[256,512]{1,0:T(8,128)(2,1)S(1)} %get-tuple-element.30), channel_id=1, source_target_pairs={{0,16},{8,24},{16,0},{24,8},{1,17},{9,25},{17,1},{25,9},{2,18},{10... | collective-permute-start | bytes 786440 | tf_op jit(solution)/shard_map/ppermute | solution.py:42
  63.0 10.3 %collective-permute-done.11.far_ref = bf16[256,512]{1,0:T(8,128)(2,1)S(1)} collective-permute-done((bf16[256,512]{1,0:T(8,128)(2,1)S(1)}, bf16[256,512]{1,0:T(8,128)(2,1)S(1)}, u32[]{:S(2)}, u32[]{:S(2)}) %collective-permute-start.11) | collective-permute-done | bytes 262176 | tf_op jit(solution)/shard_map/ppermute | solution.py:42
  73.3 1.1 collective-permute-done.10.near_ref
  75.1 2.3 %collective-permute-start.22 = (bf16[1024,256]{1,0:T(8,128)(2,1)S(1)}, bf16[1024,256]{1,0:T(8,128)(2,1)S(1)}, u32[]{:S(2)}, u32[]{:S(2)}) collective-permute-start(bf16[1024,256]{1,0:T(8,128)(2,1)S(1)} %collective-permute-done.21), channel_id=1, source_target_pairs={{0,32},{4,228},{32,64},{36,4},{64,96},{68,36},{96,128},{100,68},{1... | collective-permute-start | bytes 1572872 | tf_op jit(solution)/shard_map/ppermute | solution.py:38
  77.4 6.9 %collective-permute-done.22.refs_1_ = bf16[1024,256]{1,0:T(8,128)(2,1)S(1)} collective-permute-done((bf16[1024,256]{1,0:T(8,128)(2,1)S(1)}, bf16[1024,256]{1,0:T(8,128)(2,1)S(1)}, u32[]{:S(2)}, u32[]{:S(2)}) %collective-permute-start.22) | collective-permute-done | bytes 524320 | tf_op jit(solution)/shard_map/ppermute | solution.py:38
  84.3 2.2 %collective-permute-start.23 = (bf16[1024,256]{1,0:T(8,128)(2,1)S(1)}, bf16[1024,256]{1,0:T(8,128)(2,1)S(1)}, u32[]{:S(2)}, u32[]{:S(2)}) collective-permute-start(bf16[1024,256]{1,0:T(8,128)(2,1)S(1)} %collective-permute-done.22.refs_1_), channel_id=1, source_target_pairs={{0,32},{4,228},{32,64},{36,4},{64,96},{68,36},{96,128},{100,68},{1... | collective-permute-start | bytes 1572872 | tf_op jit(solution)/shard_map/ppermute | solution.py:38
  86.5 3.4 %collective-permute-done.18.refs_1_ = bf16[1024,256]{1,0:T(8,128)(2,1)S(1)} collective-permute-done((bf16[1024,256]{1,0:T(8,128)(2,1)S(1)}, bf16[1024,256]{1,0:T(8,128)(2,1)S(1)}, u32[]{:S(2)}, u32[]{:S(2)}) %collective-permute-start.18) | collective-permute-done | bytes 524320 | tf_op jit(solution)/shard_map/ppermute | solution.py:38
  90.0 2.2 %collective-permute-start.19 = (bf16[1024,256]{1,0:T(8,128)(2,1)S(1)}, bf16[1024,256]{1,0:T(8,128)(2,1)S(1)}, u32[]{:S(2)}, u32[]{:S(2)}) collective-permute-start(bf16[1024,256]{1,0:T(8,128)(2,1)S(1)} %collective-permute-done.18.refs_1_), channel_id=1, source_target_pairs={{0,32},{4,228},{32,64},{36,4},{64,96},{68,36},{96,128},{100,68},{1... | collective-permute-start | bytes 1572872 | tf_op jit(solution)/shard_map/ppermute | solution.py:38
  92.2 1.9 %shard_map.76 = bf16[1024,128]{1,0:T(8,128)(2,1)S(1)} custom-call(s32[4]{0:T(128)S(1)} %pad_add_fusion.i_ref, bf16[256,2048]{1,0:T(8,128)(2,1)S(1)} %get-tuple-element.23.t_ref, bf16[512,512]{1,0:T(8,128)(2,1)S(1)} %get-tuple-element.29.column, bf16[768,512]{1,0:T(8,128)(2,1)S(1)} %shard_map.75.rest, bf16[768,512]{1,0:T(8,128)(2,1)S(1)} %collective-permute-done.12.got, ...), custom_call_target="tpu_custom_call" | custom-call | bytes 4194304 | tf_op jit(solution)/shard_map/pallas_call | solution.py:62
  94.3 1.7 %collective-permute-start.27 = (bf16[256,512]{1,0:T(8,128)(2,1)S(1)}, bf16[256,512]{1,0:T(8,128)(2,1)S(1)}, u32[]{:S(2)}, u32[]{:S(2)}) collective-permute-start(bf16[256,512]{1,0:T(8,128)(2,1)S(1)} %get-tuple-element.40), channel_id=1, source_target_pairs={{0,16},{8,24},{16,0},{24,8},{1,17},{9,25},{17,1},{25,9},{2,18},{10... | collective-permute-start | bytes 786440 | tf_op jit(solution)/shard_map/ppermute | solution.py:42
  96.0 1.8 %collective-permute-start.24 = (bf16[1024,256]{1,0:T(8,128)(2,1)S(1)}, bf16[1024,256]{1,0:T(8,128)(2,1)S(1)}, u32[]{:S(2)}, u32[]{:S(2)}) collective-permute-start(bf16[1024,256]{1,0:T(8,128)(2,1)S(1)} %collective-permute-done.23.refs_2_), channel_id=1, source_target_pairs={{0,32},{4,228},{32,64},{36,4},{64,96},{68,36},{96,128},{100,68},{1... | collective-permute-start | bytes 1572872 | tf_op jit(solution)/shard_map/ppermute | solution.py:38
  97.8 3.4 %collective-permute-done.19.refs_1_ = bf16[1024,256]{1,0:T(8,128)(2,1)S(1)} collective-permute-done((bf16[1024,256]{1,0:T(8,128)(2,1)S(1)}, bf16[1024,256]{1,0:T(8,128)(2,1)S(1)}, u32[]{:S(2)}, u32[]{:S(2)}) %collective-permute-start.19) | collective-permute-done | bytes 524320 | tf_op jit(solution)/shard_map/ppermute | solution.py:38
  101.2 2.2 %collective-permute-start.20 = (bf16[1024,256]{1,0:T(8,128)(2,1)S(1)}, bf16[1024,256]{1,0:T(8,128)(2,1)S(1)}, u32[]{:S(2)}, u32[]{:S(2)}) collective-permute-start(bf16[1024,256]{1,0:T(8,128)(2,1)S(1)} %collective-permute-done.19.refs_1_), channel_id=1, source_target_pairs={{0,32},{4,228},{32,64},{36,4},{64,96},{68,36},{96,128},{100,68},{1... | collective-permute-start | bytes 1572872 | tf_op jit(solution)/shard_map/ppermute | solution.py:38
  103.4 6.4 %attend.6 = (f32[2048,128]{1,0:T(8,128)S(1)}, f32[2048,256]{1,0:T(8,128)S(1)}) custom-call(bf16[2048,128]{1,0:T(8,128)(2,1)S(1)} %pad_maximum_fusion.refs_0_, bf16[1024,256]{1,0:T(8,128)(2,1)S(1)} %constant_dynamic-update-slice_fusion.4.refs_1_, bf16[1024,256]{1,0:T(8,128)(2,1)S(1)} %collective-permute-done.17.refs_2_), custom_call_target="tpu_custom_call" | custom-call | flops 4294967296 | bytes 8388608 | tf_op jit(solution)/shard_map/attend/pallas_call | solution.py:208
  109.8 3.5 %attend.7 = (f32[2048,128]{1,0:T(8,128)S(1)}, f32[2048,256]{1,0:T(8,128)S(1)}) custom-call(bf16[2048,128]{1,0:T(8,128)(2,1)S(1)} %pad_maximum_fusion.refs_0_, bf16[1024,256]{1,0:T(8,128)(2,1)S(1)} %collective-permute-done.22.refs_1_, f32[2048,128]{1,0:T(8,128)S(1)} %get-tuple-element.31.refs_2_, ...), custom_call_target="tpu_custom_call", output_to_operand_aliasing={{0}: (2, {}), {1}: (3, {})} | custom-call | flops 2147483648 | bytes 8388608 | tf_op jit(solution)/shard_map/attend/pallas_call | solution.py:208
  113.3 6.8 %attend.8 = (f32[2048,128]{1,0:T(8,128)S(1)}, f32[2048,256]{1,0:T(8,128)S(1)}) custom-call(bf16[2048,128]{1,0:T(8,128)(2,1)S(1)} %pad_maximum_fusion.refs_0_, bf16[1024,256]{1,0:T(8,128)(2,1)S(1)} %collective-permute-done.18.refs_1_, bf16[1024,256]{1,0:T(8,128)(2,1)S(1)} %collective-permute-done.23.refs_2_, ...), custom_call_target="tpu_custom_call", output_to_operand_aliasing={{0}: (3, {}), {1}: (4, {})} | custom-call | flops 4294967296 | bytes 8388608 | tf_op jit(solution)/shard_map/attend/pallas_call | solution.py:208
  120.1 6.2 %attend.9 = (f32[2048,128]{1,0:T(8,128)S(1)}, f32[2048,256]{1,0:T(8,128)S(1)}) custom-call(bf16[2048,128]{1,0:T(8,128)(2,1)S(1)} %pad_maximum_fusion.refs_0_, bf16[1024,256]{1,0:T(8,128)(2,1)S(1)} %collective-permute-done.19.refs_1_, bf16[1024,256]{1,0:T(8,128)(2,1)S(1)} %collective-permute-done.24.refs_2_, ...), custom_call_target="tpu_custom_call", output_to_operand_aliasing={{0}: (3, {}), {1}: (4, {})} | custom-call | flops 4294967296 | bytes 8388608 | tf_op jit(solution)/shard_map/attend/pallas_call | solution.py:208
  126.4 1.8 %attend.11 = f32[1024,256]{1,0:T(8,128)S(1)} custom-call(bf16[2048,128]{1,0:T(8,128)(2,1)S(1)} %pad_maximum_fusion.refs_0_, bf16[1024,256]{1,0:T(8,128)(2,1)S(1)} %collective-permute-done.20.refs_1_, f32[2048,128]{1,0:T(8,128)S(1)} %get-tuple-element.37.refs_2_, f32[2048,256]{1,0:T(8,128)S(1)} %get-tuple-element.38.refs_3_), custom_call_target="tpu_custom_call" | custom-call | flops 1073741824 | bytes 8388608 | tf_op jit(solution)/shard_map/attend/pallas_call | solution.py:208
  128.3 0.6 shard_map.77.rest
  128.9 0.8 collective-permute-start.28
  129.8 2.3 %collective-permute-done.28.got = bf16[768,512]{1,0:T(8,128)(2,1)S(1)} collective-permute-done((bf16[768,512]{1,0:T(8,128)(2,1)S(1)}, bf16[768,512]{1,0:T(8,128)(2,1)S(1)}, u32[]{:S(2)}, u32[]{:S(2)}) %collective-permute-start.28) | collective-permute-done | bytes 786464 | tf_op jit(solution)/shard_map/ppermute | solution.py:31
  132.1 0.8 shard_map.78.w_ref
  132.9 1.8 %attend.10.own_ref = f32[1024,256]{1,0:T(8,128)S(1)} custom-call(bf16[2048,128]{1,0:T(8,128)(2,1)S(1)} %pad_maximum_fusion.refs_0_, bf16[1024,256]{1,0:T(8,128)(2,1)S(1)} %collective-permute-done.20.refs_1_, f32[2048,128]{1,0:T(8,128)S(1)} %get-tuple-element.37.refs_2_, f32[2048,256]{1,0:T(8,128)S(1)} %get-tuple-element.38.refs_3_), custom_call_target="tpu_custom_call" | custom-call | flops 1073741824 | bytes 8388608 | tf_op jit(solution)/shard_map/attend/pallas_call | solution.py:208
  134.7 1.8 %shard_map.79 = bf16[256,2048]{1,0:T(8,128)(2,1)S(1)} custom-call(s32[4]{0:T(128)S(1)} %pad_add_fusion.i_ref, f32[1024,256]{1,0:T(8,128)S(1)} %attend.10.own_ref, f32[1024,256]{1,0:T(8,128)S(1)} %collective-permute-done.25.got_ref, bf16[2048,512]{1,0:T(8,128)(2,1)S(1)} %shard_map.78.w_ref), custom_call_target="tpu_custom_call" | custom-call | bytes 4194304 | tf_op jit(solution)/shard_map/pallas_call | solution.py:62
  136.6 19.7 %all_to_all.10 = bf16[4,64,2048]{2,1,0:T(8,128)(2,1)S(1)} all-to-all(bf16[4,64,2048]{2,1,0:T(8,128)(2,1)S(1)} %bitcast.8), channel_id=1, replica_groups=mesh['sp_0'=8,'sp_1'=4,'sp_2'=2,'tp'=4] {'tp'}, dimensions={0} | all-to-all | bytes 2097152 | tf_op jit(solution)/shard_map/all_to_all | solution.py:321
  156.5 0.8 multiply_convert_fusion
  (54 shorter events, 3.5 us)
Async XLA Ops:
  0.0 39.4 %copy-start = (bf16[64,2048]{1,0:T(8,128)(2,1)S(1)}, bf16[64,2048]{1,0:T(8,128)(2,1)}, u32[]{:S(2)}) copy-start(bf16[64,2048]{1,0:T(8,128)(2,1)} %t0.1) | copy-start | bytes 786436
  0.0 39.4 %copy-start.2 = (f32[128]{0:T(128)S(1)}, f32[128]{0:T(128)}, u32[]{:S(2)}) copy-start(f32[128]{0:T(128)} %param.13) | copy-start | bytes 1540
  1.6 28.4 %all-to-all-start = ((bf16[32,32,256]{2,1,0:T(8,128)(2,1)}), bf16[32,32,256]{2,1,0:T(8,128)(2,1)S(1)}, u32[]{:S(2)}, u32[]{:S(2)}) async-start(bf16[32,32,256]{2,1,0:T(8,128)(2,1)} %broadcast_in_dim.50), calls=%async_computation | async-start | bytes 1048576 | tf_op jit(solution)/shard_map/all_to_all | solution.py:54
  12.8 19.2 %collective-permute-start = (bf16[64,2048]{1,0:T(8,128)(2,1)}, bf16[64,2048]{1,0:T(8,128)(2,1)S(1)}, u32[]{:S(2)}, u32[]{:S(2)}) collective-permute-start(bf16[64,2048]{1,0:T(8,128)(2,1)} %t0.1), channel_id=1, source_target_pairs={{0,3},{1,0},{2,1},{3,2},{4,7},{5,4},{6,5},{7,6},{8,11},{9,8},{10,9... | collective-permute-start | bytes 786440 | tf_op jit(solution)/shard_map/ppermute | solution.py:42
  15.9 16.7 %collective-permute-start.1 = (bf16[64,2048]{1,0:T(8,128)(2,1)}, bf16[64,2048]{1,0:T(8,128)(2,1)S(1)}, u32[]{:S(2)}, u32[]{:S(2)}) collective-permute-start(bf16[64,2048]{1,0:T(8,128)(2,1)} %t0.1), channel_id=1, source_target_pairs={{0,2},{1,3},{2,0},{3,1},{4,6},{5,7},{6,4},{7,5},{8,10},{9,11},{10,... | collective-permute-start | bytes 786440 | tf_op jit(solution)/shard_map/ppermute | solution.py:42
  16.5 18.5 %collective-permute-start.2 = (bf16[64,2048]{1,0:T(8,128)(2,1)}, bf16[64,2048]{1,0:T(8,128)(2,1)S(1)}, u32[]{:S(2)}, u32[]{:S(2)}) collective-permute-start(bf16[64,2048]{1,0:T(8,128)(2,1)} %t0.1), channel_id=1, source_target_pairs={{0,1},{1,2},{2,3},{3,0},{4,5},{5,6},{6,7},{7,4},{8,9},{9,10},{10,1... | collective-permute-start | bytes 786440 | tf_op jit(solution)/shard_map/ppermute | solution.py:42
  18.3 11.7 %collective-permute-start.4 = (bf16[32,1024]{1,0:T(8,128)(2,1)S(1)}, bf16[32,1024]{1,0:T(8,128)(2,1)S(1)}, u32[]{:S(2)}, u32[]{:S(2)}) collective-permute-start(bf16[32,1024]{1,0:T(8,128)(2,1)S(1)} %pad_maximum_fusion.2.own_ref), channel_id=1, source_target_pairs={{0,4},{4,0},{1,5},{5,1},{2,6},{6,2},{3,7},{7,3},{8,12},{12,8},{9,1... | collective-permute-start | bytes 196616 | tf_op jit(solution)/shard_map/ppermute | solution.py:31
  30.0 9.4 %collective-permute-start.3 = (bf16[32,32,256]{2,1,0:T(8,128)(2,1)S(1)}, bf16[32,32,256]{2,1,0:T(8,128)(2,1)S(1)}, u32[]{:S(2)}, u32[]{:S(2)}) collective-permute-start(bf16[32,32,256]{2,1,0:T(8,128)(2,1)S(1)} %all-to-all-done.own), channel_id=1, source_target_pairs={{0,4},{4,0},{1,5},{5,1},{2,6},{6,2},{3,7},{7,3},{8,12},{12,8},{9,1... | collective-permute-start | bytes 1572872 | tf_op jit(solution)/shard_map/ppermute | solution.py:31
  30.8 14.9 %collective-permute-start.5 = (bf16[64,1024]{1,0:T(8,128)(2,1)S(1)}, bf16[64,1024]{1,0:T(8,128)(2,1)S(1)}, u32[]{:S(2)}, u32[]{:S(2)}) collective-permute-start(bf16[64,1024]{1,0:T(8,128)(2,1)S(1)} %pad_maximum_fusion.1), channel_id=1, source_target_pairs={{0,32},{4,228},{32,64},{36,4},{64,96},{68,36},{96,128},{100,68},{1... | collective-permute-start | bytes 393224 | tf_op jit(solution)/shard_map/ppermute | solution.py:49
  32.0 13.7 %collective-permute-start.6 = (bf16[64,1024]{1,0:T(8,128)(2,1)S(1)}, bf16[64,1024]{1,0:T(8,128)(2,1)S(1)}, u32[]{:S(2)}, u32[]{:S(2)}) collective-permute-start(bf16[64,1024]{1,0:T(8,128)(2,1)S(1)} %pad_maximum_fusion.1), channel_id=1, source_target_pairs={{0,64},{4,196},{32,96},{36,228},{64,128},{68,4},{96,160},{100,36},... | collective-permute-start | bytes 393224 | tf_op jit(solution)/shard_map/ppermute | solution.py:49
  32.6 14.6 %collective-permute-start.7 = (bf16[64,1024]{1,0:T(8,128)(2,1)S(1)}, bf16[64,1024]{1,0:T(8,128)(2,1)S(1)}, u32[]{:S(2)}, u32[]{:S(2)}) collective-permute-start(bf16[64,1024]{1,0:T(8,128)(2,1)S(1)} %pad_maximum_fusion.1), channel_id=1, source_target_pairs={{0,96},{4,164},{32,128},{36,196},{64,160},{68,228},{96,192},{100,4... | collective-permute-start | bytes 393224 | tf_op jit(solution)/shard_map/ppermute | solution.py:49
  35.1 10.6 %collective-permute-start.8 = (bf16[32,1024]{1,0:T(8,128)(2,1)S(1)}, bf16[32,1024]{1,0:T(8,128)(2,1)S(1)}, u32[]{:S(2)}, u32[]{:S(2)}) collective-permute-start(bf16[32,1024]{1,0:T(8,128)(2,1)S(1)} %pad_maximum_fusion.2.own_ref), channel_id=1, source_target_pairs={{0,128},{4,132},{32,160},{36,164},{64,192},{68,196},{96,224},{100,... | collective-permute-start | bytes 196616 | tf_op jit(solution)/shard_map/ppermute | solution.py:49
  47.2 44.9 %copy-start.1 = (f32[128]{0:T(128)S(1)}, f32[128]{0:T(128)}, u32[]{:S(2)}) copy-start(f32[128]{0:T(128)} %param.12) | copy-start | bytes 1540
  47.3 10.3 %collective-permute-start.9 = (bf16[224,1024]{1,0:T(8,128)(2,1)S(1)}, bf16[224,1024]{1,0:T(8,128)(2,1)S(1)}, u32[]{:S(2)}, u32[]{:S(2)}) collective-permute-start(bf16[224,1024]{1,0:T(8,128)(2,1)S(1)} %constant_dynamic-update-slice_fusion.mine_ref), channel_id=1, source_target_pairs={{0,4},{4,0},{1,5},{5,1},{2,6},{6,2},{3,7},{7,3},{8,12},{12,8},{9,1... | collective-permute-start | bytes 1376264 | tf_op jit(solution)/shard_map/ppermute | solution.py:31
  47.6 7.9 %collective-permute-start.14 = (bf16[256,256]{1,0:T(8,128)(2,1)S(1)}, bf16[256,256]{1,0:T(8,128)(2,1)S(1)}, u32[]{:S(2)}, u32[]{:S(2)}) collective-permute-start(bf16[256,256]{1,0:T(8,128)(2,1)S(1)} %get-tuple-element.24), channel_id=1, source_target_pairs={{0,16},{8,24},{16,0},{24,8},{1,17},{9,25},{17,1},{25,9},{2,18},{10... | collective-permute-start | bytes 393224 | tf_op jit(solution)/shard_map/ppermute | solution.py:42
  49.2 8.4 %collective-permute-start.15 = (bf16[256,256]{1,0:T(8,128)(2,1)S(1)}, bf16[256,256]{1,0:T(8,128)(2,1)S(1)}, u32[]{:S(2)}, u32[]{:S(2)}) collective-permute-start(bf16[256,256]{1,0:T(8,128)(2,1)S(1)} %get-tuple-element.24), channel_id=1, source_target_pairs={{0,8},{8,16},{16,24},{24,0},{1,9},{9,17},{17,25},{25,1},{2,10},{10... | collective-permute-start | bytes 393224 | tf_op jit(solution)/shard_map/ppermute | solution.py:42
  49.7 8.9 %collective-permute-start.16 = (bf16[256,256]{1,0:T(8,128)(2,1)S(1)}, bf16[256,256]{1,0:T(8,128)(2,1)S(1)}, u32[]{:S(2)}, u32[]{:S(2)}) collective-permute-start(bf16[256,256]{1,0:T(8,128)(2,1)S(1)} %get-tuple-element.24), channel_id=1, source_target_pairs={{0,24},{8,0},{16,8},{24,16},{1,25},{9,1},{17,9},{25,17},{2,26},{10... | collective-permute-start | bytes 393224 | tf_op jit(solution)/shard_map/ppermute | solution.py:42
  58.3 16.1 %collective-permute-start.10 = (bf16[512,512]{1,0:T(8,128)(2,1)S(1)}, bf16[512,512]{1,0:T(8,128)(2,1)S(1)}, u32[]{:S(2)}, u32[]{:S(2)}) collective-permute-start(bf16[512,512]{1,0:T(8,128)(2,1)S(1)} %get-tuple-element.29.column), channel_id=1, source_target_pairs={{0,8},{4,28},{8,16},{12,4},{16,24},{20,12},{24,0},{28,20},{1,9},{5... | collective-permute-start | bytes 1572872 | tf_op jit(solution)/shard_map/ppermute | solution.py:38
  58.6 16.5 %collective-permute-start.21 = (bf16[1024,256]{1,0:T(8,128)(2,1)S(1)}, bf16[1024,256]{1,0:T(8,128)(2,1)S(1)}, u32[]{:S(2)}, u32[]{:S(2)}) collective-permute-start(bf16[1024,256]{1,0:T(8,128)(2,1)S(1)} %constant_dynamic-update-slice_fusion.4.refs_1_), channel_id=1, source_target_pairs={{0,4},{4,0},{1,5},{5,1},{2,6},{6,2},{3,7},{7,3},{8,12},{12,8},{9,1... | collective-permute-start | bytes 1572872 | tf_op jit(solution)/shard_map/ppermute | solution.py:31
  58.7 18.6 %collective-permute-start.17 = (bf16[1024,256]{1,0:T(8,128)(2,1)S(1)}, bf16[1024,256]{1,0:T(8,128)(2,1)S(1)}, u32[]{:S(2)}, u32[]{:S(2)}) collective-permute-start(bf16[1024,256]{1,0:T(8,128)(2,1)S(1)} %constant_dynamic-update-slice_fusion.4.refs_1_), channel_id=1, source_target_pairs={{0,32},{4,228},{32,64},{36,4},{64,96},{68,36},{96,128},{100,68},{1... | collective-permute-start | bytes 1572872 | tf_op jit(solution)/shard_map/ppermute | solution.py:38
  61.1 12.1 %collective-permute-start.11 = (bf16[256,512]{1,0:T(8,128)(2,1)S(1)}, bf16[256,512]{1,0:T(8,128)(2,1)S(1)}, u32[]{:S(2)}, u32[]{:S(2)}) collective-permute-start(bf16[256,512]{1,0:T(8,128)(2,1)S(1)} %get-tuple-element.30), channel_id=1, source_target_pairs={{0,16},{8,24},{16,0},{24,8},{1,17},{9,25},{17,1},{25,9},{2,18},{10... | collective-permute-start | bytes 786440 | tf_op jit(solution)/shard_map/ppermute | solution.py:42
  75.0 17.2 %collective-permute-start.12 = (bf16[768,512]{1,0:T(8,128)(2,1)S(1)}, bf16[768,512]{1,0:T(8,128)(2,1)S(1)}, u32[]{:S(2)}, u32[]{:S(2)}) collective-permute-start(bf16[768,512]{1,0:T(8,128)(2,1)S(1)} %shard_map.75.rest), channel_id=1, source_target_pairs={{0,4},{4,0},{1,5},{5,1},{2,6},{6,2},{3,7},{7,3},{8,12},{12,8},{9,1... | collective-permute-start | bytes 2359304 | tf_op jit(solution)/shard_map/ppermute | solution.py:31
  75.1 9.3 %collective-permute-start.22 = (bf16[1024,256]{1,0:T(8,128)(2,1)S(1)}, bf16[1024,256]{1,0:T(8,128)(2,1)S(1)}, u32[]{:S(2)}, u32[]{:S(2)}) collective-permute-start(bf16[1024,256]{1,0:T(8,128)(2,1)S(1)} %collective-permute-done.21), channel_id=1, source_target_pairs={{0,32},{4,228},{32,64},{36,4},{64,96},{68,36},{96,128},{100,68},{1... | collective-permute-start | bytes 1572872 | tf_op jit(solution)/shard_map/ppermute | solution.py:38
  77.4 12.6 %collective-permute-start.18 = (bf16[1024,256]{1,0:T(8,128)(2,1)S(1)}, bf16[1024,256]{1,0:T(8,128)(2,1)S(1)}, u32[]{:S(2)}, u32[]{:S(2)}) collective-permute-start(bf16[1024,256]{1,0:T(8,128)(2,1)S(1)} %collective-permute-done.17.refs_2_), channel_id=1, source_target_pairs={{0,32},{4,228},{32,64},{36,4},{64,96},{68,36},{96,128},{100,68},{1... | collective-permute-start | bytes 1572872 | tf_op jit(solution)/shard_map/ppermute | solution.py:38
  84.3 11.6 %collective-permute-start.23 = (bf16[1024,256]{1,0:T(8,128)(2,1)S(1)}, bf16[1024,256]{1,0:T(8,128)(2,1)S(1)}, u32[]{:S(2)}, u32[]{:S(2)}) collective-permute-start(bf16[1024,256]{1,0:T(8,128)(2,1)S(1)} %collective-permute-done.22.refs_1_), channel_id=1, source_target_pairs={{0,32},{4,228},{32,64},{36,4},{64,96},{68,36},{96,128},{100,68},{1... | collective-permute-start | bytes 1572872 | tf_op jit(solution)/shard_map/ppermute | solution.py:38
  90.0 11.2 %collective-permute-start.19 = (bf16[1024,256]{1,0:T(8,128)(2,1)S(1)}, bf16[1024,256]{1,0:T(8,128)(2,1)S(1)}, u32[]{:S(2)}, u32[]{:S(2)}) collective-permute-start(bf16[1024,256]{1,0:T(8,128)(2,1)S(1)} %collective-permute-done.18.refs_1_), channel_id=1, source_target_pairs={{0,32},{4,228},{32,64},{36,4},{64,96},{68,36},{96,128},{100,68},{1... | collective-permute-start | bytes 1572872 | tf_op jit(solution)/shard_map/ppermute | solution.py:38
  94.1 9.3 %collective-permute-start.13 = (bf16[1024,128]{1,0:T(8,128)(2,1)S(1)}, bf16[1024,128]{1,0:T(8,128)(2,1)S(1)}, u32[]{:S(2)}, u32[]{:S(2)}) collective-permute-start(bf16[1024,128]{1,0:T(8,128)(2,1)S(1)} %shard_map.76), channel_id=1, source_target_pairs={{0,4},{4,0},{1,5},{5,1},{2,6},{6,2},{3,7},{7,3},{8,12},{12,8},{9,1... | collective-permute-start | bytes 786440 | tf_op jit(solution)/shard_map/ppermute | solution.py:31
  94.2 34.1 %collective-permute-start.26 = (bf16[512,512]{1,0:T(8,128)(2,1)S(1)}, bf16[512,512]{1,0:T(8,128)(2,1)S(1)}, u32[]{:S(2)}, u32[]{:S(2)}) collective-permute-start(bf16[512,512]{1,0:T(8,128)(2,1)S(1)} %get-tuple-element.39.column), channel_id=1, source_target_pairs={{0,8},{4,28},{8,16},{12,4},{16,24},{20,12},{24,0},{28,20},{1,9},{5... | collective-permute-start | bytes 1572872 | tf_op jit(solution)/shard_map/ppermute | solution.py:38
  94.3 34.0 %collective-permute-start.27 = (bf16[256,512]{1,0:T(8,128)(2,1)S(1)}, bf16[256,512]{1,0:T(8,128)(2,1)S(1)}, u32[]{:S(2)}, u32[]{:S(2)}) collective-permute-start(bf16[256,512]{1,0:T(8,128)(2,1)S(1)} %get-tuple-element.40), channel_id=1, source_target_pairs={{0,16},{8,24},{16,0},{24,8},{1,17},{9,25},{17,1},{25,9},{2,18},{10... | collective-permute-start | bytes 786440 | tf_op jit(solution)/shard_map/ppermute | solution.py:42
  96.0 24.2 %collective-permute-start.24 = (bf16[1024,256]{1,0:T(8,128)(2,1)S(1)}, bf16[1024,256]{1,0:T(8,128)(2,1)S(1)}, u32[]{:S(2)}, u32[]{:S(2)}) collective-permute-start(bf16[1024,256]{1,0:T(8,128)(2,1)S(1)} %collective-permute-done.23.refs_2_), channel_id=1, source_target_pairs={{0,32},{4,228},{32,64},{36,4},{64,96},{68,36},{96,128},{100,68},{1... | collective-permute-start | bytes 1572872 | tf_op jit(solution)/shard_map/ppermute | solution.py:38
  101.2 25.2 %collective-permute-start.20 = (bf16[1024,256]{1,0:T(8,128)(2,1)S(1)}, bf16[1024,256]{1,0:T(8,128)(2,1)S(1)}, u32[]{:S(2)}, u32[]{:S(2)}) collective-permute-start(bf16[1024,256]{1,0:T(8,128)(2,1)S(1)} %collective-permute-done.19.refs_1_), channel_id=1, source_target_pairs={{0,32},{4,228},{32,64},{36,4},{64,96},{68,36},{96,128},{100,68},{1... | collective-permute-start | bytes 1572872 | tf_op jit(solution)/shard_map/ppermute | solution.py:38
  128.2 6.5 %collective-permute-start.25 = (f32[1024,256]{1,0:T(8,128)S(1)}, f32[1024,256]{1,0:T(8,128)S(1)}, u32[]{:S(2)}, u32[]{:S(2)}) collective-permute-start(f32[1024,256]{1,0:T(8,128)S(1)} %attend.11), channel_id=1, source_target_pairs={{0,4},{4,0},{1,5},{5,1},{2,6},{6,2},{3,7},{7,3},{8,12},{12,8},{9,1... | collective-permute-start | bytes 3145736 | tf_op jit(solution)/shard_map/ppermute | solution.py:31
  128.9 3.1 %collective-permute-start.28 = (bf16[768,512]{1,0:T(8,128)(2,1)S(1)}, bf16[768,512]{1,0:T(8,128)(2,1)S(1)}, u32[]{:S(2)}, u32[]{:S(2)}) collective-permute-start(bf16[768,512]{1,0:T(8,128)(2,1)S(1)} %shard_map.77.rest), channel_id=1, source_target_pairs={{0,4},{4,0},{1,5},{5,1},{2,6},{6,2},{3,7},{7,3},{8,12},{12,8},{9,1... | collective-permute-start | bytes 2359304 | tf_op jit(solution)/shard_map/ppermute | solution.py:31
